TPU v7x, 256 devices: a whole 4x4x8 slice. The times are simulated.
256 devices in a mesh: sp: 64 (over z, y, core), tp: 4 (over x).
Axes of the slice: x: 4, y: 4, z: 8, core: 2. Of those that a mesh axis runs over, the one named last changes fastest.
Arguments:
- tokens: bfloat16 [16384, 2048], P('sp', 'tp'), may hold values from -6 to 6
- in_gain: float32 [2048], replicated, may hold values from 0.1 to 1.9
- query_down: bfloat16 [2048, 512], replicated, may hold values from -0.125 to 0.125
- latent_down: bfloat16 [2048, 256], replicated, may hold values from -0.125 to 0.125
- rope_down: bfloat16 [2048, 32], replicated, may hold values from -0.125 to 0.125
- query_gain: float32 [512], replicated, may hold values from 0.5 to 12
- latent_gain: float32 [256], replicated, may hold values from 0.5 to 12
- query_nope: bfloat16 [512, 1024], P(None, 'tp'), may hold values from -0.25 to 0.25
- query_rope: bfloat16 [512, 512], P(None, 'tp'), may hold values from -0.25 to 0.25
- key_up: bfloat16 [256, 1024], P(None, 'tp'), may hold values from -0.375 to 0.375
- value_up: bfloat16 [256, 1024], P(None, 'tp'), may hold values from -0.375 to 0.375
- conv_value: bfloat16 [2048, 2048], P(None, 'tp'), may hold values from -0.125 to 0.125
- conv_gate: bfloat16 [2048, 2048], P(None, 'tp'), may hold values from -0.125 to 0.125
- conv_taps: float32 [31, 2048], P(None, 'tp'), may hold values from -1 to 1
- conv_bias: float32 [2048], P('tp'), may hold values from 0.05 to 2.25
- channel_gain: float32 [2048], P('tp'), may hold values from 0.1 to 1.9
- out_attend: bfloat16 [1024, 2048], P('tp'), may hold values from -0.109375 to 0.109375
- out_conv: bfloat16 [2048, 2048], P('tp'), may hold values from -0.109375 to 0.109375
Outputs:
- mixed: bfloat16 [16384, 2048], P('sp', 'tp')
All inputs are finite; a program needn't handle non-finite values.
Results may differ from a plain program's by a relative error of at most 0.013.
The roundings to bfloat16 on the way count: a program that leaves them out, or rounds other values in their place, can miss the bound.
Values may be sent and summed in bfloat16 or wider, within the bound.
A program may use at most 128 MiB of HBM per device.

v0:
```python
import math

import jax
import jax.numpy as jnp
from jax import lax
from jax.sharding import PartitionSpec as P

eps_norm = 1e-06
eps_layer = 1e-05
theta = 10000.0


def laid_out(blocks, dim):
    dims = list(blocks.shape[1:])
    dims[dim] *= blocks.shape[0]
    return jnp.moveaxis(blocks, 0, dim).reshape(dims)


def sent_to_all(shard, axis):
    copies = jnp.broadcast_to(shard, (lax.axis_size(axis), *shard.shape))
    return lax.all_to_all(copies, axis, split_axis=0, concat_axis=0, tiled=True)


def gather_directly(shard, axis, dim):
    return laid_out(sent_to_all(shard, axis), dim)


def sent_together(arrays, axis, dim, along):
    ends, at = ([], 0)
    for a in arrays[:-1]:
        at += a.shape[along]
        ends.append(at)
    both = jnp.concatenate(arrays, axis=along)
    return tuple(jnp.split(lax.all_gather(both, axis, axis=dim, tiled=True), ends, axis=along))


def padded_2(cells, sides, width):
    for axis, dim in sides:
        count = lax.axis_size(axis)
        ends = count - 1
        head = lax.slice_in_dim(cells, 0, width, axis=dim)
        tail = lax.slice_in_dim(cells, cells.shape[dim] - width, cells.shape[dim], axis=dim)
        cells = jnp.concatenate(
            [
                lax.ppermute(tail, axis, [(i, (i + 1) % count) for i in range(ends)]),
                cells,
                lax.ppermute(head, axis, [((i + 1) % count, i) for i in range(ends)]),
            ],
            axis=dim,
        )
    return cells


def over_copies(shard, axis):
    return sent_to_all(shard, axis).sum(axis=0)


def cut_along(shard, dim, peers):
    dims = shard.shape
    blocks = shard.reshape(*dims[:dim], peers, dims[dim] // peers, *dims[dim + 1 :])
    return jnp.moveaxis(blocks, dim, 0)


def sum_at_owner(shard, axis, dim):
    blocks = cut_along(shard, dim, lax.axis_size(axis))
    arrived = lax.all_to_all(blocks, axis, split_axis=0, concat_axis=0, tiled=True)
    return arrived.astype(jnp.float32).sum(axis=0)


def rms_scale(values, gain):
    return values * lax.rsqrt(jnp.mean(values * values, axis=-1, keepdims=True) + eps_norm) * gain


def rotate(values, positions):
    half = values.shape[-1] // 2
    freqs = theta ** (-jnp.arange(half).astype(jnp.float32) / half)
    angles = positions[..., None] * freqs
    cosine = jnp.cos(angles)
    sine = jnp.sin(angles)
    first = values[..., :half]
    second = values[..., half:]
    return jnp.concatenate(
        [first * cosine - second * sine, second * cosine + first * sine], axis=-1
    )


def attend_block(state, q_heads, r_heads, k_nope, values, rope_key):
    highest, total, weighted = state
    heads = q_heads.shape[1]
    key_heads = k_nope.reshape(k_nope.shape[0], heads, -1)
    value_heads = values.reshape(values.shape[0], heads, -1)
    score_scale = (q_heads.shape[2] + r_heads.shape[2]) ** (-0.5)
    scores = (
        jnp.einsum("qhd,khd->hqk", q_heads, key_heads, preferred_element_type=jnp.float32)
        + jnp.einsum("qhd,kd->hqk", r_heads, rope_key, preferred_element_type=jnp.float32)
    ) * score_scale
    new_high = jnp.maximum(highest, jnp.max(scores, axis=-1))
    factor = jnp.exp(highest - new_high)
    weight = jnp.exp(scores - new_high[..., None])
    total = total * factor + jnp.sum(weight, axis=-1)
    weighted = weighted * factor[..., None] + jnp.einsum(
        "hqk,khd->hqd", weight.astype(jnp.bfloat16), value_heads, preferred_element_type=jnp.float32
    )
    return (new_high, total, weighted)


def over_blocks(state, arrays, step):
    count = arrays[0].shape[0]
    size = math.gcd(count, 1024)
    shaped = tuple((item.reshape((count // size, size) + item.shape[1:]) for item in arrays))

    def one_block(carry, block):
        return (step(carry, block), None)

    state, unused = lax.scan(one_block, state, shaped)
    return state


def per_device(
    tokens,
    in_gain,
    query_down,
    latent_down,
    rope_down,
    query_gain,
    latent_gain,
    query_nope,
    query_rope,
    key_up,
    value_up,
    conv_value,
    conv_gate,
    conv_taps,
    conv_bias,
    channel_gain,
    out_attend,
    out_conv,
):
    row_count = tokens.shape[0]
    width = in_gain.shape[0]
    local_ch = conv_value.shape[1]
    positions = (lax.axis_index("sp") * row_count + jnp.arange(row_count)).astype(jnp.float32)
    piece_f = gather_directly(tokens, "tp", 1).astype(jnp.float32)
    scaled = (piece_f * in_gain).astype(jnp.bfloat16)

    def add_rows(weight):
        return jnp.dot(scaled, weight, preferred_element_type=jnp.float32)

    square_sum = jnp.sum(piece_f * piece_f, axis=1)
    q_pre = add_rows(query_down)
    kv_pre = add_rows(latent_down)
    rope_pre = add_rows(rope_down)
    value_pre = add_rows(conv_value)
    gate_pre = add_rows(conv_gate)
    row_scale = lax.rsqrt(square_sum / width + eps_norm)[:, None]
    q_latent = rms_scale(row_scale * q_pre, query_gain).astype(jnp.bfloat16)
    kv_latent = rms_scale(row_scale * kv_pre, latent_gain).astype(jnp.bfloat16)
    rope_key = rotate(row_scale * rope_pre, positions).astype(jnp.bfloat16)
    rope_size = rope_down.shape[1]
    heads = query_rope.shape[1] // rope_size
    q_heads = (
        jnp.dot(q_latent, query_nope, preferred_element_type=jnp.float32)
        .astype(jnp.bfloat16)
        .reshape(row_count, heads, -1)
    )
    q_turn = jnp.dot(q_latent, query_rope, preferred_element_type=jnp.float32).reshape(
        row_count, heads, rope_size
    )
    r_heads = rotate(q_turn, positions[:, None]).astype(jnp.bfloat16)
    value_size = value_up.shape[1] // heads
    start_state = (
        jnp.full((heads, row_count), -jnp.inf, jnp.float32),
        jnp.zeros((heads, row_count), jnp.float32),
        jnp.zeros((heads, row_count, value_size), jnp.float32),
    )
    own_keys = jnp.dot(kv_latent, key_up, preferred_element_type=jnp.float32).astype(jnp.bfloat16)
    own_values = jnp.dot(kv_latent, value_up, preferred_element_type=jnp.float32).astype(
        jnp.bfloat16
    )

    def head_step(state, block):
        return attend_block(state, q_heads, r_heads, block[0], block[1], block[2])

    highest, total, weighted = over_blocks(
        start_state, sent_together((own_keys, own_values, rope_key), "sp", 0, 1), head_step
    )
    attended = jnp.transpose((weighted / total[..., None]).astype(jnp.bfloat16), (1, 0, 2)).reshape(
        row_count, heads * value_size
    )
    glu = (row_scale * value_pre * jax.nn.sigmoid(row_scale * gate_pre)).astype(jnp.bfloat16)
    taps = conv_taps.shape[0]
    padded = padded_2(glu, (("sp", 0),), taps // 2).astype(jnp.float32)
    conv = jnp.zeros((row_count, local_ch), jnp.float32) + conv_bias
    for tap in range(taps):
        conv = conv + conv_taps[tap] * padded[tap : tap + row_count]
    channels = local_ch * lax.axis_size("tp")
    mean = over_copies(jnp.sum(conv, axis=-1), "tp")[:, None] / channels
    centred = conv - mean
    spread = over_copies(jnp.sum(centred * centred, axis=-1), "tp")[:, None] / channels
    activated = jax.nn.silu(centred * lax.rsqrt(spread + eps_layer) * channel_gain).astype(
        jnp.bfloat16
    )
    contract = (((0,), (1,)), ((), ()))
    summed = sum_at_owner(
        (
            lax.dot_general(out_attend, attended, contract, preferred_element_type=jnp.float32)
            + lax.dot_general(out_conv, activated, contract, preferred_element_type=jnp.float32)
        ).astype(jnp.bfloat16),
        "tp",
        0,
    )
    return jnp.transpose(summed).astype(jnp.bfloat16)


def solution(mesh):
    in_specs = (
        P("sp", "tp"),
        P(),
        P(),
        P(),
        P(),
        P(),
        P(),
        P(None, "tp"),
        P(None, "tp"),
        P(None, "tp"),
        P(None, "tp"),
        P(None, "tp"),
        P(None, "tp"),
        P(None, "tp"),
        P("tp"),
        P("tp"),
        P("tp", None),
        P("tp", None),
    )
    out_specs = P("sp", "tp")
    return jax.shard_map(
        per_device, mesh=mesh, in_specs=in_specs, out_specs=out_specs, check_vma=False
    )
```

profile of v0, /device:TPU:1, one launch (start us, length us, event | category | flops | bytes accessed | tf_op | source)
XLA Modules:
  0.0 269.6 jit_solution(14440085917408073910)
XLA Ops:
  8.8 5.0 %all-to-all-start = ((bf16[4,256,512]{1,2,0:T(8,128)(2,1)}), bf16[4,256,512]{1,2,0:T(8,128)(2,1)S(1)}, u32[]{:S(2)}, u32[]{:S(2)}) async-start(bf16[4,256,512]{1,2,0:T(8,128)(2,1)} %broadcast_in_dim.17), calls=%async_computation | async-start | bytes 2097152 | tf_op jit(solution)/shard_map/all_to_all | solution.py:21
  13.8 13.3 %all-to-all-done = bf16[4,256,512]{1,2,0:T(8,128)(2,1)S(1)} async-done(((bf16[4,256,512]{1,2,0:T(8,128)(2,1)}), bf16[4,256,512]{1,2,0:T(8,128)(2,1)S(1)}, u32[]{:S(2)}, u32[]{:S(2)}) %all-to-all-start) | async-done | bytes 1048608 | tf_op jit(solution)/shard_map/all_to_all | solution.py:21
  34.1 2.9 %fusion.18 = f32[256,512]{1,0:T(8,128)S(1)} fusion(bf16[256,2048]{0,1:T(8,128)(2,1)} %copy-done.1, bf16[2048,512]{1,0:T(8,128)(2,1)} %param.32, f32[256]{0:T(256)S(1)} %add_rsqrt_fusion.3), kind=kOutput, calls=%fused_computation.29 | convolution fusion | flops 537395200 | bytes 3671040 | tf_op jit(solution)/shard_map/dot_general | solution.py:147
  37.7 5.8 %collective-permute-start = (bf16[15,512]{1,0:T(8,128)(2,1)S(1)}, bf16[15,512]{1,0:T(8,128)(2,1)S(1)}, u32[]{:S(2)}, u32[]{:S(2)}) collective-permute-start(bf16[15,512]{1,0:T(8,128)(2,1)S(1)} %get-tuple-element.158), channel_id=1, source_target_pairs={{0,4},{4,8},{8,12},{12,16},{16,20},{20,24},{24,28},{28,32},{32,36}... | collective-permute-start | bytes 46088 | tf_op jit(solution)/shard_map/ppermute | solution.py:45
  43.6 1.9 collective-permute-start.1
  47.0 1.6 collective-permute-done.1
  48.7 2.6 fusion.58
  51.9 3.2 %all-to-all-start.1 = ((f32[4,1,256]{2,1,0:T(1,128)}), f32[4,1,256]{2,1,0:T(1,128)S(1)}, u32[]{:S(2)}, u32[]{:S(2)}) async-start(f32[4,1,256]{2,1,0:T(1,128)} %broadcast_in_dim.18), calls=%async_computation.1 | async-start | bytes 8192 | tf_op jit(solution)/shard_map/all_to_all | solution.py:21
  55.2 4.2 %all-to-all-done.1 = f32[4,1,256]{2,1,0:T(1,128)S(1)} async-done(((f32[4,1,256]{2,1,0:T(1,128)}), f32[4,1,256]{2,1,0:T(1,128)S(1)}, u32[]{:S(2)}, u32[]{:S(2)}) %all-to-all-start.1) | async-done | bytes 4128 | tf_op jit(solution)/shard_map/all_to_all | solution.py:21
  60.2 3.2 %all-to-all-start.2 = ((f32[4,1,256]{2,1,0:T(1,128)}), f32[4,1,256]{2,1,0:T(1,128)S(1)}, u32[]{:S(2)}, u32[]{:S(2)}) async-start(f32[4,1,256]{2,1,0:T(1,128)} %broadcast_in_dim.19), calls=%async_computation.2 | async-start | bytes 8192 | tf_op jit(solution)/shard_map/all_to_all | solution.py:21
  63.5 4.1 %all-to-all-done.2 = f32[4,1,256]{2,1,0:T(1,128)S(1)} async-done(((f32[4,1,256]{2,1,0:T(1,128)}), f32[4,1,256]{2,1,0:T(1,128)S(1)}, u32[]{:S(2)}, u32[]{:S(2)}) %all-to-all-start.2) | async-done | bytes 4128 | tf_op jit(solution)/shard_map/all_to_all | solution.py:21
  67.6 76.5 %all-gather.2.cloned.1.call-done = bf16[16384,544]{0,1:T(8,128)(2,1)} async-done(((bf16[256,544]{0,1:T(8,128)(2,1)}), bf16[16384,544]{0,1:T(8,128)(2,1)}) %all-gather.2.cloned.1.call-update) | async-done | bytes 17825808 | tf_op jit(solution)/shard_map/all_gather | solution.py:34
  146.5 6.7 %fusion.61 = (bf16[16384,256]{0,1:T(8,128)(2,1)S(1)}, bf16[16384,256]{0,1:T(8,128)(2,1)S(1)}) fusion(bf16[16384,544]{0,1:T(8,128)(2,1)} %all-gather.2.cloned.1.call-done), kind=kLoop, calls=%fused_computation.134 | loop fusion | bytes 33554432 | tf_op jit(solution)/shard_map/split | solution.py:34
  153.2 6.2 %copy_bitcast_fusion = (bf16[16,1024,256]{1,2,0:T(8,128)(2,1)}, bf16[16,1024,256]{1,2,0:T(8,128)(2,1)}) fusion(bf16[32,16,8,1024]{3,2,1,0:T(8,128)(2,1)S(1)} %bitcast.109, bf16[32,16,8,1024]{3,2,1,0:T(8,128)(2,1)S(1)} %bitcast.110), kind=kLoop, calls=%fused_computation.18 | loop fusion | bytes 33554432
  159.4 81.2 %while.15 = (s32[]{:T(128)}, f32[4,256]{1,0:T(4,128)S(1)}, f32[4,256]{1,0:T(4,128)S(1)}, f32[4,256,64]{1,2,0:T(8,128)S(1)}, bf16[16,1024,256]{1,2,0:T(8,128)(2,1...) while((s32[]{:T(128)}, f32[4,256]{1,0:T(4,128)S(1)}, ...), condition=%wide.region_6.7_spmd.clone, body=%wide.region_3.6_spmd.clone.sunk | while | flops 343086080 | bytes 24969352 | solution.py:115
  161.5 1.6 fusion.104
  166.6 1.6 fusion.104
  171.6 1.6 fusion.104
  176.7 1.6 fusion.104
  192.0 1.6 fusion.104
  212.3 1.6 fusion.104
  232.6 1.6 fusion.104
  240.7 1.7 fusion.66
  243.4 18.4 %all_to_all.22 = bf16[4,512,256]{1,2,0:T(8,128)(2,1)S(1)} all-to-all(bf16[4,512,256]{1,2,0:T(8,128)(2,1)S(1)} %bitcast.112), channel_id=1, replica_groups=mesh['sp'=64,'tp'=4] {'tp'}, dimensions={0} | all-to-all | bytes 2097152 | tf_op jit(solution)/shard_map/all_to_all | solution.py:66
  (195 shorter events, 86.4 us)
Async XLA Ops:
  6.5 235.9 %copy-start = (bf16[512,2048]{1,0:T(8,128)(2,1)S(1)}, bf16[512,2048]{1,0:T(8,128)(2,1)}, u32[]{:S(2)}) copy-start(bf16[512,2048]{1,0:T(8,128)(2,1)} %param.37) | copy-start | bytes 6291460
  6.5 20.9 %copy-start.7 = (f32[2048]{0:T(1024)S(1)}, f32[2048]{0:T(1024)}, u32[]{:S(2)}) copy-start(f32[2048]{0:T(1024)} %param.21) | copy-start | bytes 24580
  6.5 21.3 %copy-start.6 = (bf16[2048,32]{0,1:T(8,128)(2,1)S(1)}, bf16[2048,32]{0,1:T(8,128)(2,1)}, u32[]{:S(2)}) copy-start(bf16[2048,32]{0,1:T(8,128)(2,1)} %param.24) | copy-start | bytes 393220
  8.8 20.6 %copy-start.4 = (bf16[256,256]{1,0:T(8,128)(2,1)S(1)}, bf16[256,256]{1,0:T(8,128)(2,1)}, u32[]{:S(2)}) copy-start(bf16[256,256]{1,0:T(8,128)(2,1)} %param.30) | copy-start | bytes 393220
  8.8 20.6 %copy-start.9 = (f32[256]{0:T(256)S(1)}, f32[256]{0:T(256)}, u32[]{:S(2)}) copy-start(f32[256]{0:T(256)} %param.26) | copy-start | bytes 3076
  8.8 18.3 %all-to-all-start = ((bf16[4,256,512]{1,2,0:T(8,128)(2,1)}), bf16[4,256,512]{1,2,0:T(8,128)(2,1)S(1)}, u32[]{:S(2)}, u32[]{:S(2)}) async-start(bf16[4,256,512]{1,2,0:T(8,128)(2,1)} %broadcast_in_dim.17), calls=%async_computation | async-start | bytes 2097152 | tf_op jit(solution)/shard_map/all_to_all | solution.py:21
  13.8 130.3 %all-gather.2.cloned.1.call-start = ((), (), s32[]{:S(2)}) async-start(), calls=%async_computation.4 | async-start | bytes 18104320 | tf_op jit(solution)/shard_map/all_gather | solution.py:34
  27.1 1.7 copy-start.13
  27.8 1.0 copy-start.1
  29.4 7.5 %copy-start.2 = (bf16[256,2048]{0,1:T(8,128)(2,1)S(1)}, bf16[256,2048]{0,1:T(8,128)(2,1)}, u32[]{:S(2)}) copy-start(bf16[256,2048]{0,1:T(8,128)(2,1)} %copy-done.1) | copy-start | bytes 3145732
  31.8 5.1 %copy-start.11 = (bf16[2048,512]{1,0:T(8,128)(2,1)S(1)}, bf16[2048,512]{1,0:T(8,128)(2,1)}, u32[]{:S(2)}) copy-start(bf16[2048,512]{1,0:T(8,128)(2,1)} %param.31) | copy-start | bytes 6291460
  34.0 11.4 %copy-start.12 = (bf16[2048,512]{1,0:T(8,128)(2,1)S(1)}, bf16[2048,512]{1,0:T(8,128)(2,1)}, u32[]{:S(2)}) copy-start(bf16[2048,512]{1,0:T(8,128)(2,1)} %param.22) | copy-start | bytes 6291460
  37.0 9.4 %copy-start.3 = (bf16[512,256]{1,0:T(8,128)(2,1)S(1)}, bf16[512,256]{1,0:T(8,128)(2,1)}, u32[]{:S(2)}) copy-start(bf16[512,256]{1,0:T(8,128)(2,1)} %param.27) | copy-start | bytes 786436
  37.0 9.4 %copy-start.8 = (f32[512]{0:T(512)S(1)}, f32[512]{0:T(512)}, u32[]{:S(2)}) copy-start(f32[512]{0:T(512)} %param.25) | copy-start | bytes 6148
  37.0 9.7 %copy-start.5 = (bf16[512,128]{1,0:T(8,128)(2,1)S(1)}, bf16[512,128]{1,0:T(8,128)(2,1)}, u32[]{:S(2)}) copy-start(bf16[512,128]{1,0:T(8,128)(2,1)} %param.28) | copy-start | bytes 393220
  37.7 11.0 %copy-start.10 = (f32[512]{0:T(512)S(1)}, f32[512]{0:T(512)}, u32[]{:S(2)}) copy-start(f32[512]{0:T(512)} %param.34) | copy-start | bytes 6148
  37.7 9.3 %collective-permute-start = (bf16[15,512]{1,0:T(8,128)(2,1)S(1)}, bf16[15,512]{1,0:T(8,128)(2,1)S(1)}, u32[]{:S(2)}, u32[]{:S(2)}) collective-permute-start(bf16[15,512]{1,0:T(8,128)(2,1)S(1)} %get-tuple-element.158), channel_id=1, source_target_pairs={{0,4},{4,8},{8,12},{12,16},{16,20},{20,24},{24,28},{28,32},{32,36}... | collective-permute-start | bytes 46088 | tf_op jit(solution)/shard_map/ppermute | solution.py:45
  43.6 5.1 %collective-permute-start.1 = (bf16[15,512]{1,0:T(8,128)(2,1)S(1)}, bf16[15,512]{1,0:T(8,128)(2,1)S(1)}, u32[]{:S(2)}, u32[]{:S(2)}) collective-permute-start(bf16[15,512]{1,0:T(8,128)(2,1)S(1)} %get-tuple-element.159), channel_id=1, source_target_pairs={{4,0},{8,4},{12,8},{16,12},{20,16},{24,20},{28,24},{32,28},{36,32}... | collective-permute-start | bytes 46088 | tf_op jit(solution)/shard_map/ppermute | solution.py:47
  51.9 7.5 %all-to-all-start.1 = ((f32[4,1,256]{2,1,0:T(1,128)}), f32[4,1,256]{2,1,0:T(1,128)S(1)}, u32[]{:S(2)}, u32[]{:S(2)}) async-start(f32[4,1,256]{2,1,0:T(1,128)} %broadcast_in_dim.18), calls=%async_computation.1 | async-start | bytes 8192 | tf_op jit(solution)/shard_map/all_to_all | solution.py:21
  60.2 7.4 %all-to-all-start.2 = ((f32[4,1,256]{2,1,0:T(1,128)}), f32[4,1,256]{2,1,0:T(1,128)S(1)}, u32[]{:S(2)}, u32[]{:S(2)}) async-start(f32[4,1,256]{2,1,0:T(1,128)} %broadcast_in_dim.19), calls=%async_computation.2 | async-start | bytes 8192 | tf_op jit(solution)/shard_map/all_to_all | solution.py:21
  159.4 83.0 %copy-start.14 = (f32[512]{0:T(512)S(1)}, f32[512]{0:T(512)}, u32[]{:S(2)}) copy-start(f32[512]{0:T(512)} %param.35) | copy-start | bytes 6148
Sparse Core Ops, SparseCore 0:
  31.9 112.1 all-gather.1
where the time goes:
time: 271 us; the launch traced here: 270 us
  waiting for transfers between devices  99.7 us (37%)
  matrix products  60.4 us (22%)
  local copies, waits for them, and re-layouts  42.3 us (16%)
  starting transfers between devices  19.2 us (7%)
  blocking collectives  18.4 us (7%)
  other arithmetic  14.9 us (5%)
  between operations  13.8 us (5%)
    all_gather x1, waiting for transfers between devices, sent_together(): lax.all_gather(both, axis, axis=dim, tiled=True)  76.5 us
    dot_general x16, matrix products, attend_block(): jnp.einsum('qhd,kd->hqk', r_heads, rope_key, preferred_element_type=jnp.f...  25.5 us
    all_to_all x3, waiting for transfers between devices, sent_to_all(): return lax.all_to_all(copies, axis, split_axis=0, concat_axis=0, tiled=True)  21.6 us
    dynamic_slice x16, local copies, waits for them, and re-layouts, over_blocks(): state, unused = lax.scan(one_block, state, shaped)  20.4 us
    all_to_all x1, blocking collectives, sum_at_owner(): lax.all_to_all(blocks, axis, split_axis=0, concat_axis=0, tiled=True)  18.4 us
    dot_general x16, matrix products, attend_block(): jnp.einsum('hqk,khd->hqd', weight.astype(jnp.bfloat16), value_heads, pref...  12.8 us
    dot_general x16, matrix products, attend_block(): jnp.einsum('qhd,khd->hqk', q_heads, key_heads, preferred_element_type=jnp...  12.2 us
    all_to_all x3, starting transfers between devices, sent_to_all(): return lax.all_to_all(copies, axis, split_axis=0, concat_axis=0, tiled=True)  11.5 us
  transfers between devices with their start and end apart: 6, of which 5 were waited for; matrix products, arithmetic and copies ran while one was open for 4% of the time, Pallas kernels for 0%

commit v1 on v0

v1 whole, which is shorter than its diff:
```python
import functools
import math

import jax
import jax.numpy as jnp
from jax import lax
from jax.experimental import pallas as pl
from jax.experimental.pallas import tpu as pltpu
from jax.sharding import PartitionSpec as P

eps_norm = 1e-06
eps_layer = 1e-05
theta = 10000.0
bf16 = jnp.bfloat16
f32 = jnp.float32

CHUNKS = 4


def laid_out(blocks, dim):
    dims = list(blocks.shape[1:])
    dims[dim] *= blocks.shape[0]
    return jnp.moveaxis(blocks, 0, dim).reshape(dims)


def sent_to_all(shard, axis):
    copies = jnp.broadcast_to(shard, (lax.axis_size(axis), *shard.shape))
    return lax.all_to_all(copies, axis, split_axis=0, concat_axis=0, tiled=True)


def gather_directly(shard, axis, dim):
    return laid_out(sent_to_all(shard, axis), dim)


def padded_2(cells, sides, width):
    for axis, dim in sides:
        count = lax.axis_size(axis)
        ends = count - 1
        head = lax.slice_in_dim(cells, 0, width, axis=dim)
        tail = lax.slice_in_dim(cells, cells.shape[dim] - width, cells.shape[dim], axis=dim)
        cells = jnp.concatenate(
            [
                lax.ppermute(tail, axis, [(i, (i + 1) % count) for i in range(ends)]),
                cells,
                lax.ppermute(head, axis, [((i + 1) % count, i) for i in range(ends)]),
            ],
            axis=dim,
        )
    return cells


def cut_along(shard, dim, peers):
    dims = shard.shape
    blocks = shard.reshape(*dims[:dim], peers, dims[dim] // peers, *dims[dim + 1 :])
    return jnp.moveaxis(blocks, dim, 0)


def sum_at_owner(shard, axis, dim):
    blocks = cut_along(shard, dim, lax.axis_size(axis))
    arrived = lax.all_to_all(blocks, axis, split_axis=0, concat_axis=0, tiled=True)
    return arrived.astype(f32).sum(axis=0)


def rms_scale(values, gain):
    return values * lax.rsqrt(jnp.mean(values * values, axis=-1, keepdims=True) + eps_norm) * gain


def rotate(values, positions):
    half = values.shape[-1] // 2
    freqs = theta ** (-jnp.arange(half).astype(f32) / half)
    angles = positions[..., None] * freqs
    cosine = jnp.cos(angles)
    sine = jnp.sin(angles)
    first = values[..., :half]
    second = values[..., half:]
    return jnp.concatenate(
        [first * cosine - second * sine, second * cosine + first * sine], axis=-1
    )


def attend_kernel(heads, nope, rope, first, x_ref, qt_ref, ku_ref, vut_ref, e_ref, *refs):
    if first:
        acc_ref, stat_ref = refs
    else:
        acc_in, stat_in, acc_ref, stat_ref = refs
    scale = math.log2(math.e) * (nope + rope) ** (-0.5)
    rank = ku_ref.shape[0]

    @pl.when(pl.program_id(0) == 0)
    def _():
        if first:
            acc_ref[...] = jnp.zeros_like(acc_ref)
            stat_ref[...] = jnp.zeros_like(stat_ref)
            stat_ref[0] = jnp.full(stat_ref.shape[1:], -jnp.inf, f32)
        else:
            acc_ref[...] = acc_in[...]
            stat_ref[...] = stat_in[...]

    latent = x_ref[:, :rank]
    k = jnp.dot(latent, ku_ref[...], preferred_element_type=f32).astype(bf16)
    spread = jnp.dot(x_ref[:, rank:], e_ref[...], preferred_element_type=f32).astype(bf16)
    vt = lax.dot_general(
        vut_ref[...], latent, (((1,), (1,)), ((), ())), preferred_element_type=f32
    ).astype(bf16)
    lane = lax.broadcasted_iota(jnp.int32, spread.shape, 1)
    for h in range(heads):
        pair = k[:, 128 * (h // 2) : 128 * (h // 2) + 128]
        mask = (lane < 64) if h % 2 == 0 else (lane >= 64)
        kh = jnp.where(mask, pair, spread)
        s = jnp.dot(kh, qt_ref[h], preferred_element_type=f32)
        old = stat_ref[0, h : h + 1, :]
        new = jnp.maximum(old, jnp.max(s, axis=0, keepdims=True))
        alpha = jnp.exp2((old - new) * scale)
        p = jnp.exp2((s - new) * scale)
        stat_ref[0, h : h + 1, :] = new
        stat_ref[1, h : h + 1, :] = stat_ref[1, h : h + 1, :] * alpha + jnp.sum(
            p, axis=0, keepdims=True
        )
        rows = vt.shape[0] // heads
        acc_ref[h] = acc_ref[h] * alpha + jnp.dot(
            vt[h * rows : (h + 1) * rows], p.astype(bf16), preferred_element_type=f32
        )


def attend(x, qt, key_up, value_up_t, expand, state, nope, rope, block):
    heads, _, queries = qt.shape
    vdim = value_up_t.shape[0] // heads
    count = x.shape[0]
    first = state is None
    whole = lambda a: pl.BlockSpec(a.shape, lambda i: (0,) * a.ndim)
    shapes = (
        jax.ShapeDtypeStruct((heads, vdim, queries), f32),
        jax.ShapeDtypeStruct((2, heads, queries), f32),
    )
    consts = (qt, key_up, value_up_t, expand)
    extra = () if first else state
    return pl.pallas_call(
        functools.partial(attend_kernel, heads, nope, rope, first),
        out_shape=shapes,
        grid=(count // block,),
        in_specs=[pl.BlockSpec((block, x.shape[1]), lambda i: (i, 0))]
        + [whole(a) for a in consts + extra],
        out_specs=tuple(whole(a) for a in shapes),
        cost_estimate=pl.CostEstimate(
            flops=2 * count * queries * heads * 320,
            bytes_accessed=count * 600,
            transcendentals=count * queries * heads,
        ),
        name="attend",
    )(x, *consts, *extra)


def per_device(
    tokens,
    in_gain,
    query_down,
    latent_down,
    rope_down,
    query_gain,
    latent_gain,
    query_nope,
    query_rope,
    key_up,
    value_up,
    conv_value,
    conv_gate,
    conv_taps,
    conv_bias,
    channel_gain,
    out_attend,
    out_conv,
):
    sp = lax.axis_size("sp")
    row_count = tokens.shape[0]
    width = in_gain.shape[0]
    local_ch = conv_value.shape[1]
    positions = (lax.axis_index("sp") * row_count + jnp.arange(row_count)).astype(f32)
    piece_f = gather_directly(tokens, "tp", 1).astype(f32)
    scaled = (piece_f * in_gain).astype(bf16)

    def add_rows(weight):
        return jnp.dot(scaled, weight, preferred_element_type=f32)

    square_sum = jnp.sum(piece_f * piece_f, axis=1)
    q_pre = add_rows(query_down)
    kv_pre = add_rows(latent_down)
    rope_pre = add_rows(rope_down)
    value_pre = add_rows(conv_value)
    gate_pre = add_rows(conv_gate)
    row_scale = lax.rsqrt(square_sum / width + eps_norm)[:, None]
    q_latent = rms_scale(row_scale * q_pre, query_gain).astype(bf16)
    kv_latent = rms_scale(row_scale * kv_pre, latent_gain).astype(bf16)
    rope_key = rotate(row_scale * rope_pre, positions).astype(bf16)
    rope_size = rope_down.shape[1]
    heads = query_rope.shape[1] // rope_size
    nope = query_nope.shape[1] // heads

    x = jnp.concatenate([kv_latent, rope_key], axis=1)
    groups = [list(range(c, sp, 2)) for c in range(2)]
    part = row_count // CHUNKS
    gathered = [
        lax.all_gather(
            x[i * part : (i + 1) * part],
            "sp",
            axis=0,
            tiled=True,
            axis_index_groups=groups,
        )
        for i in range(CHUNKS)
    ]

    q_heads = (
        jnp.dot(q_latent, query_nope, preferred_element_type=f32)
        .astype(bf16)
        .reshape(row_count, heads, nope)
    )
    q_turn = jnp.dot(q_latent, query_rope, preferred_element_type=f32).reshape(
        row_count, heads, rope_size
    )
    r_heads = rotate(q_turn, positions[:, None]).astype(bf16)
    empty = jnp.zeros((row_count, 64 - rope_size), bf16)
    cols = []
    for h in range(heads):
        if h % 2 == 0:
            cols += [q_heads[:, h], r_heads[:, h], empty]
        else:
            cols += [r_heads[:, h], empty, q_heads[:, h]]
    q_own = jnp.transpose(jnp.concatenate(cols, axis=1))
    swap = [(i, i ^ 1) for i in range(sp)]
    q_other = lax.ppermute(q_own, "sp", swap)
    qt = jnp.concatenate([q_own, q_other], axis=1).reshape(heads, 128, 2 * row_count)
    expand = jnp.tile(jnp.eye(rope_size, dtype=bf16), (1, 128 // rope_size))
    state = None
    for i in range(CHUNKS):
        state = attend(
            gathered[i], qt, key_up, jnp.transpose(value_up), expand, state, nope, rope_size, 512
        )
    acc, stat = state
    acc_other = lax.ppermute(acc[:, :, row_count:], "sp", swap)
    stat_other = lax.ppermute(stat[:, :, row_count:], "sp", swap)
    acc, stat = acc[:, :, :row_count], stat[:, :, :row_count]
    scale = (nope + rope_size) ** (-0.5)
    high = jnp.maximum(stat[0], stat_other[0])
    a, b = jnp.exp((stat[0] - high) * scale), jnp.exp((stat_other[0] - high) * scale)
    total = stat[1] * a + stat_other[1] * b
    merged = (acc * a[:, None] + acc_other * b[:, None]) / total[:, None]
    attended = merged.astype(bf16).reshape(-1, row_count)

    glu = (row_scale * value_pre * jax.nn.sigmoid(row_scale * gate_pre)).astype(bf16)
    taps = conv_taps.shape[0]
    padded = padded_2(glu, (("sp", 0),), taps // 2).astype(f32)
    conv = jnp.zeros((row_count, local_ch), f32) + conv_bias
    for tap in range(taps):
        conv = conv + conv_taps[tap] * padded[tap : tap + row_count]
    peers = lax.axis_size("tp")
    channels = local_ch * peers
    own_mean = jnp.mean(conv, axis=-1)
    off = conv - own_mean[:, None]
    own_spread = jnp.sum(off * off, axis=-1)
    sums = sent_to_all(jnp.stack([own_mean, own_spread]), "tp")
    means = sums[:, 0]
    mean = jnp.mean(means, axis=0)
    apart = means - mean
    spread = (jnp.sum(sums[:, 1], axis=0) + local_ch * jnp.sum(apart * apart, axis=0)) / channels
    centred = conv - mean[:, None]
    activated = jax.nn.silu(
        centred * lax.rsqrt(spread[:, None] + eps_layer) * channel_gain
    ).astype(bf16)
    summed = sum_at_owner(
        (
            lax.dot_general(
                out_attend, attended, (((0,), (0,)), ((), ())), preferred_element_type=f32
            )
            + lax.dot_general(
                out_conv, activated, (((0,), (1,)), ((), ())), preferred_element_type=f32
            )
        ).astype(bf16),
        "tp",
        0,
    )
    return jnp.transpose(summed).astype(bf16)


def solution(mesh):
    in_specs = (
        P("sp", "tp"),
        P(),
        P(),
        P(),
        P(),
        P(),
        P(),
        P(None, "tp"),
        P(None, "tp"),
        P(None, "tp"),
        P(None, "tp"),
        P(None, "tp"),
        P(None, "tp"),
        P(None, "tp"),
        P("tp"),
        P("tp"),
        P("tp", None),
        P("tp", None),
    )
    return jax.shard_map(
        per_device, mesh=mesh, in_specs=in_specs, out_specs=P("sp", "tp"), check_vma=False
    )
```

time: 271 us -> 388 us (1.43)
  waiting for transfers between devices: 99.7 us -> 253 us
  matrix products: 60.4 us -> 13.1 us
  Pallas kernels: 0 us -> 46.3 us
  local copies, waits for them, and re-layouts: 42.3 us -> 10.5 us
  other arithmetic: 14.9 us -> 10 us
    all_gather x1 -> x4, waiting for transfers between devices: 76.5 us -> 234 us  [per_device(): lax.all_gather(x[i * part:(i + 1) * part], 'sp', axis=0, tiled=True, axis...]
    dot_general x59 -> x9, matrix products: 60.4 us -> 13.1 us  [the longest x5 7.77 us: add_rows(): return jnp.dot(scaled, weight, preferred_element_type=f32)]
    pallas_call x0 -> x4, Pallas kernels: none -> 46.3 us  [attend(): pl.pallas_call(functools.partial(attend_kernel, heads, nope, rope, first)...]
    dynamic_slice x16 -> x0, local copies, waits for them, and re-layouts: 20.4 us -> none  [over_blocks(): state, unused = lax.scan(one_block, state, shaped)]
    reduce_sum x21 -> x5, other arithmetic: 12.8 us -> 4.42 us  [the longest x1 3.27 us: per_device(): own_mean = jnp.mean(conv, axis=-1)]
    split x2 -> x0, local copies, waits for them, and re-layouts: 8.03 us -> none  [sent_together(): jnp.split(lax.all_gather(both, axis, axis=dim, tiled=True), ends, axis=al...]
    ppermute x0 -> x3, starting transfers between devices: none -> 5.63 us  [the longest x1 5.26 us: per_device(): stat_other = lax.ppermute(stat[:, :, row_count:], 'sp', swap)]
    unnamed x32 -> x103, local copies, waits for them, and re-layouts: 8.23 us -> 2.98 us
  transfers between devices with their start and end apart: 6 -> 11, of which waited for: 5 -> 7; matrix products, arithmetic and copies ran while one was open for 4% -> 6% of each run, Pallas kernels for 0% -> 9%
where the time goes in v1:
time: 388 us; the launch traced here: 387 us
  waiting for transfers between devices  253 us (65%)
  Pallas kernels  46.3 us (12%)
  starting transfers between devices  21.6 us (6%)
  blocking collectives  18.4 us (5%)
  between operations  14.1 us (4%)
  matrix products  13.1 us (3%)
  local copies, waits for them, and re-layouts  10.5 us (3%)
  other arithmetic  10 us (3%)
    all_gather x4, waiting for transfers between devices, per_device(): lax.all_gather(x[i * part:(i + 1) * part], 'sp', axis=0, tiled=True, axis...  234 us
    pallas_call x4, Pallas kernels, attend(): pl.pallas_call(functools.partial(attend_kernel, heads, nope, rope, first)...  46.3 us
    all_to_all x1, blocking collectives, sum_at_owner(): lax.all_to_all(blocks, axis, split_axis=0, concat_axis=0, tiled=True)  18.4 us
    all_to_all x2, waiting for transfers between devices, sent_to_all(): return lax.all_to_all(copies, axis, split_axis=0, concat_axis=0, tiled=True)  17.2 us
    all_to_all x2, starting transfers between devices, sent_to_all(): return lax.all_to_all(copies, axis, split_axis=0, concat_axis=0, tiled=True)  8.08 us
    dot_general x5, matrix products, add_rows(): return jnp.dot(scaled, weight, preferred_element_type=f32)  7.77 us
  transfers between devices with their start and end apart: 11, of which 7 were waited for; matrix products, arithmetic and copies ran while one was open for 6% of the time, Pallas kernels for 9%

profile of v1, /device:TPU:1, one launch (start us, length us, event | category | flops | bytes accessed | tf_op | source)
XLA Modules:
  0.0 386.7 jit_solution(15585267828246159868)
XLA Ops:
  6.5 1.2 copy.53
  7.8 1.1 broadcast_in_dim.6
  8.9 4.8 %all-to-all-start = ((bf16[4,256,512]{1,2,0:T(8,128)(2,1)}), bf16[4,256,512]{1,2,0:T(8,128)(2,1)S(1)}, u32[]{:S(2)}, u32[]{:S(2)}) async-start(bf16[4,256,512]{1,2,0:T(8,128)(2,1)} %broadcast_in_dim.6), calls=%async_computation | async-start | bytes 2097152 | tf_op jit(solution)/shard_map/all_to_all | solution.py:28
  13.7 13.3 %all-to-all-done = bf16[4,256,512]{1,2,0:T(8,128)(2,1)S(1)} async-done(((bf16[4,256,512]{1,2,0:T(8,128)(2,1)}), bf16[4,256,512]{1,2,0:T(8,128)(2,1)S(1)}, u32[]{:S(2)}, u32[]{:S(2)}) %all-to-all-start) | async-done | bytes 1048608 | tf_op jit(solution)/shard_map/all_to_all | solution.py:28
  34.0 2.9 fusion.5
  39.0 5.8 %collective-permute-start.3 = (bf16[15,512]{1,0:T(8,128)(2,1)}, bf16[15,512]{1,0:T(8,128)(2,1)}, u32[]{:S(2)}, u32[]{:S(2)}) collective-permute-start(bf16[15,512]{1,0:T(8,128)(2,1)} %get-tuple-element.28), channel_id=1, source_target_pairs={{0,4},{4,8},{8,12},{12,16},{16,20},{20,24},{24,28},{28,32},{32,36}... | collective-permute-start | bytes 46088 | tf_op jit(solution)/shard_map/ppermute | solution.py:43
  44.8 1.9 collective-permute-start.4
  47.5 3.2 multiply_reduce_fusion.2
  51.0 1.4 convolution_convert_fusion
  52.4 1.3 fusion.64
  55.8 3.3 fusion.65
  60.0 3.2 all-to-all-start.1
  63.5 3.8 all-to-all-done.1
  68.2 37.9 %all-gather.11.cloned.1.call-done.x_ref = bf16[2048,288]{1,0:T(8,128)(2,1)} async-done(((bf16[64,288]{1,0:T(8,128)(2,1)}), bf16[2048,288]{1,0:T(8,128)(2,1)}) %all-gather.11.cloned.1.call-update) | async-done | bytes 1179664 | tf_op jit(solution)/shard_map/all_gather | solution.py:202
  106.2 11.4 %attend.4 = (f32[4,64,512]{2,1,0:T(8,128)}, f32[2,4,512]{2,1,0:T(4,128)}) custom-call(bf16[2048,288]{1,0:T(8,128)(2,1)} %all-gather.11.cloned.1.call-done.x_ref, bf16[4,128,512]{2,1,0:T(8,128)(2,1)} %bitcast.129, bf16[256,256]{1,0:T(8,128)(2,1)} %ku_ref.7, bf16[256,256]{1,0:T(8,128)(2,1)} %bitcast.141, bf16[32,128]{1,0:T(8,128)(2,1)} %tile.22.e_ref), custom_call_target="tpu_custom_call" | custom-call | flops 2684354560 | bytes 1228800 | tf_op jit(solution)/shard_map/attend/pallas_call | solution.py:137
  117.6 65.5 %all-gather.9.cloned.1.call-done.x_ref = bf16[2048,288]{1,0:T(8,128)(2,1)} async-done(((bf16[64,288]{1,0:T(8,128)(2,1)}), bf16[2048,288]{1,0:T(8,128)(2,1)}) %all-gather.9.cloned.1.call-update) | async-done | bytes 1179664 | tf_op jit(solution)/shard_map/all_gather | solution.py:202
  183.1 11.6 %attend.5 = (f32[4,64,512]{2,1,0:T(8,128)}, f32[2,4,512]{2,1,0:T(4,128)}) custom-call(bf16[2048,288]{1,0:T(8,128)(2,1)} %all-gather.9.cloned.1.call-done.x_ref, bf16[4,128,512]{2,1,0:T(8,128)(2,1)} %bitcast.130, bf16[256,256]{1,0:T(8,128)(2,1)} %ku_ref.7, bf16[256,256]{1,0:T(8,128)(2,1)} %bitcast.142, bf16[32,128]{1,0:T(8,128)(2,1)} %tile.22.e_ref, ...), custom_call_target="tpu_custom_call" | custom-call | flops 2684354560 | bytes 1228800 | tf_op jit(solution)/shard_map/attend/pallas_call | solution.py:137
  194.8 65.3 %all-gather.7.cloned.1.call-done.x_ref = bf16[2048,288]{1,0:T(8,128)(2,1)} async-done(((bf16[64,288]{1,0:T(8,128)(2,1)}), bf16[2048,288]{1,0:T(8,128)(2,1)}) %all-gather.7.cloned.1.call-update) | async-done | bytes 1179664 | tf_op jit(solution)/shard_map/all_gather | solution.py:202
  260.1 11.6 %attend.6 = (f32[4,64,512]{2,1,0:T(8,128)}, f32[2,4,512]{2,1,0:T(4,128)}) custom-call(bf16[2048,288]{1,0:T(8,128)(2,1)} %all-gather.7.cloned.1.call-done.x_ref, bf16[4,128,512]{2,1,0:T(8,128)(2,1)} %bitcast.131, bf16[256,256]{1,0:T(8,128)(2,1)} %ku_ref.7, bf16[256,256]{1,0:T(8,128)(2,1)} %bitcast.143, bf16[32,128]{1,0:T(8,128)(2,1)} %tile.22.e_ref, ...), custom_call_target="tpu_custom_call" | custom-call | flops 2684354560 | bytes 1228800 | tf_op jit(solution)/shard_map/attend/pallas_call | solution.py:137
  271.7 65.2 %all-gather.5.cloned.1.call-done.x_ref = bf16[2048,288]{1,0:T(8,128)(2,1)} async-done(((bf16[64,288]{1,0:T(8,128)(2,1)}), bf16[2048,288]{1,0:T(8,128)(2,1)}) %all-gather.5.cloned.1.call-update) | async-done | bytes 1179664 | tf_op jit(solution)/shard_map/all_gather | solution.py:202
  336.9 11.6 %attend.7 = (f32[4,64,512]{2,1,0:T(8,128)}, f32[2,4,512]{2,1,0:T(4,128)}) custom-call(bf16[2048,288]{1,0:T(8,128)(2,1)} %all-gather.5.cloned.1.call-done.x_ref, bf16[4,128,512]{2,1,0:T(8,128)(2,1)} %bitcast.132, bf16[256,256]{1,0:T(8,128)(2,1)} %ku_ref.7, bf16[256,256]{1,0:T(8,128)(2,1)} %bitcast.144, bf16[32,128]{1,0:T(8,128)(2,1)} %tile.22.e_ref, ...), custom_call_target="tpu_custom_call" | custom-call | flops 2684354560 | bytes 1228800 | tf_op jit(solution)/shard_map/attend/pallas_call | solution.py:137
  349.3 5.3 %collective-permute-start.1 = (f32[2,4,256]{2,1,0:T(4,128)S(1)}, f32[2,4,256]{2,1,0:T(4,128)S(1)}, u32[]{:S(2)}, u32[]{:S(2)}) collective-permute-start(f32[2,4,256]{2,1,0:T(4,128)S(1)} %slice.290), channel_id=1, source_target_pairs={{0,4},{4,0},{8,12},{12,8},{16,20},{20,16},{24,28},{28,24},{32,36},... | collective-permute-start | bytes 24584 | tf_op jit(solution)/shard_map/ppermute | solution.py:240
  358.1 1.7 fusion.73
  360.8 18.4 %all_to_all.15 = bf16[4,512,256]{1,2,0:T(8,128)(2,1)S(1)} all-to-all(bf16[4,512,256]{1,2,0:T(8,128)(2,1)S(1)} %bitcast.127), channel_id=1, replica_groups=mesh['sp'=64,'tp'=4] {'tp'}, dimensions={0} | all-to-all | bytes 2097152 | tf_op jit(solution)/shard_map/all_to_all | solution.py:60
  (162 shorter events, 19.6 us)
Async XLA Ops:
  6.5 353.3 %copy-start = (bf16[512,2048]{1,0:T(8,128)(2,1)S(1)}, bf16[512,2048]{1,0:T(8,128)(2,1)}, u32[]{:S(2)}) copy-start(bf16[512,2048]{1,0:T(8,128)(2,1)} %param.35) | copy-start | bytes 6291460
  7.8 19.6 %copy-start.11 = (f32[2048]{0:T(1024)S(1)}, f32[2048]{0:T(1024)}, u32[]{:S(2)}) copy-start(f32[2048]{0:T(1024)} %param.19) | copy-start | bytes 24580
  8.9 18.2 %all-to-all-start = ((bf16[4,256,512]{1,2,0:T(8,128)(2,1)}), bf16[4,256,512]{1,2,0:T(8,128)(2,1)S(1)}, u32[]{:S(2)}, u32[]{:S(2)}) async-start(bf16[4,256,512]{1,2,0:T(8,128)(2,1)} %broadcast_in_dim.6), calls=%async_computation | async-start | bytes 2097152 | tf_op jit(solution)/shard_map/all_to_all | solution.py:28
  13.7 14.0 %copy-start.45 = (bf16[2048,32]{0,1:T(8,128)(2,1)S(1)}, bf16[2048,32]{0,1:T(8,128)(2,1)}, u32[]{:S(2)}) copy-start(bf16[2048,32]{0,1:T(8,128)(2,1)} %param.22) | copy-start | bytes 393220
  13.7 92.5 %all-gather.11.cloned.1.call-start = ((), (), s32[]{:S(2)}) async-start(), calls=%async_computation.6 | async-start | bytes 1622016 | tf_op jit(solution)/shard_map/all_gather | solution.py:202
  27.3 9.6 %copy-start.10 = (f32[256]{0:T(256)}, f32[256]{0:T(256)S(1)}, u32[]{:S(2)}) copy-start(f32[256]{0:T(256)S(1)} %add_rsqrt_fusion.3) | copy-start | bytes 3076
  30.4 152.8 %all-gather.9.cloned.1.call-start = ((), (), s32[]{:S(2)}) async-start(), calls=%async_computation.5 | async-start | bytes 1622016 | tf_op jit(solution)/shard_map/all_gather | solution.py:202
  31.1 229.0 %all-gather.7.cloned.1.call-start = ((), (), s32[]{:S(2)}) async-start(), calls=%async_computation.4 | async-start | bytes 1622016 | tf_op jit(solution)/shard_map/all_gather | solution.py:202
  39.0 15.7 %collective-permute-start.3 = (bf16[15,512]{1,0:T(8,128)(2,1)}, bf16[15,512]{1,0:T(8,128)(2,1)}, u32[]{:S(2)}, u32[]{:S(2)}) collective-permute-start(bf16[15,512]{1,0:T(8,128)(2,1)} %get-tuple-element.28), channel_id=1, source_target_pairs={{0,4},{4,8},{8,12},{12,16},{16,20},{20,24},{24,28},{28,32},{32,36}... | collective-permute-start | bytes 46088 | tf_op jit(solution)/shard_map/ppermute | solution.py:43
  44.8 9.9 %collective-permute-start.4 = (bf16[15,512]{1,0:T(8,128)(2,1)}, bf16[15,512]{1,0:T(8,128)(2,1)}, u32[]{:S(2)}, u32[]{:S(2)}) collective-permute-start(bf16[15,512]{1,0:T(8,128)(2,1)} %get-tuple-element.29), channel_id=1, source_target_pairs={{4,0},{8,4},{12,8},{16,12},{20,16},{24,20},{28,24},{32,28},{36,32}... | collective-permute-start | bytes 46088 | tf_op jit(solution)/shard_map/ppermute | solution.py:45
  47.5 5.0 %copy-start.8 = (bf16[512,128]{1,0:T(8,128)(2,1)S(1)}, bf16[512,128]{1,0:T(8,128)(2,1)}, u32[]{:S(2)}) copy-start(bf16[512,128]{1,0:T(8,128)(2,1)} %param.26) | copy-start | bytes 393220
  50.6 4.9 %copy-start.14 = (f32[1,512]{1,0:T(1,128)S(1)}, f32[1,512]{1,0:T(1,128)}, u32[]{:S(2)}) copy-start(f32[1,512]{1,0:T(1,128)} %get-tuple-element.59) | copy-start | bytes 6148
  50.6 4.9 %copy-start.15 = (f32[1,512]{1,0:T(1,128)S(1)}, f32[1,512]{1,0:T(1,128)}, u32[]{:S(2)}) copy-start(f32[1,512]{1,0:T(1,128)} %get-tuple-element.60) | copy-start | bytes 6148
  50.7 4.9 %copy-start.16 = (f32[1,512]{1,0:T(1,128)S(1)}, f32[1,512]{1,0:T(1,128)}, u32[]{:S(2)}) copy-start(f32[1,512]{1,0:T(1,128)} %get-tuple-element.61) | copy-start | bytes 6148
  50.7 4.9 %copy-start.17 = (f32[1,512]{1,0:T(1,128)S(1)}, f32[1,512]{1,0:T(1,128)}, u32[]{:S(2)}) copy-start(f32[1,512]{1,0:T(1,128)} %get-tuple-element.62) | copy-start | bytes 6148
  50.7 4.9 %copy-start.18 = (f32[1,512]{1,0:T(1,128)S(1)}, f32[1,512]{1,0:T(1,128)}, u32[]{:S(2)}) copy-start(f32[1,512]{1,0:T(1,128)} %get-tuple-element.63) | copy-start | bytes 6148
  50.7 4.9 %copy-start.19 = (f32[1,512]{1,0:T(1,128)S(1)}, f32[1,512]{1,0:T(1,128)}, u32[]{:S(2)}) copy-start(f32[1,512]{1,0:T(1,128)} %get-tuple-element.64) | copy-start | bytes 6148
  50.7 4.9 %copy-start.20 = (f32[1,512]{1,0:T(1,128)S(1)}, f32[1,512]{1,0:T(1,128)}, u32[]{:S(2)}) copy-start(f32[1,512]{1,0:T(1,128)} %get-tuple-element.65) | copy-start | bytes 6148
  50.7 4.9 %copy-start.21 = (f32[1,512]{1,0:T(1,128)S(1)}, f32[1,512]{1,0:T(1,128)}, u32[]{:S(2)}) copy-start(f32[1,512]{1,0:T(1,128)} %get-tuple-element.66) | copy-start | bytes 6148
  51.0 286.0 %all-gather.5.cloned.1.call-start = ((), (), s32[]{:S(2)}) async-start(), calls=%async_computation.3 | async-start | bytes 1622016 | tf_op jit(solution)/shard_map/all_gather | solution.py:202
  60.0 7.4 %all-to-all-start.1 = ((f32[4,2,256]{2,1,0:T(2,128)}), f32[4,2,256]{2,1,0:T(2,128)S(1)}, u32[]{:S(2)}, u32[]{:S(2)}) async-start(f32[4,2,256]{2,1,0:T(2,128)} %broadcast_in_dim.8), calls=%async_computation.1 | async-start | bytes 16384 | tf_op jit(solution)/shard_map/all_to_all | solution.py:28
  63.2 4.2 %collective-permute-start = (bf16[512,256]{1,0:T(8,128)(2,1)S(1)}, bf16[512,256]{1,0:T(8,128)(2,1)S(1)}, u32[]{:S(2)}, u32[]{:S(2)}) collective-permute-start(bf16[512,256]{1,0:T(8,128)(2,1)S(1)} %bitcast.139), channel_id=1, source_target_pairs={{0,4},{4,0},{8,12},{12,8},{16,20},{20,16},{24,28},{28,24},{32,36},... | collective-permute-start | bytes 786440 | tf_op jit(solution)/shard_map/ppermute | solution.py:230
  349.3 6.4 %collective-permute-start.1 = (f32[2,4,256]{2,1,0:T(4,128)S(1)}, f32[2,4,256]{2,1,0:T(4,128)S(1)}, u32[]{:S(2)}, u32[]{:S(2)}) collective-permute-start(f32[2,4,256]{2,1,0:T(4,128)S(1)} %slice.290), channel_id=1, source_target_pairs={{0,4},{4,0},{8,12},{12,8},{16,20},{20,16},{24,28},{28,24},{32,36},... | collective-permute-start | bytes 24584 | tf_op jit(solution)/shard_map/ppermute | solution.py:240
  355.5 1.6 collective-permute-start.2
  (34 other events, 143.4 us)
Sparse Core Ops, SparseCore 0:
  30.5 75.6 all-gather.10
  108.7 74.3 all-gather.8
  185.7 74.3 all-gather.6
  262.5 74.3 all-gather.4

commit v2 on v1

--- a/solution.py
+++ b/solution.py
@@ -13,9 +13,6 @@
 theta = 10000.0
 bf16 = jnp.bfloat16
 f32 = jnp.float32
-
-CHUNKS = 4
-
 
 def laid_out(blocks, dim):
     dims = list(blocks.shape[1:])
@@ -78,76 +75,260 @@
     )
 
 
-def attend_kernel(heads, nope, rope, first, x_ref, qt_ref, ku_ref, vut_ref, e_ref, *refs):
-    if first:
-        acc_ref, stat_ref = refs
-    else:
-        acc_in, stat_in, acc_ref, stat_ref = refs
-    scale = math.log2(math.e) * (nope + rope) ** (-0.5)
-    rank = ku_ref.shape[0]
-
-    @pl.when(pl.program_id(0) == 0)
-    def _():
-        if first:
-            acc_ref[...] = jnp.zeros_like(acc_ref)
-            stat_ref[...] = jnp.zeros_like(stat_ref)
-            stat_ref[0] = jnp.full(stat_ref.shape[1:], -jnp.inf, f32)
+def attend_kernel(
+    heads, scale, xp_ref, qt_ref, ku_ref, vut_ref, out_ref,
+    x, q, acc, high, acc_in, high_in,
+    got, sent_a, sent_y, sent_bz, sent_by, sent_br, pair_sem,
+):
+    sp, tp = lax.axis_index("sp"), lax.axis_index("tp")
+    core = lax.rem(sp, 2)
+    y = lax.rem(sp // 2, 4)
+    z = sp // 8
+    rows = xp_ref.shape[1]
+    own_q = qt_ref.shape[2]
+
+    def device(pz, py):
+        return (((pz * 4 + py) * 2 + core), tp)
+
+    def turn(a, n):
+        return lax.rem(a + 2 * n, n)
+
+    up, down = device(turn(z + 1, 8), y), device(turn(z - 1, 8), y)
+    right, left = device(z, turn(y + 1, 4)), device(z, turn(y - 1, 4))
+    across = device(z, turn(y + 2, 4))
+    sibling = (sp + 1 - 2 * core, tp)
+
+    def slot(pz, py, color):
+        return (pz * 4 + py) * 2 + color
+
+    def send(src, at, sem, target):
+        return pltpu.make_async_remote_copy(
+            src_ref=src, dst_ref=x.at[at], send_sem=sem, recv_sem=got.at[at],
+            device_id=target, device_id_type=pl.DeviceIdType.MESH,
+        )
+
+    def arrived(at):
+        send(x.at[at], at, got.at[at], sibling).wait_recv()
+
+    barrier = pltpu.get_barrier_semaphore()
+    peers = (up, down, right, left, across, sibling)
+    for peer in peers:
+        pl.semaphore_signal(barrier, inc=1, device_id=peer, device_id_type=pl.DeviceIdType.MESH)
+    pl.semaphore_wait(barrier, len(peers))
+
+    own_a, own_b = slot(z, y, 0), slot(z, y, 1)
+    first = [
+        send(xp_ref.at[1], own_b, sent_bz.at[0, 0], up),
+        send(xp_ref.at[1], own_b, sent_bz.at[0, 1], down),
+        send(xp_ref.at[0], own_a, sent_y.at[0], right),
+        send(xp_ref.at[0], own_a, sent_y.at[1], left),
+        send(xp_ref.at[0], own_a, sent_y.at[2], across),
+        send(xp_ref.at[1], own_b, sent_by.at[0, 0], right),
+        send(xp_ref.at[1], own_b, sent_by.at[0, 1], left),
+        send(xp_ref.at[0], own_a, sent_a.at[0, 0, 0], up),
+        send(xp_ref.at[0], own_a, sent_a.at[0, 0, 1], down),
+    ]
+    for copy in first:
+        copy.start()
+    q_copy = pltpu.make_async_remote_copy(
+        src_ref=qt_ref, dst_ref=q.at[1], send_sem=pair_sem.at[0], recv_sem=pair_sem.at[1],
+        device_id=sibling, device_id_type=pl.DeviceIdType.MESH,
+    )
+    q_copy.start()
+    x[own_a] = xp_ref[0]
+    x[own_b] = xp_ref[1]
+    q[0] = qt_ref[...]
+    acc[...] = jnp.zeros_like(acc)
+    high[...] = jnp.full_like(high, -jnp.inf)
+
+    def plane(k):
+        return turn(z + (1 - 2 * lax.rem(k, 2)) * ((k + 1) // 2), 8)
+
+    def b_copies(k):
+        pz = plane(k)
+        at = slot(pz, y, 1)
+        onward = device(turn(z + 2 * lax.rem(k, 2) - 1, 8), y)
+        along = send(x.at[at], at, sent_bz.at[k, 0], onward)
+        return (
+            along,
+            send(x.at[at], at, sent_by.at[k, 0], right),
+            send(x.at[at], at, sent_by.at[k, 1], left),
+        )
+
+    def b_first(k):
+        arrived(slot(plane(k), y, 1))
+        along, one, two = b_copies(k)
+
+        @pl.when(k < 6)
+        def _():
+            along.start()
+
+        one.start()
+        two.start()
+
+    def relay_copy(k):
+        back = (1 - lax.rem(k, 2)) * ((k + 7) // 8)
+        at = slot(plane(k), turn(y - 1 + 2 * back, 4), 1)
+        return send(x.at[at], at, sent_br.at[k], device(z, turn(y + 1 - 2 * back, 4)))
+
+    def relay(k):
+        arrived(slot(plane(k), turn(y - 1, 4), 1))
+        arrived(slot(plane(k), turn(y + 1, 4), 1))
+        relay_copy(k).start()
+
+    def a_copy(k, j, way):
+        at = slot(plane(k), turn(y + j, 4), 0)
+        return send(x.at[at], at, sent_a.at[k, j, way], up if way == 0 else down)
+
+    def a_goes(k, j, way):
+        if way == 0:
+            most = 5 if j < 2 else 3
+            rule = jnp.logical_and(lax.rem(k, 2) == 1, k <= most)
         else:
-            acc_ref[...] = acc_in[...]
-            stat_ref[...] = stat_in[...]
-
-    latent = x_ref[:, :rank]
-    k = jnp.dot(latent, ku_ref[...], preferred_element_type=f32).astype(bf16)
-    spread = jnp.dot(x_ref[:, rank:], e_ref[...], preferred_element_type=f32).astype(bf16)
-    vt = lax.dot_general(
-        vut_ref[...], latent, (((1,), (1,)), ((), ())), preferred_element_type=f32
-    ).astype(bf16)
-    lane = lax.broadcasted_iota(jnp.int32, spread.shape, 1)
+            most = 6 if j >= 2 else 4
+            rule = jnp.logical_and(lax.rem(k, 2) == 0, k <= most)
+        if j == 0:
+            return jnp.logical_and(rule, k > 0)
+        return jnp.logical_or(rule, k == 0)
+
+    def a_first(k):
+        for j in (1, 3, 2, 0):
+            at = slot(plane(k), turn(y + j, 4), 0)
+            if j == 0:
+                pl.when(k > 0)(functools.partial(arrived, at))
+            else:
+                arrived(at)
+            for way in range(2):
+                pl.when(a_goes(k, j, way))(a_copy(k, j, way).start)
+
+    def compute(pz, color):
+        at = [slot(pz, j, color) for j in range(4)]
+        keys = rows - 16
+        latent = jnp.concatenate([x[s, :keys, :] for s in at], axis=0)
+        k = jnp.dot(latent, ku_ref[...], preferred_element_type=f32).astype(bf16)
+        vt = lax.dot_general(
+            vut_ref[...], latent, (((1,), (1,)), ((), ())), preferred_element_type=f32
+        ).astype(bf16)
+        even, odd = [], []
+        for s in at:
+            for half in range(2):
+                part = x[s, keys:, 128 * half : 128 * half + 128].astype(f32)
+                r1, r2, r3 = (pltpu.roll(part, 32 * n, 1) for n in (1, 2, 3))
+                even += [r2, r1, part, r3]
+                odd += [part, r3, r2, r1]
+        even = jnp.concatenate(even, axis=0).astype(bf16)
+        odd = jnp.concatenate(odd, axis=0).astype(bf16)
+        lane = lax.broadcasted_iota(jnp.int32, even.shape, 1)
+        count = latent.shape[0]
+        ones = jnp.ones((16, count), bf16)
+        vrows = vt.shape[0] // heads
+
+        def score(h):
+            pair = k[:, 128 * (h // 2) : 128 * (h // 2) + 128]
+            kh = jnp.where(lane < 64, pair, even) if h % 2 == 0 else jnp.where(lane >= 64, pair, odd)
+            both = jnp.concatenate([q[0, h], q[1, h]], axis=1)
+            return jnp.dot(kh, both, preferred_element_type=f32)
+
+        following = score(0)
+        for h in range(heads):
+            s = following
+            if h + 1 < heads:
+                following = score(h + 1)
+            old = high[h : h + 1, :]
+            new = jnp.maximum(old, jnp.max(s, axis=0, keepdims=True))
+            alpha = jnp.exp2((old - new) * scale)
+            p = jnp.exp2((s - new) * scale).astype(bf16)
+            high[h : h + 1, :] = new
+            v = jnp.concatenate([vt[h * vrows : (h + 1) * vrows], ones], axis=0)
+            acc[h] = acc[h] * alpha + jnp.dot(v, p, preferred_element_type=f32)
+
+    b_first(1)
+    b_first(2)
+    relay(0)
+    q_copy.wait()
+
+    @pl.loop(0, 8)
+    def _(k):
+        a_first(k)
+        compute(plane(k), 0)
+        pl.when(k < 5)(lambda: b_first(k + 3))
+        pl.when(k < 7)(lambda: relay(k + 1))
+        arrived(slot(plane(k), turn(y + 2, 4), 1))
+        compute(plane(k), 1)
+
+    for copy in first:
+        copy.wait_send()
+
+    @pl.loop(0, 8)
+    def _(k):
+        for j in range(4):
+            for way in range(2):
+                pl.when(a_goes(k, j, way))(a_copy(k, j, way).wait_send)
+        along, one, two = b_copies(k)
+        pl.when(jnp.logical_and(k > 0, k < 6))(along.wait_send)
+        pl.when(k > 0)(one.wait_send)
+        pl.when(k > 0)(two.wait_send)
+        relay_copy(k).wait_send()
+
+    copies = [
+        pltpu.make_async_remote_copy(
+            src_ref=a.at[:, own_q:] if a.ndim == 2 else a.at[:, :, own_q:],
+            dst_ref=b, send_sem=pair_sem.at[2 * n + 2], recv_sem=pair_sem.at[2 * n + 3],
+            device_id=sibling, device_id_type=pl.DeviceIdType.MESH,
+        )
+        for n, (a, b) in enumerate(((acc, acc_in), (high, high_in)))
+    ]
+    for copy in copies:
+        copy.start()
+    for copy in copies:
+        copy.wait()
+    vrows = vut_ref.shape[0] // heads
     for h in range(heads):
-        pair = k[:, 128 * (h // 2) : 128 * (h // 2) + 128]
-        mask = (lane < 64) if h % 2 == 0 else (lane >= 64)
-        kh = jnp.where(mask, pair, spread)
-        s = jnp.dot(kh, qt_ref[h], preferred_element_type=f32)
-        old = stat_ref[0, h : h + 1, :]
-        new = jnp.maximum(old, jnp.max(s, axis=0, keepdims=True))
-        alpha = jnp.exp2((old - new) * scale)
-        p = jnp.exp2((s - new) * scale)
-        stat_ref[0, h : h + 1, :] = new
-        stat_ref[1, h : h + 1, :] = stat_ref[1, h : h + 1, :] * alpha + jnp.sum(
-            p, axis=0, keepdims=True
-        )
-        rows = vt.shape[0] // heads
-        acc_ref[h] = acc_ref[h] * alpha + jnp.dot(
-            vt[h * rows : (h + 1) * rows], p.astype(bf16), preferred_element_type=f32
-        )
-
-
-def attend(x, qt, key_up, value_up_t, expand, state, nope, rope, block):
-    heads, _, queries = qt.shape
+        m0, m1 = high[h : h + 1, :own_q], high_in[h : h + 1, :]
+        top = jnp.maximum(m0, m1)
+        a0, a1 = jnp.exp2((m0 - top) * scale), jnp.exp2((m1 - top) * scale)
+        total = acc[h, vrows : vrows + 1, :own_q] * a0 + acc_in[h, vrows : vrows + 1, :] * a1
+        merged = acc[h, :vrows, :own_q] * a0 + acc_in[h, :vrows, :] * a1
+        out_ref[h * vrows : (h + 1) * vrows, :] = (merged / total).astype(bf16)
+
+
+def attend(xp, qt, key_up, value_up_t, size):
+    heads, width, own_q = qt.shape
     vdim = value_up_t.shape[0] // heads
-    count = x.shape[0]
-    first = state is None
-    whole = lambda a: pl.BlockSpec(a.shape, lambda i: (0,) * a.ndim)
-    shapes = (
-        jax.ShapeDtypeStruct((heads, vdim, queries), f32),
-        jax.ShapeDtypeStruct((2, heads, queries), f32),
-    )
-    consts = (qt, key_up, value_up_t, expand)
-    extra = () if first else state
+    pieces = lax.axis_size("sp")
+    vmem = pl.BlockSpec(memory_space=pltpu.VMEM)
+    dma = pltpu.SemaphoreType.DMA
+    scale = math.log2(math.e) * size ** (-0.5)
     return pl.pallas_call(
-        functools.partial(attend_kernel, heads, nope, rope, first),
-        out_shape=shapes,
-        grid=(count // block,),
-        in_specs=[pl.BlockSpec((block, x.shape[1]), lambda i: (i, 0))]
-        + [whole(a) for a in consts + extra],
-        out_specs=tuple(whole(a) for a in shapes),
+        functools.partial(attend_kernel, heads, scale),
+        out_shape=jax.ShapeDtypeStruct((heads * vdim, own_q), bf16),
+        in_specs=[vmem] * 4,
+        out_specs=vmem,
+        scratch_shapes=[
+            pltpu.VMEM((pieces, *xp.shape[1:]), bf16),
+            pltpu.VMEM((2, heads, width, own_q), bf16),
+            pltpu.VMEM((heads, vdim + 16, 2 * own_q), f32),
+            pltpu.VMEM((heads, 2 * own_q), f32),
+            pltpu.VMEM((heads, vdim + 16, own_q), f32),
+            pltpu.VMEM((heads, own_q), f32),
+            dma((pieces,)),
+            dma((8, 4, 2)),
+            dma((3,)),
+            dma((8, 2)),
+            dma((8, 2)),
+            dma((8,)),
+            dma((6,)),
+        ],
+        compiler_params=pltpu.CompilerParams(
+            collective_id=0, has_side_effects=True, vmem_limit_bytes=56 * 2**20
+        ),
         cost_estimate=pl.CostEstimate(
-            flops=2 * count * queries * heads * 320,
-            bytes_accessed=count * 600,
-            transcendentals=count * queries * heads,
+            flops=2 * 128 * pieces * 2 * own_q * heads * 320,
+            bytes_accessed=2 * 10**6,
+            transcendentals=128 * pieces * 2 * own_q * heads,
         ),
         name="attend",
-    )(x, *consts, *extra)
+    )(xp, qt, key_up, value_up_t)
 
 
 def per_device(
@@ -170,7 +351,6 @@
     out_attend,
     out_conv,
 ):
-    sp = lax.axis_size("sp")
     row_count = tokens.shape[0]
     width = in_gain.shape[0]
     local_ch = conv_value.shape[1]
@@ -195,19 +375,8 @@
     heads = query_rope.shape[1] // rope_size
     nope = query_nope.shape[1] // heads
 
-    x = jnp.concatenate([kv_latent, rope_key], axis=1)
-    groups = [list(range(c, sp, 2)) for c in range(2)]
-    part = row_count // CHUNKS
-    gathered = [
-        lax.all_gather(
-            x[i * part : (i + 1) * part],
-            "sp",
-            axis=0,
-            tiled=True,
-            axis_index_groups=groups,
-        )
-        for i in range(CHUNKS)
-    ]
+    packed = jnp.transpose(rope_key.reshape(2, 8, 16, rope_size), (0, 2, 1, 3)).reshape(2, 16, 8 * rope_size)
+    xp = jnp.concatenate([kv_latent.reshape(2, row_count // 2, -1), packed], axis=1)
 
     q_heads = (
         jnp.dot(q_latent, query_nope, preferred_element_type=f32)
@@ -226,25 +395,9 @@
         else:
             cols += [r_heads[:, h], empty, q_heads[:, h]]
     q_own = jnp.transpose(jnp.concatenate(cols, axis=1))
-    swap = [(i, i ^ 1) for i in range(sp)]
-    q_other = lax.ppermute(q_own, "sp", swap)
-    qt = jnp.concatenate([q_own, q_other], axis=1).reshape(heads, 128, 2 * row_count)
-    expand = jnp.tile(jnp.eye(rope_size, dtype=bf16), (1, 128 // rope_size))
-    state = None
-    for i in range(CHUNKS):
-        state = attend(
-            gathered[i], qt, key_up, jnp.transpose(value_up), expand, state, nope, rope_size, 512
-        )
-    acc, stat = state
-    acc_other = lax.ppermute(acc[:, :, row_count:], "sp", swap)
-    stat_other = lax.ppermute(stat[:, :, row_count:], "sp", swap)
-    acc, stat = acc[:, :, :row_count], stat[:, :, :row_count]
-    scale = (nope + rope_size) ** (-0.5)
-    high = jnp.maximum(stat[0], stat_other[0])
-    a, b = jnp.exp((stat[0] - high) * scale), jnp.exp((stat_other[0] - high) * scale)
-    total = stat[1] * a + stat_other[1] * b
-    merged = (acc * a[:, None] + acc_other * b[:, None]) / total[:, None]
-    attended = merged.astype(bf16).reshape(-1, row_count)
+    attended = attend(
+        xp, q_own.reshape(heads, 128, row_count), key_up, jnp.transpose(value_up), nope + rope_size
+    )
 
     glu = (row_scale * value_pre * jax.nn.sigmoid(row_scale * gate_pre)).astype(bf16)
     taps = conv_taps.shape[0]

time: 388 us -> 127 us (0.33)
  waiting for transfers between devices: 253 us -> 13 us
  between operations: 14.1 us -> 0.66 us
  Pallas kernels: 46.3 us -> 55.2 us
  starting transfers between devices: 21.6 us -> 15.9 us
  other arithmetic: 10 us -> 5.57 us
    all_gather x4 -> x0, waiting for transfers between devices: 234 us -> none  [per_device(): lax.all_gather(x[i * part:(i + 1) * part], 'sp', axis=0, tiled=True, axis...]
    pallas_call x4 -> x1, Pallas kernels: 46.3 us -> 55.2 us  [attend(): pl.pallas_call(functools.partial(attend_kernel, heads, scale), out_shape=...]
    ppermute x3 -> x0, starting transfers between devices: 5.63 us -> none  [the longest x1 5.26 us: per_device(): stat_other = lax.ppermute(stat[:, :, row_count:], 'sp', swap)]
    all_to_all x2, waiting for transfers between devices: 17.2 us -> 13 us  [sent_to_all(): return lax.all_to_all(copies, axis, split_axis=0, concat_axis=0, tiled=True)]
  transfers between devices with their start and end apart: 11 -> 4, of which waited for: 7 -> 2; matrix products, arithmetic and copies ran while one was open for 6% -> 5% of each run, Pallas kernels for 9% -> 44%
where the time goes in v2:
time: 127 us
  Pallas kernels  55.2 us (43%)
  blocking collectives  17 us (13%)
  starting transfers between devices  15.9 us (13%)
  waiting for transfers between devices  13 us (10%)
  matrix products  12.6 us (10%)
  local copies, waits for them, and re-layouts  6.92 us (5%)
  other arithmetic  5.57 us (4%)
    pallas_call x1, Pallas kernels, attend(): pl.pallas_call(functools.partial(attend_kernel, heads, scale), out_shape=...  55.2 us
    all_to_all x1, blocking collectives, sum_at_owner(): lax.all_to_all(blocks, axis, split_axis=0, concat_axis=0, tiled=True)  17 us
    all_to_all x2, waiting for transfers between devices, sent_to_all(): return lax.all_to_all(copies, axis, split_axis=0, concat_axis=0, tiled=True)  13 us
    all_to_all x2, starting transfers between devices, sent_to_all(): return lax.all_to_all(copies, axis, split_axis=0, concat_axis=0, tiled=True)  8.21 us
    dot_general x5, matrix products, add_rows(): return jnp.dot(scaled, weight, preferred_element_type=f32)  6.46 us
    ppermute x1, starting transfers between devices, padded_2(): lax.ppermute(tail, axis, [(i, (i + 1) % count) for i in range(ends)])  5.79 us
    unnamed x69, local copies, waits for them, and re-layouts  3.89 us
    dot_general x1, matrix products, per_device(): lax.dot_general(out_attend, attended, (((0,), (0,)), ((), ())), preferred...  3.02 us
  transfers between devices with their start and end apart: 4, of which 2 were waited for; matrix products, arithmetic and copies ran while one was open for 5% of the time, Pallas kernels for 44%

profile of v2, /device:TPU:1, one launch (start us, length us, event | category | flops | bytes accessed | tf_op | source)
XLA Modules:
  0.0 126.8 jit_solution(4121807600649210466)
XLA Ops:
  0.0 1.2 copy.36
  1.2 1.1 broadcast_in_dim.6
  2.3 5.0 %all-to-all-start = ((bf16[4,256,512]{1,2,0:T(8,128)(2,1)}), bf16[4,256,512]{1,2,0:T(8,128)(2,1)S(1)}, u32[]{:S(2)}, u32[]{:S(2)}) async-start(bf16[4,256,512]{1,2,0:T(8,128)(2,1)} %broadcast_in_dim.6), calls=%async_computation | async-start | bytes 2097152 | tf_op jit(solution)/shard_map/all_to_all | solution.py:25
  7.3 0.8 copy.39
  8.1 0.7 fusion.61
  8.8 11.9 %all-to-all-done = bf16[4,256,512]{1,2,0:T(8,128)(2,1)S(1)} async-done(((bf16[4,256,512]{1,2,0:T(8,128)(2,1)}), bf16[4,256,512]{1,2,0:T(8,128)(2,1)S(1)}, u32[]{:S(2)}, u32[]{:S(2)}) %all-to-all-start) | async-done | bytes 1048608 | tf_op jit(solution)/shard_map/all_to_all | solution.py:25
  21.3 1.0 copy-done.1
  23.4 2.1 %multiply_reduce_fusion.3 = (f32[256]{0:T(256)S(1)}, f32[256,256]{1,0:T(8,128)S(1)}) fusion(bf16[256,2048]{0,1:T(8,128)(2,1)} %copy-done.1, bf16[2048,256]{1,0:T(8,128)(2,1)} %param.21, f32[256]{0:T(256)S(1)} %add_rsqrt_fusion.3), kind=kOutput, calls=%fused_computation.90 | convolution fusion | flops 268631808 | bytes 2361344 | tf_op jit(solution)/shard_map/dot_general | solution.py:362
  25.5 2.5 %fusion.5 = f32[256,512]{1,0:T(8,128)S(1)} fusion(bf16[256,2048]{0,1:T(8,128)(2,1)S(1)} %copy-done.2, bf16[2048,512]{1,0:T(8,128)(2,1)} %param.30, f32[256]{0:T(256)S(1)} %add_rsqrt_fusion.3), kind=kOutput, calls=%fused_computation.9 | convolution fusion | flops 537395200 | bytes 3671040 | tf_op jit(solution)/shard_map/dot_general | solution.py:362
  28.1 0.8 multiply_reduce_fusion.2
  28.9 0.8 copy-done.28
  29.7 0.7 fusion.7
  30.5 5.8 %collective-permute-start = (bf16[15,512]{1,0:T(8,128)(2,1)S(1)}, bf16[15,512]{1,0:T(8,128)(2,1)S(1)}, u32[]{:S(2)}, u32[]{:S(2)}) collective-permute-start(bf16[15,512]{1,0:T(8,128)(2,1)S(1)} %get-tuple-element.9), channel_id=1, source_target_pairs={{0,4},{4,8},{8,12},{12,16},{16,20},{20,24},{24,28},{28,32},{32,36}... | collective-permute-start | bytes 46088 | tf_op jit(solution)/shard_map/ppermute | solution.py:40
  36.3 1.9 %collective-permute-start.1 = (bf16[15,512]{1,0:T(8,128)(2,1)S(1)}, bf16[15,512]{1,0:T(8,128)(2,1)S(1)}, u32[]{:S(2)}, u32[]{:S(2)}) collective-permute-start(bf16[15,512]{1,0:T(8,128)(2,1)S(1)} %get-tuple-element.10), channel_id=1, source_target_pairs={{4,0},{8,4},{12,8},{16,12},{20,16},{24,20},{28,24},{32,28},{36,32}... | collective-permute-start | bytes 46088 | tf_op jit(solution)/shard_map/ppermute | solution.py:42
  39.2 0.7 pad_maximum_fusion.xp_ref
  40.0 55.2 %attend.1 = bf16[256,256]{1,0:T(8,128)(2,1)} custom-call(bf16[2,144,256]{2,1,0:T(8,128)(2,1)} %pad_maximum_fusion.xp_ref, bf16[4,128,256]{2,1,0:T(8,128)(2,1)} %bitcast.155, bf16[256,256]{1,0:T(8,128)(2,1)} %ku_ref.1, bf16[256,256]{1,0:T(8,128)(2,1)} %bitcast.121), custom_call_target="tpu_custom_call" | custom-call | flops 10737418240 | bytes 2000000 | tf_op jit(solution)/shard_map/attend/pallas_call | solution.py:302
  95.5 2.6 %fusion.58 = (f32[256]{0:T(256)S(1)}, f32[256,512]{1,0:T(8,128)S(1)}) fusion(f32[286,512]{1,0:T(8,128)S(1)} %maximum_convert_fusion, f32[512]{0:T(512)S(1)} %bitcast.133, f32[512]{0:T(512)S(1)} %bitcast.134, f32[512]{0:T(512)S(1)} %bitcast.136, f32[512]{0:T(512)S(1)} %bitcast.137, f32[512]{0:T(512)S(1)} %bitcast.138, f32[512]{0:T(512)S(1)} %bitcast.139, ...), kind=kLoop, calls=%fused_computation.145 | loop fusion | flops 8257280 | bytes 16843776 | tf_op jit(solution)/shard_map/reduce_sum | solution.py:410
  98.3 0.6 broadcast_in_dim.8
  98.9 3.2 %all-to-all-start.1 = ((f32[4,2,256]{2,1,0:T(2,128)}), f32[4,2,256]{2,1,0:T(2,128)S(1)}, u32[]{:S(2)}, u32[]{:S(2)}) async-start(f32[4,2,256]{2,1,0:T(2,128)} %broadcast_in_dim.8), calls=%async_computation.1 | async-start | bytes 16384 | tf_op jit(solution)/shard_map/all_to_all | solution.py:25
  102.1 3.0 %fusion.63 = f32[256,2048]{1,0:T(8,128)} fusion(bf16[256,256]{1,0:T(8,128)(2,1)S(1)} %copy-done.4, bf16[256,2048]{1,0:T(8,128)(2,1)} %param.34), kind=kOutput, calls=%fused_computation.149 | convolution fusion | flops 268435456 | bytes 3276800 | tf_op jit(solution)/shard_map/dot_general | solution.py:424
  105.2 1.1 all-to-all-done.1
  106.4 2.4 %fusion = bf16[256,2048]{1,0:T(8,128)(2,1)S(1)} fusion(f32[256,2048]{1,0:T(8,128)} %fusion.63, bf16[512,2048]{1,0:T(8,128)(2,1)S(1)} %copy-done, f32[256,512]{1,0:T(8,128)S(1)} %get-tuple-element.8, f32[512]{0:T(512)S(1)} %copy-done.29, f32[256]{0:T(256)S(1)} %add_rsqrt_fusion, f32[256]{0:T(256)S(1)} %broadcast_multiply_fusion), kind=kOutput, calls=%fused_computation.1 | convolution fusion | flops 538968064 | bytes 5771264 | tf_op jit(solution)/shard_map/dot_general | solution.py:427
  108.9 17.0 %all_to_all.15 = bf16[4,512,256]{1,2,0:T(8,128)(2,1)S(1)} all-to-all(bf16[4,512,256]{1,2,0:T(8,128)(2,1)S(1)} %bitcast.113), channel_id=1, replica_groups=mesh['sp'=64,'tp'=4] {'tp'}, dimensions={0} | all-to-all | bytes 2097152 | tf_op jit(solution)/shard_map/all_to_all | solution.py:57
  125.9 0.9 reduce_sum.92
  (102 shorter events, 3.2 us)
Async XLA Ops:
  0.0 106.3 %copy-start = (bf16[512,2048]{1,0:T(8,128)(2,1)S(1)}, bf16[512,2048]{1,0:T(8,128)(2,1)}, u32[]{:S(2)}) copy-start(bf16[512,2048]{1,0:T(8,128)(2,1)} %param.35) | copy-start | bytes 6291460
  2.3 18.6 %copy-start.9 = (f32[2048]{0:T(1024)S(1)}, f32[2048]{0:T(1024)}, u32[]{:S(2)}) copy-start(f32[2048]{0:T(1024)} %param.19) | copy-start | bytes 24580
  2.3 18.3 %all-to-all-start = ((bf16[4,256,512]{1,2,0:T(8,128)(2,1)}), bf16[4,256,512]{1,2,0:T(8,128)(2,1)S(1)}, u32[]{:S(2)}, u32[]{:S(2)}) async-start(bf16[4,256,512]{1,2,0:T(8,128)(2,1)} %broadcast_in_dim.6), calls=%async_computation | async-start | bytes 2097152 | tf_op jit(solution)/shard_map/all_to_all | solution.py:25
  7.3 15.0 %copy-start.7 = (bf16[2048,32]{0,1:T(8,128)(2,1)S(1)}, bf16[2048,32]{0,1:T(8,128)(2,1)}, u32[]{:S(2)}) copy-start(bf16[2048,32]{0,1:T(8,128)(2,1)} %param.22) | copy-start | bytes 393220
  29.7 8.5 %copy-start.10 = (f32[512]{0:T(512)S(1)}, f32[512]{0:T(512)}, u32[]{:S(2)}) copy-start(f32[512]{0:T(512)} %param.23) | copy-start | bytes 6148
  29.7 8.8 %copy-start.3 = (bf16[512,256]{1,0:T(8,128)(2,1)S(1)}, bf16[512,256]{1,0:T(8,128)(2,1)}, u32[]{:S(2)}) copy-start(bf16[512,256]{1,0:T(8,128)(2,1)} %param.25) | copy-start | bytes 786436
  30.4 8.6 %copy-start.26 = (f32[256]{0:T(256)S(1)}, f32[256]{0:T(256)}, u32[]{:S(2)}) copy-start(f32[256]{0:T(256)} %param.24) | copy-start | bytes 3076
  30.5 64.7 %collective-permute-start = (bf16[15,512]{1,0:T(8,128)(2,1)S(1)}, bf16[15,512]{1,0:T(8,128)(2,1)S(1)}, u32[]{:S(2)}, u32[]{:S(2)}) collective-permute-start(bf16[15,512]{1,0:T(8,128)(2,1)S(1)} %get-tuple-element.9), channel_id=1, source_target_pairs={{0,4},{4,8},{8,12},{12,16},{16,20},{20,24},{24,28},{28,32},{32,36}... | collective-permute-start | bytes 46088 | tf_op jit(solution)/shard_map/ppermute | solution.py:40
  36.3 58.9 %collective-permute-start.1 = (bf16[15,512]{1,0:T(8,128)(2,1)S(1)}, bf16[15,512]{1,0:T(8,128)(2,1)S(1)}, u32[]{:S(2)}, u32[]{:S(2)}) collective-permute-start(bf16[15,512]{1,0:T(8,128)(2,1)S(1)} %get-tuple-element.10), channel_id=1, source_target_pairs={{4,0},{8,4},{12,8},{16,12},{20,16},{24,20},{28,24},{32,28},{36,32}... | collective-permute-start | bytes 46088 | tf_op jit(solution)/shard_map/ppermute | solution.py:42
  39.9 55.4 %copy-start.11 = (f32[1,512]{1,0:T(1,128)S(1)}, f32[1,512]{1,0:T(1,128)}, u32[]{:S(2)}) copy-start(f32[1,512]{1,0:T(1,128)} %get-tuple-element.19) | copy-start | bytes 6148
  39.9 55.4 %copy-start.12 = (f32[1,512]{1,0:T(1,128)S(1)}, f32[1,512]{1,0:T(1,128)}, u32[]{:S(2)}) copy-start(f32[1,512]{1,0:T(1,128)} %get-tuple-element.20) | copy-start | bytes 6148
  39.9 55.4 %copy-start.13 = (f32[1,512]{1,0:T(1,128)S(1)}, f32[1,512]{1,0:T(1,128)}, u32[]{:S(2)}) copy-start(f32[1,512]{1,0:T(1,128)} %get-tuple-element.21) | copy-start | bytes 6148
  39.9 55.5 %copy-start.14 = (f32[1,512]{1,0:T(1,128)S(1)}, f32[1,512]{1,0:T(1,128)}, u32[]{:S(2)}) copy-start(f32[1,512]{1,0:T(1,128)} %get-tuple-element.22) | copy-start | bytes 6148
  39.9 55.5 %copy-start.15 = (f32[1,512]{1,0:T(1,128)S(1)}, f32[1,512]{1,0:T(1,128)}, u32[]{:S(2)}) copy-start(f32[1,512]{1,0:T(1,128)} %get-tuple-element.23) | copy-start | bytes 6148
  39.9 55.5 %copy-start.16 = (f32[1,512]{1,0:T(1,128)S(1)}, f32[1,512]{1,0:T(1,128)}, u32[]{:S(2)}) copy-start(f32[1,512]{1,0:T(1,128)} %get-tuple-element.24) | copy-start | bytes 6148
  39.9 55.5 %copy-start.17 = (f32[1,512]{1,0:T(1,128)S(1)}, f32[1,512]{1,0:T(1,128)}, u32[]{:S(2)}) copy-start(f32[1,512]{1,0:T(1,128)} %get-tuple-element.25) | copy-start | bytes 6148
  39.9 55.5 %copy-start.18 = (f32[1,512]{1,0:T(1,128)S(1)}, f32[1,512]{1,0:T(1,128)}, u32[]{:S(2)}) copy-start(f32[1,512]{1,0:T(1,128)} %get-tuple-element.26) | copy-start | bytes 6148
  39.9 55.5 %copy-start.19 = (f32[1,512]{1,0:T(1,128)S(1)}, f32[1,512]{1,0:T(1,128)}, u32[]{:S(2)}) copy-start(f32[1,512]{1,0:T(1,128)} %get-tuple-element.27) | copy-start | bytes 6148
  39.9 55.5 %copy-start.20 = (f32[1,512]{1,0:T(1,128)S(1)}, f32[1,512]{1,0:T(1,128)}, u32[]{:S(2)}) copy-start(f32[1,512]{1,0:T(1,128)} %get-tuple-element.28) | copy-start | bytes 6148
  40.0 55.5 %copy-start.21 = (f32[1,512]{1,0:T(1,128)S(1)}, f32[1,512]{1,0:T(1,128)}, u32[]{:S(2)}) copy-start(f32[1,512]{1,0:T(1,128)} %get-tuple-element.29) | copy-start | bytes 6148
  40.0 55.5 %copy-start.22 = (f32[1,512]{1,0:T(1,128)S(1)}, f32[1,512]{1,0:T(1,128)}, u32[]{:S(2)}) copy-start(f32[1,512]{1,0:T(1,128)} %get-tuple-element.30) | copy-start | bytes 6148
  40.0 55.5 %copy-start.23 = (f32[1,512]{1,0:T(1,128)S(1)}, f32[1,512]{1,0:T(1,128)}, u32[]{:S(2)}) copy-start(f32[1,512]{1,0:T(1,128)} %get-tuple-element.31) | copy-start | bytes 6148
  40.0 55.5 %copy-start.25 = (f32[512]{0:T(512)S(1)}, f32[512]{0:T(512)}, u32[]{:S(2)}) copy-start(f32[512]{0:T(512)} %param.32) | copy-start | bytes 6148
  98.9 7.4 %all-to-all-start.1 = ((f32[4,2,256]{2,1,0:T(2,128)}), f32[4,2,256]{2,1,0:T(2,128)S(1)}, u32[]{:S(2)}, u32[]{:S(2)}) async-start(f32[4,2,256]{2,1,0:T(2,128)} %broadcast_in_dim.8), calls=%async_computation.1 | async-start | bytes 16384 | tf_op jit(solution)/shard_map/all_to_all | solution.py:25
  (10 other events, 47.8 us)

commit v3 on v2

v3 whole, which is shorter than its diff:
```python
import functools
import math

import jax
import jax.numpy as jnp
from jax import lax
from jax.experimental import pallas as pl
from jax.experimental.pallas import tpu as pltpu
from jax.sharding import PartitionSpec as P

eps_norm = 1e-06
eps_layer = 1e-05
theta = 10000.0
bf16 = jnp.bfloat16
f32 = jnp.float32

def laid_out(blocks, dim):
    dims = list(blocks.shape[1:])
    dims[dim] *= blocks.shape[0]
    return jnp.moveaxis(blocks, 0, dim).reshape(dims)


def sent_to_all(shard, axis):
    copies = jnp.broadcast_to(shard, (lax.axis_size(axis), *shard.shape))
    return lax.all_to_all(copies, axis, split_axis=0, concat_axis=0, tiled=True)


def gather_directly(shard, axis, dim):
    return laid_out(sent_to_all(shard, axis), dim)


def padded_2(cells, sides, width):
    for axis, dim in sides:
        count = lax.axis_size(axis)
        ends = count - 1
        head = lax.slice_in_dim(cells, 0, width, axis=dim)
        tail = lax.slice_in_dim(cells, cells.shape[dim] - width, cells.shape[dim], axis=dim)
        cells = jnp.concatenate(
            [
                lax.ppermute(tail, axis, [(i, (i + 1) % count) for i in range(ends)]),
                cells,
                lax.ppermute(head, axis, [((i + 1) % count, i) for i in range(ends)]),
            ],
            axis=dim,
        )
    return cells


def cut_along(shard, dim, peers):
    dims = shard.shape
    blocks = shard.reshape(*dims[:dim], peers, dims[dim] // peers, *dims[dim + 1 :])
    return jnp.moveaxis(blocks, dim, 0)


def sum_at_owner(shard, axis, dim):
    blocks = cut_along(shard, dim, lax.axis_size(axis))
    arrived = lax.all_to_all(blocks, axis, split_axis=0, concat_axis=0, tiled=True)
    return arrived.astype(f32).sum(axis=0)


def rms_scale(values, gain):
    return values * lax.rsqrt(jnp.mean(values * values, axis=-1, keepdims=True) + eps_norm) * gain


def rotate(values, positions):
    half = values.shape[-1] // 2
    freqs = theta ** (-jnp.arange(half).astype(f32) / half)
    angles = positions[..., None] * freqs
    cosine = jnp.cos(angles)
    sine = jnp.sin(angles)
    first = values[..., :half]
    second = values[..., half:]
    return jnp.concatenate(
        [first * cosine - second * sine, second * cosine + first * sine], axis=-1
    )


def attend_kernel(
    heads, scale, xp_ref, qt_ref, ku_ref, vut_ref, out_ref,
    x, q, keys, vals, acc, high, acc_in, high_in, part_out, part_in,
    got_x, sent_x, got_q, sent_q, sent_relay, sent_pair_q, got_pair_q, pair_sem, part_sem,
):
    sp, tp = lax.axis_index("sp"), lax.axis_index("tp")
    core = lax.rem(sp, 2)
    y = lax.rem(sp // 2, 4)
    z = sp // 8
    own_q = qt_ref.shape[2]
    depth = xp_ref.shape[1] - 16
    vrows = vut_ref.shape[0] // heads
    half_heads = heads // 2

    def device(pz, py):
        return (((pz * 4 + py) * 2 + core), tp)

    def turn(a, n):
        return lax.rem(a + 2 * n, n)

    up, down = device(turn(z + 1, 8), y), device(turn(z - 1, 8), y)
    right, left = device(z, turn(y + 1, 4)), device(z, turn(y - 1, 4))
    across = device(z, turn(y + 2, 4))
    sibling = (sp + 1 - 2 * core, tp)

    def remote(src, dst, sent, got, target):
        return pltpu.make_async_remote_copy(
            src_ref=src, dst_ref=dst, send_sem=sent, recv_sem=got,
            device_id=target, device_id_type=pl.DeviceIdType.MESH,
        )

    barrier = pltpu.get_barrier_semaphore()
    peers = (up, down, right, left, across, sibling)
    for peer in peers:
        pl.semaphore_signal(barrier, inc=1, device_id=peer, device_id_type=pl.DeviceIdType.MESH)
    pl.semaphore_wait(barrier, len(peers))

    def plane(k):
        return turn(z + (1 - 2 * lax.rem(k, 2)) * ((k + 1) // 2), 8)

    def x_copy(k, n, target):
        at = x.at[plane(k), n]
        return remote(at, at, sent_x.at[k, n], got_x.at[plane(k), n], target)

    def part_of(ref, n):
        return ref.at[n * half_heads : (n + 1) * half_heads]

    def q_slot(py, who, n):
        return q.at[py, who, n * half_heads : (n + 1) * half_heads]

    first = []
    for n in range(2):
        for way, target in enumerate((up, down)):
            first.append(
                remote(xp_ref.at[n], x.at[z, n], sent_x.at[7 * way, n], got_x.at[z, n], target)
            )
    for n in range(2):
        for way, target in enumerate((right, left)):
            m = n if way == 0 else 1 - n
            first.append(
                remote(part_of(qt_ref, m), q_slot(y, core, m), sent_q.at[way, m], got_q.at[y, m], target)
            )
    for n in range(2):
        first.append(
            remote(
                part_of(qt_ref, n), q_slot(y, core, n), sent_pair_q.at[0, n],
                got_pair_q.at[y, n], sibling,
            )
        )
    for copy in first:
        copy.start()
    x[z] = xp_ref[...]
    q[y, core] = qt_ref[...]
    acc[...] = jnp.zeros_like(acc)
    high[...] = jnp.full_like(high, -jnp.inf)

    def x_next(k):
        return [
            (x_copy(k, n, up if k % 2 else down), k < 5 or (k == 5 and n == 0) or (k == 6 and n == 1))
            for n in range(2)
        ]

    def x_first(k):
        for copy, goes in x_next(k):
            copy.wait_recv()
            if goes:
                copy.start()

    def pair_q(r, n):
        py = turn(y + r, 4)
        at = q_slot(py, core, n)
        return remote(at, at, sent_pair_q.at[r, n], got_pair_q.at[py, n], sibling)

    def arrived_q(r, n):
        py = turn(y + r, 4)
        at = q_slot(py, core, n)
        remote(at, at, sent_relay.at[n], got_q.at[py, n], sibling).wait_recv()

    def relay_q(n):
        py = turn(y - 1 + 2 * n, 4)
        at = q_slot(py, core, n)
        return remote(at, at, sent_relay.at[n], got_q.at[py, n], right if n == 0 else left)

    def pair_arrived(r):
        py = turn(y + r, 4)
        for n in range(2):
            at = q_slot(py, 1 - core, n)
            remote(at, at, sent_relay.at[n], got_pair_q.at[py, n], sibling).wait_recv()

    def q_from(r, order):
        for n in order:
            arrived_q(r, n)
            if (r, n) in ((3, 0), (1, 1)):
                relay_q(n).start()
            pair_q(r, n).start()

    def swap(r):
        return [
            remote(
                acc.at[r, :, :, own_q:], acc_in.at[r], pair_sem.at[r, 0], pair_sem.at[r, 1], sibling
            ),
            remote(high.at[r, :, own_q:], high_in.at[r], pair_sem.at[r, 2], pair_sem.at[r, 3], sibling),
        ]

    def swap_start(r):
        for copy in swap(r):
            copy.start()

    def part_copy(r):
        return remote(
            part_out.at[r - 1], part_in.at[r - 1], part_sem.at[r - 1, 0], part_sem.at[r - 1, 1],
            {1: right, 2: across, 3: left}[r],
        )

    def merge(r):
        for copy in swap(r):
            copy.wait()
        for h in range(heads):
            m0, m1 = high[r, h : h + 1, :own_q], high_in[r, h : h + 1, :]
            top = jnp.maximum(m0, m1)
            a0, a1 = jnp.exp2((m0 - top) * scale), jnp.exp2((m1 - top) * scale)
            part_out[r - 1, h, :vrows, :] = (
                acc[r, h, :vrows, :own_q] * a0 + acc_in[r, h, :vrows, :] * a1
            )
            total = acc[r, h, vrows : vrows + 1, :own_q] * a0 + acc_in[r, h, vrows : vrows + 1, :] * a1
            part_out[r - 1, h, vrows:, :] = jnp.concatenate([total] * 4 + [top] * 4, axis=0)
        part_copy(r).start()

    def expand(c):
        at = [plane(2 * c), plane(2 * c + 1)]
        latent = jnp.concatenate([x[s, n, :depth, :] for s in at for n in range(2)], axis=0)
        k = jnp.dot(latent, ku_ref[...], preferred_element_type=f32).astype(bf16)
        vt = lax.dot_general(
            vut_ref[...], latent, (((1,), (1,)), ((), ())), preferred_element_type=f32
        ).astype(bf16)
        even, odd = [], []
        for s in at:
            for n in range(2):
                for half in range(2):
                    part = x[s, n, depth:, 128 * half : 128 * half + 128].astype(f32)
                    r1, r2, r3 = (pltpu.roll(part, 32 * m, 1) for m in (1, 2, 3))
                    even += [r2, r1, part, r3]
                    odd += [part, r3, r2, r1]
        even = jnp.concatenate(even, axis=0).astype(bf16)
        odd = jnp.concatenate(odd, axis=0).astype(bf16)
        lane = lax.broadcasted_iota(jnp.int32, even.shape, 1)
        for h in range(heads):
            pair = k[:, 128 * (h // 2) : 128 * (h // 2) + 128]
            keys[c, h] = (
                jnp.where(lane < 64, pair, even) if h % 2 == 0 else jnp.where(lane >= 64, pair, odd)
            )
            vals[c, h, :vrows, :] = vt[h * vrows : (h + 1) * vrows]
            vals[c, h, vrows:, :] = jnp.ones((16, vt.shape[1]), bf16)

    def compute(r, c):
        py = turn(y + r, 4)

        def score(h):
            both = jnp.concatenate([q[py, core, h], q[py, 1 - core, h]], axis=1)
            return jnp.dot(keys[c, h], both, preferred_element_type=f32)

        following = score(0)
        for h in range(heads):
            s = following
            if h + 1 < heads:
                following = score(h + 1)
            old = high[r, h : h + 1, :]
            new = jnp.maximum(old, jnp.max(s, axis=0, keepdims=True))
            alpha = jnp.exp2((old - new) * scale)
            p = jnp.exp2((s - new) * scale).astype(bf16)
            high[r, h : h + 1, :] = new
            acc[r, h] = acc[r, h] * alpha + jnp.dot(vals[c, h], p, preferred_element_type=f32)

    x_first(1)
    x_first(2)
    expand(0)
    pair_arrived(0)

    def before(step):
        if step == 1:
            x_first(3)
            x_first(4)
            q_from(1, (1, 0))
            q_from(3, (0, 1))
            pair_arrived(1)
        if step == 2:
            expand(1)
        if step == 3:
            x_first(5)
            x_first(6)
            expand(2)
        if step == 4:
            x_first(7)
            q_from(2, (0, 1))
            expand(3)
        if step == 5:
            pair_arrived(2)
            swap_start(1)
        if step == 6:
            merge(1)
        if step == 9:
            pair_arrived(3)
            swap_start(2)
        if step == 10:
            merge(2)
        if step == 13:
            swap_start(3)
        if step == 14:
            merge(3)

    @pl.loop(0, 16)
    def _(step):
        for s in (1, 2, 3, 4, 5, 6, 9, 10, 13, 14):
            pl.when(step == s)(functools.partial(before, s))
        r = lax.rem((step + 3) // 4, 4)
        c = lax.rem(step + 3, 4) + (step + 3) // 16 - 3 * (1 - (step + 15) // 16)
        compute(r, c)

    swap_start(0)
    for copy in first:
        copy.wait_send()
    for k in range(1, 8):
        for copy, goes in x_next(k):
            if goes:
                copy.wait_send()
    for n in range(2):
        relay_q(n).wait_send()
        for r in range(1, 4):
            pair_q(r, n).wait_send()
    for r in range(1, 4):
        part_copy(r).wait()
    for copy in swap(0):
        copy.wait()
    for h in range(heads):
        tops = [high[0, h : h + 1, :own_q], high_in[0, h : h + 1, :]]
        parts = [acc[0, h, : vrows + 1, :own_q], acc_in[0, h, : vrows + 1, :]]
        for r in range(3):
            tops.append(part_in[r, h, vrows + 4 : vrows + 5, :])
            parts.append(part_in[r, h, : vrows + 1, :])
        top = functools.reduce(jnp.maximum, tops)
        whole = sum(p * jnp.exp2((m - top) * scale) for p, m in zip(parts, tops))
        out_ref[h * vrows : (h + 1) * vrows, :] = (whole[:vrows] / whole[vrows : vrows + 1]).astype(bf16)


def attend(xp, qt, key_up, value_up_t, size):
    heads, width, own_q = qt.shape
    vdim = value_up_t.shape[0] // heads
    vmem = pl.BlockSpec(memory_space=pltpu.VMEM)
    dma = pltpu.SemaphoreType.DMA
    scale = math.log2(math.e) * size ** (-0.5)
    return pl.pallas_call(
        functools.partial(attend_kernel, heads, scale),
        out_shape=jax.ShapeDtypeStruct((heads * vdim, own_q), bf16),
        in_specs=[vmem] * 4,
        out_specs=vmem,
        scratch_shapes=[
            pltpu.VMEM((8, *xp.shape), bf16),
            pltpu.VMEM((4, 2, heads, width, own_q), bf16),
            pltpu.VMEM((4, heads, 2 * own_q, width), bf16),
            pltpu.VMEM((4, heads, vdim + 16, 2 * own_q), bf16),
            pltpu.VMEM((4, heads, vdim + 16, 2 * own_q), f32),
            pltpu.VMEM((4, heads, 2 * own_q), f32),
            pltpu.VMEM((4, heads, vdim + 16, own_q), f32),
            pltpu.VMEM((4, heads, own_q), f32),
            pltpu.VMEM((3, heads, vdim + 8, own_q), f32),
            pltpu.VMEM((3, heads, vdim + 8, own_q), f32),
            dma((8, 2)),
            dma((8, 2)),
            dma((4, 2)),
            dma((2, 2)),
            dma((2,)),
            dma((4, 2)),
            dma((4, 2)),
            dma((4, 4)),
            dma((3, 2)),
        ],
        compiler_params=pltpu.CompilerParams(
            collective_id=0, has_side_effects=True, vmem_limit_bytes=56 * 2**20
        ),
        cost_estimate=pl.CostEstimate(
            flops=2 * 8192 * 2 * own_q * heads * 320,
            bytes_accessed=2 * 10**6,
            transcendentals=8192 * 2 * own_q * heads,
        ),
        name="attend",
    )(xp, qt, key_up, value_up_t)


def per_device(
    tokens,
    in_gain,
    query_down,
    latent_down,
    rope_down,
    query_gain,
    latent_gain,
    query_nope,
    query_rope,
    key_up,
    value_up,
    conv_value,
    conv_gate,
    conv_taps,
    conv_bias,
    channel_gain,
    out_attend,
    out_conv,
):
    row_count = tokens.shape[0]
    width = in_gain.shape[0]
    local_ch = conv_value.shape[1]
    positions = (lax.axis_index("sp") * row_count + jnp.arange(row_count)).astype(f32)
    piece_f = gather_directly(tokens, "tp", 1).astype(f32)
    scaled = (piece_f * in_gain).astype(bf16)

    def add_rows(weight):
        return jnp.dot(scaled, weight, preferred_element_type=f32)

    square_sum = jnp.sum(piece_f * piece_f, axis=1)
    q_pre = add_rows(query_down)
    kv_pre = add_rows(latent_down)
    rope_pre = add_rows(rope_down)
    value_pre = add_rows(conv_value)
    gate_pre = add_rows(conv_gate)
    row_scale = lax.rsqrt(square_sum / width + eps_norm)[:, None]
    q_latent = rms_scale(row_scale * q_pre, query_gain).astype(bf16)
    kv_latent = rms_scale(row_scale * kv_pre, latent_gain).astype(bf16)
    rope_key = rotate(row_scale * rope_pre, positions).astype(bf16)
    rope_size = rope_down.shape[1]
    heads = query_rope.shape[1] // rope_size
    nope = query_nope.shape[1] // heads

    packed = jnp.transpose(rope_key.reshape(2, 8, 16, rope_size), (0, 2, 1, 3)).reshape(2, 16, 8 * rope_size)
    xp = jnp.concatenate([kv_latent.reshape(2, row_count // 2, -1), packed], axis=1)

    q_heads = (
        jnp.dot(q_latent, query_nope, preferred_element_type=f32)
        .astype(bf16)
        .reshape(row_count, heads, nope)
    )
    q_turn = jnp.dot(q_latent, query_rope, preferred_element_type=f32).reshape(
        row_count, heads, rope_size
    )
    r_heads = rotate(q_turn, positions[:, None]).astype(bf16)
    empty = jnp.zeros((row_count, 64 - rope_size), bf16)
    cols = []
    for h in range(heads):
        if h % 2 == 0:
            cols += [q_heads[:, h], r_heads[:, h], empty]
        else:
            cols += [r_heads[:, h], empty, q_heads[:, h]]
    q_own = jnp.transpose(jnp.concatenate(cols, axis=1))
    attended = attend(
        xp, q_own.reshape(heads, 128, row_count), key_up, jnp.transpose(value_up), nope + rope_size
    )

    glu = (row_scale * value_pre * jax.nn.sigmoid(row_scale * gate_pre)).astype(bf16)
    taps = conv_taps.shape[0]
    padded = padded_2(glu, (("sp", 0),), taps // 2).astype(f32)
    conv = jnp.zeros((row_count, local_ch), f32) + conv_bias
    for tap in range(taps):
        conv = conv + conv_taps[tap] * padded[tap : tap + row_count]
    peers = lax.axis_size("tp")
    channels = local_ch * peers
    own_mean = jnp.mean(conv, axis=-1)
    off = conv - own_mean[:, None]
    own_spread = jnp.sum(off * off, axis=-1)
    sums = sent_to_all(jnp.stack([own_mean, own_spread]), "tp")
    means = sums[:, 0]
    mean = jnp.mean(means, axis=0)
    apart = means - mean
    spread = (jnp.sum(sums[:, 1], axis=0) + local_ch * jnp.sum(apart * apart, axis=0)) / channels
    centred = conv - mean[:, None]
    activated = jax.nn.silu(
        centred * lax.rsqrt(spread[:, None] + eps_layer) * channel_gain
    ).astype(bf16)
    summed = sum_at_owner(
        (
            lax.dot_general(
                out_attend, attended, (((0,), (0,)), ((), ())), preferred_element_type=f32
            )
            + lax.dot_general(
                out_conv, activated, (((0,), (1,)), ((), ())), preferred_element_type=f32
            )
        ).astype(bf16),
        "tp",
        0,
    )
    return jnp.transpose(summed).astype(bf16)


def solution(mesh):
    in_specs = (
        P("sp", "tp"),
        P(),
        P(),
        P(),
        P(),
        P(),
        P(),
        P(None, "tp"),
        P(None, "tp"),
        P(None, "tp"),
        P(None, "tp"),
        P(None, "tp"),
        P(None, "tp"),
        P(None, "tp"),
        P("tp"),
        P("tp"),
        P("tp", None),
        P("tp", None),
    )
    return jax.shard_map(
        per_device, mesh=mesh, in_specs=in_specs, out_specs=P("sp", "tp"), check_vma=False
    )
```

time: 127 us -> 129 us (1.016)
  Pallas kernels: 55.2 us -> 56.7 us
    pallas_call x1, Pallas kernels: 55.2 us -> 56.7 us  [attend(): pl.pallas_call(functools.partial(attend_kernel, heads, scale), out_shape=...]
where the time goes in v3:
time: 129 us; the launch traced here: 128 us
  Pallas kernels  56.7 us (44%)
  blocking collectives  16.9 us (13%)
  starting transfers between devices  15.9 us (12%)
  waiting for transfers between devices  13 us (10%)
  matrix products  12.6 us (10%)
  local copies, waits for them, and re-layouts  6.92 us (5%)
  other arithmetic  5.57 us (4%)
    pallas_call x1, Pallas kernels, attend(): pl.pallas_call(functools.partial(attend_kernel, heads, scale), out_shape=...  56.7 us
    all_to_all x1, blocking collectives, sum_at_owner(): lax.all_to_all(blocks, axis, split_axis=0, concat_axis=0, tiled=True)  16.9 us
    all_to_all x2, waiting for transfers between devices, sent_to_all(): return lax.all_to_all(copies, axis, split_axis=0, concat_axis=0, tiled=True)  13 us
    all_to_all x2, starting transfers between devices, sent_to_all(): return lax.all_to_all(copies, axis, split_axis=0, concat_axis=0, tiled=True)  8.21 us
    dot_general x5, matrix products, add_rows(): return jnp.dot(scaled, weight, preferred_element_type=f32)  6.46 us
    ppermute x1, starting transfers between devices, padded_2(): lax.ppermute(tail, axis, [(i, (i + 1) % count) for i in range(ends)])  5.79 us
    unnamed x69, local copies, waits for them, and re-layouts  3.89 us
    dot_general x1, matrix products, per_device(): lax.dot_general(out_attend, attended, (((0,), (0,)), ((), ())), preferred...  3.02 us
  transfers between devices with their start and end apart: 4, of which 2 were waited for; matrix products, arithmetic and copies ran while one was open for 5% of the time, Pallas kernels for 44%

profile of v3, /device:TPU:1, one launch (start us, length us, event | category | flops | bytes accessed | tf_op | source)
XLA Modules:
  0.0 128.2 jit_solution(2035795018143149238)
XLA Ops:
  0.0 1.2 copy.36
  1.2 1.1 broadcast_in_dim.6
  2.3 5.0 %all-to-all-start = ((bf16[4,256,512]{1,2,0:T(8,128)(2,1)}), bf16[4,256,512]{1,2,0:T(8,128)(2,1)S(1)}, u32[]{:S(2)}, u32[]{:S(2)}) async-start(bf16[4,256,512]{1,2,0:T(8,128)(2,1)} %broadcast_in_dim.6), calls=%async_computation | async-start | bytes 2097152 | tf_op jit(solution)/shard_map/all_to_all | solution.py:25
  7.3 0.8 copy.39
  8.1 0.7 fusion.61
  8.8 11.9 %all-to-all-done = bf16[4,256,512]{1,2,0:T(8,128)(2,1)S(1)} async-done(((bf16[4,256,512]{1,2,0:T(8,128)(2,1)}), bf16[4,256,512]{1,2,0:T(8,128)(2,1)S(1)}, u32[]{:S(2)}, u32[]{:S(2)}) %all-to-all-start) | async-done | bytes 1048608 | tf_op jit(solution)/shard_map/all_to_all | solution.py:25
  21.3 1.0 copy-done.1
  23.4 2.1 %multiply_reduce_fusion.3 = (f32[256]{0:T(256)S(1)}, f32[256,256]{1,0:T(8,128)S(1)}) fusion(bf16[256,2048]{0,1:T(8,128)(2,1)} %copy-done.1, bf16[2048,256]{1,0:T(8,128)(2,1)} %param.21, f32[256]{0:T(256)S(1)} %add_rsqrt_fusion.3), kind=kOutput, calls=%fused_computation.90 | convolution fusion | flops 268631808 | bytes 2361344 | tf_op jit(solution)/shard_map/dot_general | solution.py:414
  25.5 2.5 %fusion.5 = f32[256,512]{1,0:T(8,128)S(1)} fusion(bf16[256,2048]{0,1:T(8,128)(2,1)S(1)} %copy-done.2, bf16[2048,512]{1,0:T(8,128)(2,1)} %param.30, f32[256]{0:T(256)S(1)} %add_rsqrt_fusion.3), kind=kOutput, calls=%fused_computation.9 | convolution fusion | flops 537395200 | bytes 3671040 | tf_op jit(solution)/shard_map/dot_general | solution.py:414
  28.1 0.8 multiply_reduce_fusion.2
  28.9 0.8 copy-done.28
  29.7 0.7 fusion.7
  30.5 5.8 %collective-permute-start = (bf16[15,512]{1,0:T(8,128)(2,1)S(1)}, bf16[15,512]{1,0:T(8,128)(2,1)S(1)}, u32[]{:S(2)}, u32[]{:S(2)}) collective-permute-start(bf16[15,512]{1,0:T(8,128)(2,1)S(1)} %get-tuple-element.9), channel_id=1, source_target_pairs={{0,4},{4,8},{8,12},{12,16},{16,20},{20,24},{24,28},{28,32},{32,36}... | collective-permute-start | bytes 46088 | tf_op jit(solution)/shard_map/ppermute | solution.py:40
  36.3 1.9 %collective-permute-start.1 = (bf16[15,512]{1,0:T(8,128)(2,1)S(1)}, bf16[15,512]{1,0:T(8,128)(2,1)S(1)}, u32[]{:S(2)}, u32[]{:S(2)}) collective-permute-start(bf16[15,512]{1,0:T(8,128)(2,1)S(1)} %get-tuple-element.10), channel_id=1, source_target_pairs={{4,0},{8,4},{12,8},{16,12},{20,16},{24,20},{28,24},{32,28},{36,32}... | collective-permute-start | bytes 46088 | tf_op jit(solution)/shard_map/ppermute | solution.py:42
  39.2 0.7 pad_maximum_fusion.xp_ref
  40.0 56.7 %attend.1 = bf16[256,256]{1,0:T(8,128)(2,1)} custom-call(bf16[2,144,256]{2,1,0:T(8,128)(2,1)} %pad_maximum_fusion.xp_ref, bf16[4,128,256]{2,1,0:T(8,128)(2,1)} %bitcast.155, bf16[256,256]{1,0:T(8,128)(2,1)} %ku_ref.1, bf16[256,256]{1,0:T(8,128)(2,1)} %bitcast.121), custom_call_target="tpu_custom_call" | custom-call | flops 10737418240 | bytes 2000000 | tf_op jit(solution)/shard_map/attend/pallas_call | solution.py:348
  97.0 2.6 %fusion.58 = (f32[256]{0:T(256)S(1)}, f32[256,512]{1,0:T(8,128)S(1)}) fusion(f32[286,512]{1,0:T(8,128)S(1)} %maximum_convert_fusion, f32[512]{0:T(512)S(1)} %bitcast.133, f32[512]{0:T(512)S(1)} %bitcast.134, f32[512]{0:T(512)S(1)} %bitcast.136, f32[512]{0:T(512)S(1)} %bitcast.137, f32[512]{0:T(512)S(1)} %bitcast.138, f32[512]{0:T(512)S(1)} %bitcast.139, ...), kind=kLoop, calls=%fused_computation.145 | loop fusion | flops 8257280 | bytes 16843776 | tf_op jit(solution)/shard_map/reduce_sum | solution.py:462
  99.8 0.6 broadcast_in_dim.8
  100.4 3.2 %all-to-all-start.1 = ((f32[4,2,256]{2,1,0:T(2,128)}), f32[4,2,256]{2,1,0:T(2,128)S(1)}, u32[]{:S(2)}, u32[]{:S(2)}) async-start(f32[4,2,256]{2,1,0:T(2,128)} %broadcast_in_dim.8), calls=%async_computation.1 | async-start | bytes 16384 | tf_op jit(solution)/shard_map/all_to_all | solution.py:25
  103.6 3.0 %fusion.63 = f32[256,2048]{1,0:T(8,128)} fusion(bf16[256,256]{1,0:T(8,128)(2,1)S(1)} %copy-done.4, bf16[256,2048]{1,0:T(8,128)(2,1)} %param.34), kind=kOutput, calls=%fused_computation.149 | convolution fusion | flops 268435456 | bytes 3276800 | tf_op jit(solution)/shard_map/dot_general | solution.py:476
  106.7 1.1 all-to-all-done.1
  107.9 2.4 %fusion = bf16[256,2048]{1,0:T(8,128)(2,1)S(1)} fusion(f32[256,2048]{1,0:T(8,128)} %fusion.63, bf16[512,2048]{1,0:T(8,128)(2,1)S(1)} %copy-done, f32[256,512]{1,0:T(8,128)S(1)} %get-tuple-element.8, f32[512]{0:T(512)S(1)} %copy-done.29, f32[256]{0:T(256)S(1)} %add_rsqrt_fusion, f32[256]{0:T(256)S(1)} %broadcast_multiply_fusion), kind=kOutput, calls=%fused_computation.1 | convolution fusion | flops 538968064 | bytes 5771264 | tf_op jit(solution)/shard_map/dot_general | solution.py:479
  110.4 16.9 %all_to_all.15 = bf16[4,512,256]{1,2,0:T(8,128)(2,1)S(1)} all-to-all(bf16[4,512,256]{1,2,0:T(8,128)(2,1)S(1)} %bitcast.113), channel_id=1, replica_groups=mesh['sp'=64,'tp'=4] {'tp'}, dimensions={0} | all-to-all | bytes 2097152 | tf_op jit(solution)/shard_map/all_to_all | solution.py:57
  127.3 0.9 reduce_sum.92
  (102 shorter events, 3.2 us)
Async XLA Ops:
  0.0 107.8 %copy-start = (bf16[512,2048]{1,0:T(8,128)(2,1)S(1)}, bf16[512,2048]{1,0:T(8,128)(2,1)}, u32[]{:S(2)}) copy-start(bf16[512,2048]{1,0:T(8,128)(2,1)} %param.35) | copy-start | bytes 6291460
  2.3 18.6 %copy-start.9 = (f32[2048]{0:T(1024)S(1)}, f32[2048]{0:T(1024)}, u32[]{:S(2)}) copy-start(f32[2048]{0:T(1024)} %param.19) | copy-start | bytes 24580
  2.3 18.3 %all-to-all-start = ((bf16[4,256,512]{1,2,0:T(8,128)(2,1)}), bf16[4,256,512]{1,2,0:T(8,128)(2,1)S(1)}, u32[]{:S(2)}, u32[]{:S(2)}) async-start(bf16[4,256,512]{1,2,0:T(8,128)(2,1)} %broadcast_in_dim.6), calls=%async_computation | async-start | bytes 2097152 | tf_op jit(solution)/shard_map/all_to_all | solution.py:25
  7.3 15.0 %copy-start.7 = (bf16[2048,32]{0,1:T(8,128)(2,1)S(1)}, bf16[2048,32]{0,1:T(8,128)(2,1)}, u32[]{:S(2)}) copy-start(bf16[2048,32]{0,1:T(8,128)(2,1)} %param.22) | copy-start | bytes 393220
  29.7 8.5 %copy-start.10 = (f32[512]{0:T(512)S(1)}, f32[512]{0:T(512)}, u32[]{:S(2)}) copy-start(f32[512]{0:T(512)} %param.23) | copy-start | bytes 6148
  29.7 8.8 %copy-start.3 = (bf16[512,256]{1,0:T(8,128)(2,1)S(1)}, bf16[512,256]{1,0:T(8,128)(2,1)}, u32[]{:S(2)}) copy-start(bf16[512,256]{1,0:T(8,128)(2,1)} %param.25) | copy-start | bytes 786436
  30.4 8.6 %copy-start.26 = (f32[256]{0:T(256)S(1)}, f32[256]{0:T(256)}, u32[]{:S(2)}) copy-start(f32[256]{0:T(256)} %param.24) | copy-start | bytes 3076
  30.5 66.2 %collective-permute-start = (bf16[15,512]{1,0:T(8,128)(2,1)S(1)}, bf16[15,512]{1,0:T(8,128)(2,1)S(1)}, u32[]{:S(2)}, u32[]{:S(2)}) collective-permute-start(bf16[15,512]{1,0:T(8,128)(2,1)S(1)} %get-tuple-element.9), channel_id=1, source_target_pairs={{0,4},{4,8},{8,12},{12,16},{16,20},{20,24},{24,28},{28,32},{32,36}... | collective-permute-start | bytes 46088 | tf_op jit(solution)/shard_map/ppermute | solution.py:40
  36.3 60.4 %collective-permute-start.1 = (bf16[15,512]{1,0:T(8,128)(2,1)S(1)}, bf16[15,512]{1,0:T(8,128)(2,1)S(1)}, u32[]{:S(2)}, u32[]{:S(2)}) collective-permute-start(bf16[15,512]{1,0:T(8,128)(2,1)S(1)} %get-tuple-element.10), channel_id=1, source_target_pairs={{4,0},{8,4},{12,8},{16,12},{20,16},{24,20},{28,24},{32,28},{36,32}... | collective-permute-start | bytes 46088 | tf_op jit(solution)/shard_map/ppermute | solution.py:42
  39.9 56.9 %copy-start.11 = (f32[1,512]{1,0:T(1,128)S(1)}, f32[1,512]{1,0:T(1,128)}, u32[]{:S(2)}) copy-start(f32[1,512]{1,0:T(1,128)} %get-tuple-element.19) | copy-start | bytes 6148
  39.9 56.9 %copy-start.12 = (f32[1,512]{1,0:T(1,128)S(1)}, f32[1,512]{1,0:T(1,128)}, u32[]{:S(2)}) copy-start(f32[1,512]{1,0:T(1,128)} %get-tuple-element.20) | copy-start | bytes 6148
  39.9 56.9 %copy-start.13 = (f32[1,512]{1,0:T(1,128)S(1)}, f32[1,512]{1,0:T(1,128)}, u32[]{:S(2)}) copy-start(f32[1,512]{1,0:T(1,128)} %get-tuple-element.21) | copy-start | bytes 6148
  39.9 57.0 %copy-start.14 = (f32[1,512]{1,0:T(1,128)S(1)}, f32[1,512]{1,0:T(1,128)}, u32[]{:S(2)}) copy-start(f32[1,512]{1,0:T(1,128)} %get-tuple-element.22) | copy-start | bytes 6148
  39.9 57.0 %copy-start.15 = (f32[1,512]{1,0:T(1,128)S(1)}, f32[1,512]{1,0:T(1,128)}, u32[]{:S(2)}) copy-start(f32[1,512]{1,0:T(1,128)} %get-tuple-element.23) | copy-start | bytes 6148
  39.9 57.0 %copy-start.16 = (f32[1,512]{1,0:T(1,128)S(1)}, f32[1,512]{1,0:T(1,128)}, u32[]{:S(2)}) copy-start(f32[1,512]{1,0:T(1,128)} %get-tuple-element.24) | copy-start | bytes 6148
  39.9 57.0 %copy-start.17 = (f32[1,512]{1,0:T(1,128)S(1)}, f32[1,512]{1,0:T(1,128)}, u32[]{:S(2)}) copy-start(f32[1,512]{1,0:T(1,128)} %get-tuple-element.25) | copy-start | bytes 6148
  39.9 57.0 %copy-start.18 = (f32[1,512]{1,0:T(1,128)S(1)}, f32[1,512]{1,0:T(1,128)}, u32[]{:S(2)}) copy-start(f32[1,512]{1,0:T(1,128)} %get-tuple-element.26) | copy-start | bytes 6148
  39.9 57.0 %copy-start.19 = (f32[1,512]{1,0:T(1,128)S(1)}, f32[1,512]{1,0:T(1,128)}, u32[]{:S(2)}) copy-start(f32[1,512]{1,0:T(1,128)} %get-tuple-element.27) | copy-start | bytes 6148
  39.9 57.0 %copy-start.20 = (f32[1,512]{1,0:T(1,128)S(1)}, f32[1,512]{1,0:T(1,128)}, u32[]{:S(2)}) copy-start(f32[1,512]{1,0:T(1,128)} %get-tuple-element.28) | copy-start | bytes 6148
  40.0 57.0 %copy-start.21 = (f32[1,512]{1,0:T(1,128)S(1)}, f32[1,512]{1,0:T(1,128)}, u32[]{:S(2)}) copy-start(f32[1,512]{1,0:T(1,128)} %get-tuple-element.29) | copy-start | bytes 6148
  40.0 57.0 %copy-start.22 = (f32[1,512]{1,0:T(1,128)S(1)}, f32[1,512]{1,0:T(1,128)}, u32[]{:S(2)}) copy-start(f32[1,512]{1,0:T(1,128)} %get-tuple-element.30) | copy-start | bytes 6148
  40.0 57.0 %copy-start.23 = (f32[1,512]{1,0:T(1,128)S(1)}, f32[1,512]{1,0:T(1,128)}, u32[]{:S(2)}) copy-start(f32[1,512]{1,0:T(1,128)} %get-tuple-element.31) | copy-start | bytes 6148
  40.0 57.0 %copy-start.25 = (f32[512]{0:T(512)S(1)}, f32[512]{0:T(512)}, u32[]{:S(2)}) copy-start(f32[512]{0:T(512)} %param.32) | copy-start | bytes 6148
  100.4 7.4 %all-to-all-start.1 = ((f32[4,2,256]{2,1,0:T(2,128)}), f32[4,2,256]{2,1,0:T(2,128)S(1)}, u32[]{:S(2)}, u32[]{:S(2)}) async-start(f32[4,2,256]{2,1,0:T(2,128)} %broadcast_in_dim.8), calls=%async_computation.1 | async-start | bytes 16384 | tf_op jit(solution)/shard_map/all_to_all | solution.py:25
  (10 other events, 47.8 us)

commit v4 on v3

--- a/solution.py
+++ b/solution.py
@@ -46,18 +46,6 @@
     return cells
 
 
-def cut_along(shard, dim, peers):
-    dims = shard.shape
-    blocks = shard.reshape(*dims[:dim], peers, dims[dim] // peers, *dims[dim + 1 :])
-    return jnp.moveaxis(blocks, dim, 0)
-
-
-def sum_at_owner(shard, axis, dim):
-    blocks = cut_along(shard, dim, lax.axis_size(axis))
-    arrived = lax.all_to_all(blocks, axis, split_axis=0, concat_axis=0, tiled=True)
-    return arrived.astype(f32).sum(axis=0)
-
-
 def rms_scale(values, gain):
     return values * lax.rsqrt(jnp.mean(values * values, axis=-1, keepdims=True) + eps_norm) * gain
 
@@ -76,9 +64,10 @@
 
 
 def attend_kernel(
-    heads, scale, xp_ref, qt_ref, ku_ref, vut_ref, out_ref,
-    x, q, keys, vals, acc, high, acc_in, high_in, part_out, part_in,
+    heads, scale, xp_ref, qt_ref, ku_ref, vut_ref, wa_ref, cp_ref, out_ref,
+    x, q, keys, vals, acc, high, acc_in, high_in, part_out, stat_out, part_in, stat_in, wide, conv_in, weight_in,
     got_x, sent_x, got_q, sent_q, sent_relay, sent_pair_q, got_pair_q, pair_sem, part_sem,
+    sent_t, got_t,
 ):
     sp, tp = lax.axis_index("sp"), lax.axis_index("tp")
     core = lax.rem(sp, 2)
@@ -107,7 +96,8 @@
         )
 
     barrier = pltpu.get_barrier_semaphore()
-    peers = (up, down, right, left, across, sibling)
+    others = [(sp, lax.rem(tp + i, 4)) for i in (1, 3, 2)]
+    peers = (up, down, right, left, across, sibling, *others)
     for peer in peers:
         pl.semaphore_signal(barrier, inc=1, device_id=peer, device_id_type=pl.DeviceIdType.MESH)
     pl.semaphore_wait(barrier, len(peers))
@@ -144,6 +134,16 @@
                 got_pair_q.at[y, n], sibling,
             )
         )
+    columns = out_ref.shape[1]
+
+    def block(ref, n):
+        return ref.at[:, pl.ds(pl.multiple_of(n * columns, columns), columns)]
+
+    for i, peer in enumerate(others):
+        for kind, (src, dst) in enumerate(((wa_ref, weight_in), (cp_ref, conv_in))):
+            first.append(
+                remote(block(src, peer[1]), dst.at[tp], sent_t.at[kind, i], got_t.at[kind, tp], peer)
+            )
     for copy in first:
         copy.start()
     x[z] = xp_ref[...]
@@ -151,16 +151,14 @@
     acc[...] = jnp.zeros_like(acc)
     high[...] = jnp.full_like(high, -jnp.inf)
 
-    def x_next(k):
-        return [
-            (x_copy(k, n, up if k % 2 else down), k < 5 or (k == 5 and n == 0) or (k == 6 and n == 1))
-            for n in range(2)
-        ]
+    def goes(k, n):
+        return k < 5 or (k == 5 and n == 0) or (k == 6 and n == 1)
 
     def x_first(k):
-        for copy, goes in x_next(k):
+        for n in range(2):
+            copy = x_copy(k, n, up if k % 2 else down)
             copy.wait_recv()
-            if goes:
+            if goes(k, n):
                 copy.start()
 
     def pair_q(r, n):
@@ -204,10 +202,13 @@
             copy.start()
 
     def part_copy(r):
-        return remote(
-            part_out.at[r - 1], part_in.at[r - 1], part_sem.at[r - 1, 0], part_sem.at[r - 1, 1],
-            {1: right, 2: across, 3: left}[r],
-        )
+        return [
+            remote(
+                out.at[r - 1], into.at[r - 1], part_sem.at[r - 1, n, 0], part_sem.at[r - 1, n, 1],
+                {1: right, 2: across, 3: left}[r],
+            )
+            for n, (out, into) in enumerate(((stat_out, stat_in), (part_out, part_in)))
+        ]
 
     def merge(r):
         for copy in swap(r):
@@ -216,12 +217,12 @@
             m0, m1 = high[r, h : h + 1, :own_q], high_in[r, h : h + 1, :]
             top = jnp.maximum(m0, m1)
             a0, a1 = jnp.exp2((m0 - top) * scale), jnp.exp2((m1 - top) * scale)
-            part_out[r - 1, h, :vrows, :] = (
-                acc[r, h, :vrows, :own_q] * a0 + acc_in[r, h, :vrows, :] * a1
-            )
             total = acc[r, h, vrows : vrows + 1, :own_q] * a0 + acc_in[r, h, vrows : vrows + 1, :] * a1
-            part_out[r - 1, h, vrows:, :] = jnp.concatenate([total] * 4 + [top] * 4, axis=0)
-        part_copy(r).start()
+            whole = acc[r, h, :vrows, :own_q] * a0 + acc_in[r, h, :vrows, :] * a1
+            part_out[r - 1, h] = (whole / total).astype(bf16)
+            stat_out[r - 1, h] = jnp.concatenate([total] * 4 + [top] * 4, axis=0)
+        for copy in part_copy(r):
+            copy.start()
 
     def expand(c):
         at = [plane(2 * c), plane(2 * c + 1)]
@@ -317,38 +318,62 @@
     for copy in first:
         copy.wait_send()
     for k in range(1, 8):
-        for copy, goes in x_next(k):
-            if goes:
-                copy.wait_send()
+        for n in range(2):
+            if goes(k, n):
+                x_copy(k, n, up if k % 2 else down).wait_send()
     for n in range(2):
         relay_q(n).wait_send()
         for r in range(1, 4):
             pair_q(r, n).wait_send()
     for r in range(1, 4):
-        part_copy(r).wait()
+        for copy in part_copy(r):
+            copy.wait()
     for copy in swap(0):
         copy.wait()
     for h in range(heads):
         tops = [high[0, h : h + 1, :own_q], high_in[0, h : h + 1, :]]
-        parts = [acc[0, h, : vrows + 1, :own_q], acc_in[0, h, : vrows + 1, :]]
+        totals = [acc[0, h, vrows : vrows + 1, :own_q], acc_in[0, h, vrows : vrows + 1, :]]
         for r in range(3):
-            tops.append(part_in[r, h, vrows + 4 : vrows + 5, :])
-            parts.append(part_in[r, h, : vrows + 1, :])
+            tops.append(stat_in[r, h, 4:5, :])
+            totals.append(stat_in[r, h, 0:1, :])
         top = functools.reduce(jnp.maximum, tops)
-        whole = sum(p * jnp.exp2((m - top) * scale) for p, m in zip(parts, tops))
-        out_ref[h * vrows : (h + 1) * vrows, :] = (whole[:vrows] / whole[vrows : vrows + 1]).astype(bf16)
-
-
-def attend(xp, qt, key_up, value_up_t, size):
+        shares = [jnp.exp2((m - top) * scale) for m in tops]
+        total = sum(t * a for t, a in zip(totals, shares))
+        whole = acc[0, h, :vrows, :own_q] * shares[0] + acc_in[0, h, :vrows, :] * shares[1]
+        for r in range(3):
+            whole = whole + part_in[r, h].astype(f32) * (shares[2 + r] * totals[2 + r])
+        wide[tp, :, h * vrows : (h + 1) * vrows] = jnp.transpose(whole / total).astype(bf16)
+    last = [
+        remote(wide.at[tp], wide.at[tp], sent_t.at[2, i], got_t.at[2, tp], peer)
+        for i, peer in enumerate(others)
+    ]
+    for copy in last:
+        copy.start()
+    result = jnp.dot(wide[tp], block(wa_ref, tp)[...], preferred_element_type=f32)
+    result = result + block(cp_ref, tp)[...].astype(f32)
+    for i in (1, 3, 2):
+        source = lax.rem(tp + i, 4)
+        for kind, dst in enumerate((weight_in, conv_in, wide)):
+            at = dst.at[source]
+            remote(at, at, sent_t.at[kind, 0], got_t.at[kind, source], others[0]).wait_recv()
+        result = result + jnp.dot(wide[source], weight_in[source], preferred_element_type=f32)
+        result = result + conv_in[source].astype(f32)
+    out_ref[...] = result.astype(bf16)
+    for copy in last:
+        copy.wait_send()
+
+
+def attend(xp, qt, key_up, value_up_t, out_attend, conv_part, size):
     heads, width, own_q = qt.shape
     vdim = value_up_t.shape[0] // heads
+    columns = out_attend.shape[1] // 4
     vmem = pl.BlockSpec(memory_space=pltpu.VMEM)
     dma = pltpu.SemaphoreType.DMA
     scale = math.log2(math.e) * size ** (-0.5)
     return pl.pallas_call(
         functools.partial(attend_kernel, heads, scale),
-        out_shape=jax.ShapeDtypeStruct((heads * vdim, own_q), bf16),
-        in_specs=[vmem] * 4,
+        out_shape=jax.ShapeDtypeStruct((own_q, columns), bf16),
+        in_specs=[vmem] * 6,
         out_specs=vmem,
         scratch_shapes=[
             pltpu.VMEM((8, *xp.shape), bf16),
@@ -359,8 +384,13 @@
             pltpu.VMEM((4, heads, 2 * own_q), f32),
             pltpu.VMEM((4, heads, vdim + 16, own_q), f32),
             pltpu.VMEM((4, heads, own_q), f32),
-            pltpu.VMEM((3, heads, vdim + 8, own_q), f32),
-            pltpu.VMEM((3, heads, vdim + 8, own_q), f32),
+            pltpu.VMEM((3, heads, vdim, own_q), bf16),
+            pltpu.VMEM((3, heads, 8, own_q), f32),
+            pltpu.VMEM((3, heads, vdim, own_q), bf16),
+            pltpu.VMEM((3, heads, 8, own_q), f32),
+            pltpu.VMEM((4, own_q, heads * vdim), bf16),
+            pltpu.VMEM((4, own_q, columns), bf16),
+            pltpu.VMEM((4, heads * vdim, columns), bf16),
             dma((8, 2)),
             dma((8, 2)),
             dma((4, 2)),
@@ -369,7 +399,9 @@
             dma((4, 2)),
             dma((4, 2)),
             dma((4, 4)),
-            dma((3, 2)),
+            dma((3, 2, 2)),
+            dma((3, 3)),
+            dma((3, 4)),
         ],
         compiler_params=pltpu.CompilerParams(
             collective_id=0, has_side_effects=True, vmem_limit_bytes=56 * 2**20
@@ -380,7 +412,7 @@
             transcendentals=8192 * 2 * own_q * heads,
         ),
         name="attend",
-    )(xp, qt, key_up, value_up_t)
+    )(xp, qt, key_up, value_up_t, out_attend, conv_part)
 
 
 def per_device(
@@ -447,10 +479,6 @@
         else:
             cols += [r_heads[:, h], empty, q_heads[:, h]]
     q_own = jnp.transpose(jnp.concatenate(cols, axis=1))
-    attended = attend(
-        xp, q_own.reshape(heads, 128, row_count), key_up, jnp.transpose(value_up), nope + rope_size
-    )
-
     glu = (row_scale * value_pre * jax.nn.sigmoid(row_scale * gate_pre)).astype(bf16)
     taps = conv_taps.shape[0]
     padded = padded_2(glu, (("sp", 0),), taps // 2).astype(f32)
@@ -471,19 +499,16 @@
     activated = jax.nn.silu(
         centred * lax.rsqrt(spread[:, None] + eps_layer) * channel_gain
     ).astype(bf16)
-    summed = sum_at_owner(
-        (
-            lax.dot_general(
-                out_attend, attended, (((0,), (0,)), ((), ())), preferred_element_type=f32
-            )
-            + lax.dot_general(
-                out_conv, activated, (((0,), (1,)), ((), ())), preferred_element_type=f32
-            )
-        ).astype(bf16),
-        "tp",
-        0,
+    conv_part = jnp.dot(activated, out_conv, preferred_element_type=f32).astype(bf16)
+    return attend(
+        xp,
+        q_own.reshape(heads, 128, row_count),
+        key_up,
+        jnp.transpose(value_up),
+        out_attend,
+        conv_part,
+        nope + rope_size,
     )
-    return jnp.transpose(summed).astype(bf16)
 
 
 def solution(mesh):

time: 129 us -> 120 us (0.930)
  blocking collectives: 16.9 us -> 0 us
  Pallas kernels: 56.7 us -> 62.5 us
  matrix products: 12.6 us -> 9.57 us
  local copies, waits for them, and re-layouts: 6.92 us -> 9.77 us
  waiting for transfers between devices: 13 us -> 15.7 us
    all_to_all x1 -> x0, blocking collectives: 16.9 us -> none  [sum_at_owner(): lax.all_to_all(blocks, axis, split_axis=0, concat_axis=0, tiled=True)]
    pallas_call x1, Pallas kernels: 56.7 us -> 62.5 us  [attend(): pl.pallas_call(functools.partial(attend_kernel, heads, scale), out_shape=...]
    dot_general x2 -> x1, matrix products: 5.46 us -> 1.82 us  [per_device(): jnp.dot(activated, out_conv, preferred_element_type=f32).astype(bf16)]
    unnamed x69 -> x108, local copies, waits for them, and re-layouts: 3.89 us -> 6.21 us
    all_to_all x2, waiting for transfers between devices: 13 us -> 14.7 us  [sent_to_all(): return lax.all_to_all(copies, axis, split_axis=0, concat_axis=0, tiled=True)]
  transfers between devices with their start and end apart: 4 -> 4, of which waited for: 2 -> 3; matrix products, arithmetic and copies ran while one was open for 5% -> 3% of each run, Pallas kernels for 44% -> 0%
where the time goes in v4:
time: 120 us
  Pallas kernels  62.5 us (52%)
  starting transfers between devices  15.9 us (13%)
  waiting for transfers between devices  15.7 us (13%)
  local copies, waits for them, and re-layouts  9.77 us (8%)
  matrix products  9.57 us (8%)
  other arithmetic  5.25 us (4%)
    pallas_call x1, Pallas kernels, attend(): pl.pallas_call(functools.partial(attend_kernel, heads, scale), out_shape=...  62.5 us
    all_to_all x2, waiting for transfers between devices, sent_to_all(): return lax.all_to_all(copies, axis, split_axis=0, concat_axis=0, tiled=True)  14.7 us
    all_to_all x2, starting transfers between devices, sent_to_all(): return lax.all_to_all(copies, axis, split_axis=0, concat_axis=0, tiled=True)  8.2 us
    dot_general x5, matrix products, add_rows(): return jnp.dot(scaled, weight, preferred_element_type=f32)  7.11 us
    unnamed x108, local copies, waits for them, and re-layouts  6.21 us
    ppermute x1, starting transfers between devices, padded_2(): lax.ppermute(tail, axis, [(i, (i + 1) % count) for i in range(ends)])  5.8 us
    reduce_sum x1, other arithmetic, per_device(): own_mean = jnp.mean(conv, axis=-1)  2.57 us
  transfers between devices with their start and end apart: 4, of which 3 were waited for; matrix products, arithmetic and copies ran while one was open for 3% of the time, Pallas kernels for 0%

profile of v4, /device:TPU:1, one launch (start us, length us, event | category | flops | bytes accessed | tf_op | source)
XLA Modules:
  0.0 119.7 jit_solution(11078689116548608114)
XLA Ops:
  0.0 1.2 %copy.30 = bf16[256,512]{0,1:T(8,128)(2,1)S(1)} copy(bf16[256,512]{1,0:T(8,128)(2,1)} %param.18) | data formatting | bytes 524288 | tf_op args[0]
  1.2 1.0 broadcast_in_dim.6
  2.3 5.0 %all-to-all-start = ((bf16[4,256,512]{1,2,0:T(8,128)(2,1)}), bf16[4,256,512]{1,2,0:T(8,128)(2,1)S(1)}, u32[]{:S(2)}, u32[]{:S(2)}) async-start(bf16[4,256,512]{1,2,0:T(8,128)(2,1)} %broadcast_in_dim.6), calls=%async_computation | async-start | bytes 2097152 | tf_op jit(solution)/shard_map/all_to_all | solution.py:25
  7.3 0.8 copy.33
  8.1 0.6 fusion.61
  8.7 0.7 fusion.60
  9.4 11.2 %all-to-all-done = bf16[4,256,512]{1,2,0:T(8,128)(2,1)S(1)} async-done(((bf16[4,256,512]{1,2,0:T(8,128)(2,1)}), bf16[4,256,512]{1,2,0:T(8,128)(2,1)S(1)}, u32[]{:S(2)}, u32[]{:S(2)}) %all-to-all-start) | async-done | bytes 1048608 | tf_op jit(solution)/shard_map/all_to_all | solution.py:25
  21.3 1.0 copy-done.1
  22.5 0.8 multiply_cosine_fusion
  23.8 2.1 %multiply_reduce_fusion.3 = (f32[256]{0:T(256)S(1)}, f32[256,256]{1,0:T(8,128)S(1)}) fusion(bf16[256,2048]{0,1:T(8,128)(2,1)} %copy-done.1, bf16[2048,256]{1,0:T(8,128)(2,1)} %param.21, f32[256]{0:T(256)S(1)} %add_rsqrt_fusion.3), kind=kOutput, calls=%fused_computation.88 | convolution fusion | flops 268631808 | bytes 2361344 | tf_op jit(solution)/shard_map/dot_general | solution.py:446
  25.9 2.5 %fusion.4 = f32[256,512]{1,0:T(8,128)S(1)} fusion(bf16[256,2048]{0,1:T(8,128)(2,1)S(1)} %copy-done.2, bf16[2048,512]{1,0:T(8,128)(2,1)} %param.30, f32[256]{0:T(256)S(1)} %add_rsqrt_fusion.3), kind=kOutput, calls=%fused_computation.8 | convolution fusion | flops 537395200 | bytes 3671040 | tf_op jit(solution)/shard_map/dot_general | solution.py:446
  28.5 0.8 multiply_reduce_fusion.2
  29.3 0.8 copy-done.47
  30.1 1.4 %fusion.6 = bf16[256,512]{1,0:T(8,128)(2,1)S(1)} fusion(f32[256,512]{1,0:T(8,128)S(1)} %fusion.4, bf16[256,2048]{0,1:T(8,128)(2,1)S(1)} %copy-done.2, bf16[2048,512]{1,0:T(8,128)(2,1)S(1)} %copy-done.47, f32[256]{0:T(256)} %copy-done.9), kind=kOutput, calls=%fused_computation.12 | convolution fusion | flops 537264128 | bytes 3933184 | tf_op jit(solution)/shard_map/dot_general | solution.py:446
  31.5 5.8 %collective-permute-start = (bf16[15,512]{1,0:T(8,128)(2,1)S(1)}, bf16[15,512]{1,0:T(8,128)(2,1)S(1)}, u32[]{:S(2)}, u32[]{:S(2)}) collective-permute-start(bf16[15,512]{1,0:T(8,128)(2,1)S(1)} %get-tuple-element.9), channel_id=1, source_target_pairs={{0,4},{4,8},{8,12},{12,16},{16,20},{20,24},{24,28},{28,32},{32,36}... | collective-permute-start | bytes 46088 | tf_op jit(solution)/shard_map/ppermute | solution.py:40
  37.3 1.9 %collective-permute-start.1 = (bf16[15,512]{1,0:T(8,128)(2,1)S(1)}, bf16[15,512]{1,0:T(8,128)(2,1)S(1)}, u32[]{:S(2)}, u32[]{:S(2)}) collective-permute-start(bf16[15,512]{1,0:T(8,128)(2,1)S(1)} %get-tuple-element.10), channel_id=1, source_target_pairs={{4,0},{8,4},{12,8},{16,12},{20,16},{24,20},{28,24},{32,28},{36,32}... | collective-permute-start | bytes 46088 | tf_op jit(solution)/shard_map/ppermute | solution.py:42
  41.4 1.0 collective-permute-done.1
  42.8 2.6 %fusion.57 = (f32[256]{0:T(256)S(1)}, f32[256,512]{1,0:T(8,128)S(1)}) fusion(f32[286,512]{1,0:T(8,128)S(1)} %maximum_convert_fusion, f32[512]{0:T(512)S(1)} %bitcast.123, f32[512]{0:T(512)S(1)} %bitcast.124, f32[512]{0:T(512)S(1)} %bitcast.126, f32[512]{0:T(512)S(1)} %bitcast.127, f32[512]{0:T(512)S(1)} %bitcast.128, f32[512]{0:T(512)S(1)} %bitcast.129, ...), kind=kLoop, calls=%fused_computation.143 | loop fusion | flops 8257280 | bytes 16843776 | tf_op jit(solution)/shard_map/reduce_sum | solution.py:490
  46.2 3.2 %all-to-all-start.1 = ((f32[4,2,256]{2,1,0:T(2,128)}), f32[4,2,256]{2,1,0:T(2,128)S(1)}, u32[]{:S(2)}, u32[]{:S(2)}) async-start(f32[4,2,256]{2,1,0:T(2,128)} %broadcast_in_dim.8), calls=%async_computation.1 | async-start | bytes 16384 | tf_op jit(solution)/shard_map/all_to_all | solution.py:25
  49.5 0.7 pad_maximum_fusion.xp_ref
  50.1 3.5 %all-to-all-done.1 = f32[4,2,256]{2,1,0:T(2,128)S(1)} async-done(((f32[4,2,256]{2,1,0:T(2,128)}), f32[4,2,256]{2,1,0:T(2,128)S(1)}, u32[]{:S(2)}, u32[]{:S(2)}) %all-to-all-start.1) | async-done | bytes 8224 | tf_op jit(solution)/shard_map/all_to_all | solution.py:25
  53.7 1.8 %convolution_convert_fusion.cp_ref = bf16[256,2048]{1,0:T(8,128)(2,1)} fusion(bf16[512,2048]{1,0:T(8,128)(2,1)S(1)} %copy-done, f32[256,512]{1,0:T(8,128)S(1)} %get-tuple-element.8, f32[512]{0:T(512)S(1)} %copy-done.48, f32[256]{0:T(256)S(1)} %add_rsqrt_fusion, f32[256]{0:T(256)S(1)} %broadcast_multiply_fusion), kind=kOutput, calls=%fused_computation | convolution fusion | flops 538443776 | bytes 3674112 | tf_op jit(solution)/shard_map/dot_general | solution.py:502
  55.5 62.5 %attend.1 = bf16[256,512]{1,0:T(8,128)(2,1)} custom-call(bf16[2,144,256]{2,1,0:T(8,128)(2,1)} %pad_maximum_fusion.xp_ref, bf16[4,128,256]{2,1,0:T(8,128)(2,1)} %bitcast.145, bf16[256,256]{1,0:T(8,128)(2,1)} %ku_ref.1, bf16[256,256]{1,0:T(8,128)(2,1)} %bitcast.111, bf16[256,2048]{1,0:T(8,128)(2,1)} %wa_ref.1, bf16[256,2048]{1,0:T(8,128)(2,1)} %convolution_convert_fusion.cp_ref), custom_call_target="tpu_custom_call" | custom-call | flops 10737418240 | bytes 2000000 | tf_op jit(solution)/shard_map/attend/pallas_call | solution.py:373
  118.0 1.7 %copy.52 = bf16[256,512]{1,0:T(8,128)(2,1)} copy(bf16[256,512]{1,0:T(8,128)(2,1)} %attend.1) | data formatting | bytes 524288
  (137 shorter events, 4.2 us)
Async XLA Ops:
  0.0 53.7 %copy-start = (bf16[512,2048]{1,0:T(8,128)(2,1)S(1)}, bf16[512,2048]{1,0:T(8,128)(2,1)}, u32[]{:S(2)}) copy-start(bf16[512,2048]{1,0:T(8,128)(2,1)} %param.35) | copy-start | bytes 6291460
  0.0 7.3 %copy-start.4 = (bf16[256,256]{1,0:T(8,128)(2,1)S(1)}, bf16[256,256]{1,0:T(8,128)(2,1)}, u32[]{:S(2)}) copy-start(bf16[256,256]{1,0:T(8,128)(2,1)} %param.28) | copy-start | bytes 393220
  0.0 8.0 %copy-start.8 = (f32[31,512]{1,0:T(8,128)S(1)}, f32[31,512]{1,0:T(8,128)}, u32[]{:S(2)}) copy-start(f32[31,512]{1,0:T(8,128)} %param.31) | copy-start | bytes 190468
  2.3 18.6 %copy-start.10 = (f32[2048]{0:T(1024)S(1)}, f32[2048]{0:T(1024)}, u32[]{:S(2)}) copy-start(f32[2048]{0:T(1024)} %param.19) | copy-start | bytes 24580
  2.3 18.3 %all-to-all-start = ((bf16[4,256,512]{1,2,0:T(8,128)(2,1)}), bf16[4,256,512]{1,2,0:T(8,128)(2,1)S(1)}, u32[]{:S(2)}, u32[]{:S(2)}) async-start(bf16[4,256,512]{1,2,0:T(8,128)(2,1)} %broadcast_in_dim.6), calls=%async_computation | async-start | bytes 2097152 | tf_op jit(solution)/shard_map/all_to_all | solution.py:25
  7.3 15.0 %copy-start.6 = (bf16[2048,32]{0,1:T(8,128)(2,1)S(1)}, bf16[2048,32]{0,1:T(8,128)(2,1)}, u32[]{:S(2)}) copy-start(bf16[2048,32]{0,1:T(8,128)(2,1)} %param.22) | copy-start | bytes 393220
  20.9 7.6 %copy-start.9 = (f32[256]{0:T(256)}, f32[256]{0:T(256)S(1)}, u32[]{:S(2)}) copy-start(f32[256]{0:T(256)S(1)} %add_rsqrt_fusion.3) | copy-start | bytes 3076
  22.5 3.4 %copy-start.2 = (bf16[256,2048]{0,1:T(8,128)(2,1)S(1)}, bf16[256,2048]{0,1:T(8,128)(2,1)}, u32[]{:S(2)}) copy-start(bf16[256,2048]{0,1:T(8,128)(2,1)} %copy-done.1) | copy-start | bytes 3145732
  30.1 9.2 %copy-start.5 = (bf16[512,128]{1,0:T(8,128)(2,1)S(1)}, bf16[512,128]{1,0:T(8,128)(2,1)}, u32[]{:S(2)}) copy-start(bf16[512,128]{1,0:T(8,128)(2,1)} %param.26) | copy-start | bytes 393220
  30.1 9.2 %copy-start.11 = (f32[512]{0:T(512)S(1)}, f32[512]{0:T(512)}, u32[]{:S(2)}) copy-start(f32[512]{0:T(512)} %param.23) | copy-start | bytes 6148
  30.1 9.8 %copy-start.3 = (bf16[512,256]{1,0:T(8,128)(2,1)S(1)}, bf16[512,256]{1,0:T(8,128)(2,1)}, u32[]{:S(2)}) copy-start(bf16[512,256]{1,0:T(8,128)(2,1)} %param.25) | copy-start | bytes 786436
  30.1 10.2 %copy-start.7 = (f32[256,16]{0,1:T(8,128)S(1)}, f32[256,16]{0,1:T(8,128)}, u32[]{:S(2)}) copy-start(f32[256,16]{0,1:T(8,128)} %get-tuple-element.48) | copy-start | bytes 49156
  31.5 9.0 %copy-start.45 = (f32[256]{0:T(256)S(1)}, f32[256]{0:T(256)}, u32[]{:S(2)}) copy-start(f32[256]{0:T(256)} %param.24) | copy-start | bytes 3076
  31.5 9.8 %collective-permute-start = (bf16[15,512]{1,0:T(8,128)(2,1)S(1)}, bf16[15,512]{1,0:T(8,128)(2,1)S(1)}, u32[]{:S(2)}, u32[]{:S(2)}) collective-permute-start(bf16[15,512]{1,0:T(8,128)(2,1)S(1)} %get-tuple-element.9), channel_id=1, source_target_pairs={{0,4},{4,8},{8,12},{12,16},{16,20},{20,24},{24,28},{28,32},{32,36}... | collective-permute-start | bytes 46088 | tf_op jit(solution)/shard_map/ppermute | solution.py:40
  37.3 5.1 %collective-permute-start.1 = (bf16[15,512]{1,0:T(8,128)(2,1)S(1)}, bf16[15,512]{1,0:T(8,128)(2,1)S(1)}, u32[]{:S(2)}, u32[]{:S(2)}) collective-permute-start(bf16[15,512]{1,0:T(8,128)(2,1)S(1)} %get-tuple-element.10), channel_id=1, source_target_pairs={{4,0},{8,4},{12,8},{16,12},{20,16},{24,20},{28,24},{32,28},{36,32}... | collective-permute-start | bytes 46088 | tf_op jit(solution)/shard_map/ppermute | solution.py:42
  39.3 3.2 %copy-start.12 = (f32[1,512]{1,0:T(1,128)S(1)}, f32[1,512]{1,0:T(1,128)}, u32[]{:S(2)}) copy-start(f32[1,512]{1,0:T(1,128)} %get-tuple-element.32) | copy-start | bytes 6148
  39.3 3.2 %copy-start.13 = (f32[1,512]{1,0:T(1,128)S(1)}, f32[1,512]{1,0:T(1,128)}, u32[]{:S(2)}) copy-start(f32[1,512]{1,0:T(1,128)} %get-tuple-element.33) | copy-start | bytes 6148
  39.3 3.2 %copy-start.14 = (f32[1,512]{1,0:T(1,128)S(1)}, f32[1,512]{1,0:T(1,128)}, u32[]{:S(2)}) copy-start(f32[1,512]{1,0:T(1,128)} %get-tuple-element.34) | copy-start | bytes 6148
  39.3 3.2 %copy-start.15 = (f32[1,512]{1,0:T(1,128)S(1)}, f32[1,512]{1,0:T(1,128)}, u32[]{:S(2)}) copy-start(f32[1,512]{1,0:T(1,128)} %get-tuple-element.35) | copy-start | bytes 6148
  39.3 3.2 %copy-start.16 = (f32[1,512]{1,0:T(1,128)S(1)}, f32[1,512]{1,0:T(1,128)}, u32[]{:S(2)}) copy-start(f32[1,512]{1,0:T(1,128)} %get-tuple-element.36) | copy-start | bytes 6148
  39.3 3.2 %copy-start.17 = (f32[1,512]{1,0:T(1,128)S(1)}, f32[1,512]{1,0:T(1,128)}, u32[]{:S(2)}) copy-start(f32[1,512]{1,0:T(1,128)} %get-tuple-element.37) | copy-start | bytes 6148
  39.3 3.2 %copy-start.18 = (f32[1,512]{1,0:T(1,128)S(1)}, f32[1,512]{1,0:T(1,128)}, u32[]{:S(2)}) copy-start(f32[1,512]{1,0:T(1,128)} %get-tuple-element.38) | copy-start | bytes 6148
  42.8 10.9 %copy-start.48 = (f32[512]{0:T(512)S(1)}, f32[512]{0:T(512)}, u32[]{:S(2)}) copy-start(f32[512]{0:T(512)} %param.33) | copy-start | bytes 6148
  46.2 7.4 %all-to-all-start.1 = ((f32[4,2,256]{2,1,0:T(2,128)}), f32[4,2,256]{2,1,0:T(2,128)S(1)}, u32[]{:S(2)}, u32[]{:S(2)}) async-start(f32[4,2,256]{2,1,0:T(2,128)} %broadcast_in_dim.8), calls=%async_computation.1 | async-start | bytes 16384 | tf_op jit(solution)/shard_map/all_to_all | solution.py:25
  (29 other events, 85.8 us)

commit v5 on v4

--- a/solution.py
+++ b/solution.py
@@ -27,23 +27,6 @@
 
 def gather_directly(shard, axis, dim):
     return laid_out(sent_to_all(shard, axis), dim)
-
-
-def padded_2(cells, sides, width):
-    for axis, dim in sides:
-        count = lax.axis_size(axis)
-        ends = count - 1
-        head = lax.slice_in_dim(cells, 0, width, axis=dim)
-        tail = lax.slice_in_dim(cells, cells.shape[dim] - width, cells.shape[dim], axis=dim)
-        cells = jnp.concatenate(
-            [
-                lax.ppermute(tail, axis, [(i, (i + 1) % count) for i in range(ends)]),
-                cells,
-                lax.ppermute(head, axis, [((i + 1) % count, i) for i in range(ends)]),
-            ],
-            axis=dim,
-        )
-    return cells
 
 
 def rms_scale(values, gain):
@@ -64,10 +47,12 @@
 
 
 def attend_kernel(
-    heads, scale, xp_ref, qt_ref, ku_ref, vut_ref, wa_ref, cp_ref, out_ref,
+    heads, scale, xp_ref, qt_ref, ku_ref, vut_ref, wa_ref, glu_ref,
+    taps_ref, bias_ref, gain_ref, oc_ref, out_ref,
     x, q, keys, vals, acc, high, acc_in, high_in, part_out, stat_out, part_in, stat_in, wide, conv_in, weight_in,
+    halo, padded, shifted, conv, moments, active, cp_ref,
     got_x, sent_x, got_q, sent_q, sent_relay, sent_pair_q, got_pair_q, pair_sem, part_sem,
-    sent_t, got_t,
+    sent_t, got_t, halo_sem, sent_m, got_m,
 ):
     sp, tp = lax.axis_index("sp"), lax.axis_index("tp")
     core = lax.rem(sp, 2)
@@ -97,7 +82,9 @@
 
     barrier = pltpu.get_barrier_semaphore()
     others = [(sp, lax.rem(tp + i, 4)) for i in (1, 3, 2)]
-    peers = (up, down, right, left, across, sibling, *others)
+    count = 64
+    beside = [(lax.rem(sp + 1, count), tp), (lax.rem(sp + count - 1, count), tp)]
+    peers = (up, down, right, left, across, sibling, *others, *beside)
     for peer in peers:
         pl.semaphore_signal(barrier, inc=1, device_id=peer, device_id_type=pl.DeviceIdType.MESH)
     pl.semaphore_wait(barrier, len(peers))
@@ -139,11 +126,18 @@
     def block(ref, n):
         return ref.at[:, pl.ds(pl.multiple_of(n * columns, columns), columns)]
 
-    for i, peer in enumerate(others):
-        for kind, (src, dst) in enumerate(((wa_ref, weight_in), (cp_ref, conv_in))):
-            first.append(
-                remote(block(src, peer[1]), dst.at[tp], sent_t.at[kind, i], got_t.at[kind, tp], peer)
-            )
+    def block_copy(kind, i, src, dst):
+        peer = others[i]
+        return remote(block(src, peer[1]), dst.at[tp], sent_t.at[kind, i], got_t.at[kind, tp], peer)
+
+    halos = [
+        remote(
+            glu_ref.at[own_q - 16 :] if n == 0 else glu_ref.at[:16],
+            halo.at[n], halo_sem.at[n, 0], halo_sem.at[n, 1], beside[n],
+        )
+        for n in range(2)
+    ]
+    first = halos + first + [block_copy(0, i, wa_ref, weight_in) for i in range(3)]
     for copy in first:
         copy.start()
     x[z] = xp_ref[...]
@@ -269,54 +263,113 @@
             high[r, h : h + 1, :] = new
             acc[r, h] = acc[r, h] * alpha + jnp.dot(vals[c, h], p, preferred_element_type=f32)
 
+    channels = glu_ref.shape[1]
+
+    def convolve():
+        for copy in halos:
+            copy.wait_recv()
+        padded[16 : 16 + own_q, :] = glu_ref[...].astype(f32)
+        padded[:16, :] = jnp.where(sp > 0, halo[0].astype(f32), 0.0)
+        padded[16 + own_q :, :] = jnp.where(sp < count - 1, halo[1].astype(f32), 0.0)
+        taps = taps_ref.shape[0]
+        for at in range(0, channels, 128):
+            lanes = slice(at, at + 128)
+            total = jnp.broadcast_to(bias_ref[:, lanes], (own_q, 128))
+            for r in range(8):
+                part = None
+                for j in range(4):
+                    k = 8 * j + r - 1
+                    if 0 <= k < taps:
+                        term = taps_ref[k : k + 1, lanes] * padded[8 * j : 8 * j + own_q + 8, lanes]
+                        part = term if part is None else part + term
+                shifted[...] = part
+                total = total + shifted[r : r + own_q, :]
+            conv[:, lanes] = total
+        whole = conv[...]
+        mean = jnp.sum(whole, axis=1, keepdims=True) / channels
+        off = whole - mean
+        spread = jnp.sum(off * off, axis=1, keepdims=True)
+        lane = lax.broadcasted_iota(jnp.int32, (own_q, 128), 1)
+        moments[tp] = jnp.transpose(jnp.where(lane == 0, mean, spread))[:8]
+
+    def moment_copy(i):
+        at = moments.at[tp]
+        return remote(at, at, sent_m.at[i], got_m.at[tp], others[i])
+
+    def activate():
+        for i in range(1, 4):
+            source = lax.rem(tp + i, 4)
+            at = moments.at[source]
+            remote(at, at, sent_m.at[0], got_m.at[source], others[0]).wait_recv()
+        means = [moments[n, 0:1, :] for n in range(4)]
+        mean = sum(means) / 4
+        apart = sum((m - mean) * (m - mean) for m in means)
+        spread = (sum(moments[n, 1:2, :] for n in range(4)) + channels * apart) / (4 * channels)
+        tall = lambda row: jnp.transpose(jnp.broadcast_to(row, (128, own_q)))
+        mean, scaling = tall(mean), tall(lax.rsqrt(spread + eps_layer))
+        for at in range(0, channels, 128):
+            lanes = slice(at, at + 128)
+            value = (conv[:, lanes] - mean) * scaling * gain_ref[:, lanes]
+            active[:, lanes] = jax.nn.silu(value).astype(bf16)
+        for n in range(4):
+            cols = slice(n * columns, (n + 1) * columns)
+            cp_ref[:, cols] = jnp.dot(
+                active[...], oc_ref[:, cols], preferred_element_type=f32
+            ).astype(bf16)
+
+    convolve()
     x_first(1)
     x_first(2)
+    for i in range(3):
+        moment_copy(i).start()
     expand(0)
+    q_from(1, (1, 0))
+    q_from(3, (0, 1))
+    activate()
+    x_first(3)
+    x_first(4)
+    for i in range(3):
+        block_copy(1, i, cp_ref, conv_in).start()
     pair_arrived(0)
 
-    def before(step):
-        if step == 1:
-            x_first(3)
-            x_first(4)
-            q_from(1, (1, 0))
-            q_from(3, (0, 1))
-            pair_arrived(1)
-        if step == 2:
-            expand(1)
-        if step == 3:
-            x_first(5)
-            x_first(6)
-            expand(2)
-        if step == 4:
-            x_first(7)
-            q_from(2, (0, 1))
-            expand(3)
-        if step == 5:
-            pair_arrived(2)
-            swap_start(1)
-        if step == 6:
-            merge(1)
-        if step == 9:
-            pair_arrived(3)
-            swap_start(2)
-        if step == 10:
-            merge(2)
-        if step == 13:
-            swap_start(3)
-        if step == 14:
-            merge(3)
+    blocks = (0, 1, 3, 1, 3, 1, 1, 2, 2, 2, 2, 3, 3, 0, 0, 0)
+    chunks = (0, 0, 0, 1, 1, 2, 3, 0, 1, 2, 3, 2, 3, 1, 2, 3)
+
+    def looked_up(step, values):
+        found = values[0]
+        for n in range(1, 16):
+            if values[n] != values[n - 1]:
+                found = found + (values[n] - values[n - 1]) * ((step + 16 - n) // 16)
+        return found
+
+    hooks = {
+        1: lambda: pair_arrived(1),
+        2: lambda: pair_arrived(3),
+        3: lambda: (x_first(5), x_first(6), q_from(2, (0, 1)), expand(1)),
+        5: lambda: (x_first(7), expand(2)),
+        6: lambda: expand(3),
+        7: lambda: (pair_arrived(2), swap_start(1)),
+        8: lambda: merge(1),
+        11: lambda: swap_start(2),
+        12: lambda: merge(2),
+        13: lambda: swap_start(3),
+        14: lambda: merge(3),
+    }
 
     @pl.loop(0, 16)
     def _(step):
-        for s in (1, 2, 3, 4, 5, 6, 9, 10, 13, 14):
-            pl.when(step == s)(functools.partial(before, s))
-        r = lax.rem((step + 3) // 4, 4)
-        c = lax.rem(step + 3, 4) + (step + 3) // 16 - 3 * (1 - (step + 15) // 16)
-        compute(r, c)
+        for n, hook in hooks.items():
+            def run(hook=hook):
+                hook()
+            pl.when(step == n)(run)
+        compute(looked_up(step, blocks), looked_up(step, chunks))
 
     swap_start(0)
     for copy in first:
         copy.wait_send()
+    for i in range(3):
+        moment_copy(i).wait_send()
+        block_copy(1, i, cp_ref, conv_in).wait_send()
     for k in range(1, 8):
         for n in range(2):
             if goes(k, n):
@@ -363,17 +416,18 @@
         copy.wait_send()
 
 
-def attend(xp, qt, key_up, value_up_t, out_attend, conv_part, size):
+def attend(xp, qt, key_up, value_up_t, out_attend, glu, taps, bias, gain, out_conv, size):
     heads, width, own_q = qt.shape
     vdim = value_up_t.shape[0] // heads
     columns = out_attend.shape[1] // 4
+    channels = glu.shape[1]
     vmem = pl.BlockSpec(memory_space=pltpu.VMEM)
     dma = pltpu.SemaphoreType.DMA
     scale = math.log2(math.e) * size ** (-0.5)
     return pl.pallas_call(
         functools.partial(attend_kernel, heads, scale),
         out_shape=jax.ShapeDtypeStruct((own_q, columns), bf16),
-        in_specs=[vmem] * 6,
+        in_specs=[vmem] * 10,
         out_specs=vmem,
         scratch_shapes=[
             pltpu.VMEM((8, *xp.shape), bf16),
@@ -391,6 +445,13 @@
             pltpu.VMEM((4, own_q, heads * vdim), bf16),
             pltpu.VMEM((4, own_q, columns), bf16),
             pltpu.VMEM((4, heads * vdim, columns), bf16),
+            pltpu.VMEM((2, 16, channels), bf16),
+            pltpu.VMEM((own_q + 32, channels), f32),
+            pltpu.VMEM((own_q + 8, 128), f32),
+            pltpu.VMEM((own_q, channels), f32),
+            pltpu.VMEM((4, 8, own_q), f32),
+            pltpu.VMEM((own_q, channels), bf16),
+            pltpu.VMEM((own_q, 4 * columns), bf16),
             dma((8, 2)),
             dma((8, 2)),
             dma((4, 2)),
@@ -402,6 +463,9 @@
             dma((3, 2, 2)),
             dma((3, 3)),
             dma((3, 4)),
+            dma((2, 2)),
+            dma((3,)),
+            dma((4,)),
         ],
         compiler_params=pltpu.CompilerParams(
             collective_id=0, has_side_effects=True, vmem_limit_bytes=56 * 2**20
@@ -412,7 +476,7 @@
             transcendentals=8192 * 2 * own_q * heads,
         ),
         name="attend",
-    )(xp, qt, key_up, value_up_t, out_attend, conv_part)
+    )(xp, qt, key_up, value_up_t, out_attend, glu, taps, bias[None], gain[None], out_conv)
 
 
 def per_device(
@@ -437,7 +501,6 @@
 ):
     row_count = tokens.shape[0]
     width = in_gain.shape[0]
-    local_ch = conv_value.shape[1]
     positions = (lax.axis_index("sp") * row_count + jnp.arange(row_count)).astype(f32)
     piece_f = gather_directly(tokens, "tp", 1).astype(f32)
     scaled = (piece_f * in_gain).astype(bf16)
@@ -480,33 +543,17 @@
             cols += [r_heads[:, h], empty, q_heads[:, h]]
     q_own = jnp.transpose(jnp.concatenate(cols, axis=1))
     glu = (row_scale * value_pre * jax.nn.sigmoid(row_scale * gate_pre)).astype(bf16)
-    taps = conv_taps.shape[0]
-    padded = padded_2(glu, (("sp", 0),), taps // 2).astype(f32)
-    conv = jnp.zeros((row_count, local_ch), f32) + conv_bias
-    for tap in range(taps):
-        conv = conv + conv_taps[tap] * padded[tap : tap + row_count]
-    peers = lax.axis_size("tp")
-    channels = local_ch * peers
-    own_mean = jnp.mean(conv, axis=-1)
-    off = conv - own_mean[:, None]
-    own_spread = jnp.sum(off * off, axis=-1)
-    sums = sent_to_all(jnp.stack([own_mean, own_spread]), "tp")
-    means = sums[:, 0]
-    mean = jnp.mean(means, axis=0)
-    apart = means - mean
-    spread = (jnp.sum(sums[:, 1], axis=0) + local_ch * jnp.sum(apart * apart, axis=0)) / channels
-    centred = conv - mean[:, None]
-    activated = jax.nn.silu(
-        centred * lax.rsqrt(spread[:, None] + eps_layer) * channel_gain
-    ).astype(bf16)
-    conv_part = jnp.dot(activated, out_conv, preferred_element_type=f32).astype(bf16)
     return attend(
         xp,
         q_own.reshape(heads, 128, row_count),
         key_up,
         jnp.transpose(value_up),
         out_attend,
-        conv_part,
+        glu,
+        conv_taps,
+        conv_bias,
+        channel_gain,
+        out_conv,
         nope + rope_size,
     )
 

time: 120 us -> 99.8 us (0.83)
  starting transfers between devices: 15.9 us -> 4.83 us
  Pallas kernels: 62.5 us -> 66.8 us
  local copies, waits for them, and re-layouts: 9.77 us -> 6.07 us
  matrix products: 9.57 us -> 5.89 us
  waiting for transfers between devices: 15.7 us -> 12.6 us
  other arithmetic: 5.25 us -> 2.94 us
    ppermute x2 -> x0, starting transfers between devices: 7.72 us -> none  [the longest x1 5.8 us: padded_2(): lax.ppermute(tail, axis, [(i, (i + 1) % count) for i in range(ends)])]
    pallas_call x1, Pallas kernels: 62.5 us -> 66.8 us  [attend(): pl.pallas_call(functools.partial(attend_kernel, heads, scale), out_shape=...]
    all_to_all x2 -> x1, starting transfers between devices: 8.2 us -> 4.83 us  [sent_to_all(): return lax.all_to_all(copies, axis, split_axis=0, concat_axis=0, tiled=True)]
    reduce_sum x4 -> x0, other arithmetic: 2.82 us -> none  [the longest x1 2.57 us: per_device(): own_mean = jnp.mean(conv, axis=-1)]
    all_to_all x2 -> x1, waiting for transfers between devices: 14.7 us -> 12.6 us  [sent_to_all(): return lax.all_to_all(copies, axis, split_axis=0, concat_axis=0, tiled=True)]
    dot_general x5, matrix products: 7.11 us -> 5.25 us  [add_rows(): return jnp.dot(scaled, weight, preferred_element_type=f32)]
    dot_general x1 -> x0, matrix products: 1.82 us -> none  [per_device(): jnp.dot(activated, out_conv, preferred_element_type=f32).astype(bf16)]
    unnamed x108 -> x34, local copies, waits for them, and re-layouts: 6.21 us -> 4.44 us
  transfers between devices with their start and end apart: 4 -> 1, of which waited for: 3 -> 1; matrix products, arithmetic and copies ran while one was open for 3% -> 1% of each run, Pallas kernels for 0% -> 0%
where the time goes in v5:
time: 99.8 us; the launch traced here: 99.4 us
  Pallas kernels  66.8 us (67%)
  waiting for transfers between devices  12.6 us (13%)
  local copies, waits for them, and re-layouts  6.07 us (6%)
  matrix products  5.89 us (6%)
  starting transfers between devices  4.83 us (5%)
  other arithmetic  2.94 us (3%)
    pallas_call x1, Pallas kernels, attend(): pl.pallas_call(functools.partial(attend_kernel, heads, scale), out_shape=...  66.8 us
    all_to_all x1, waiting for transfers between devices, sent_to_all(): return lax.all_to_all(copies, axis, split_axis=0, concat_axis=0, tiled=True)  12.6 us
    dot_general x5, matrix products, add_rows(): return jnp.dot(scaled, weight, preferred_element_type=f32)  5.25 us
    all_to_all x1, starting transfers between devices, sent_to_all(): return lax.all_to_all(copies, axis, split_axis=0, concat_axis=0, tiled=True)  4.83 us
    unnamed x34, local copies, waits for them, and re-layouts  4.44 us
  transfers between devices with their start and end apart: 1, of which 1 were waited for; matrix products, arithmetic and copies ran while one was open for 1% of the time, Pallas kernels for 0%

profile of v5, /device:TPU:1, one launch (start us, length us, event | category | flops | bytes accessed | tf_op | source)
XLA Modules:
  0.0 99.4 jit_solution(849502145831973121)
XLA Ops:
  0.0 1.2 %copy.22 = bf16[256,512]{0,1:T(8,128)(2,1)S(1)} copy(bf16[256,512]{1,0:T(8,128)(2,1)} %param.18) | data formatting | bytes 524288 | tf_op args[0]
  1.3 1.0 %broadcast_in_dim.8 = bf16[4,256,512]{1,2,0:T(8,128)(2,1)} broadcast(bf16[256,512]{0,1:T(8,128)(2,1)S(1)} %copy.22), dimensions={1,2} | broadcast | bytes 1310720 | tf_op jit(solution)/shard_map/broadcast_in_dim | solution.py:24
  2.3 4.8 %all-to-all-start = ((bf16[4,256,512]{1,2,0:T(8,128)(2,1)}), bf16[4,256,512]{1,2,0:T(8,128)(2,1)S(1)}, u32[]{:S(2)}, u32[]{:S(2)}) async-start(bf16[4,256,512]{1,2,0:T(8,128)(2,1)} %broadcast_in_dim.8), calls=%async_computation | async-start | bytes 2097152 | tf_op jit(solution)/shard_map/all_to_all | solution.py:25
  7.1 0.8 copy.25
  7.9 12.6 %all-to-all-done = bf16[4,256,512]{1,2,0:T(8,128)(2,1)S(1)} async-done(((bf16[4,256,512]{1,2,0:T(8,128)(2,1)}), bf16[4,256,512]{1,2,0:T(8,128)(2,1)S(1)}, u32[]{:S(2)}, u32[]{:S(2)}) %all-to-all-start) | async-done | bytes 1048608 | tf_op jit(solution)/shard_map/all_to_all | solution.py:25
  20.5 0.3 multiply_reduce_fusion
  20.8 0.7 copy-done.1
  21.4 1.6 %fusion = bf16[256,2048]{0,1:T(8,128)(2,1)S(1)} fusion(f32[2048]{0:T(1024)S(1)} %copy-done.6, bf16[4,256,512]{1,2,0:T(8,128)(2,1)} %copy-done.1), kind=kLoop, calls=%fused_computation.1 | loop fusion | flops 1572864 | bytes 2105344 | tf_op jit(solution)/shard_map/convert_element_type | solution.py:506
  23.0 0.3 convolution_multiply_fusion.4
  23.3 0.1 multiply_cosine_fusion
  23.5 0.1 concatenate.20
  23.6 0.1 copy.24
  23.8 0.1 copy.23
  24.1 0.1 reshape.130
  24.2 1.9 %multiply_reduce_fusion.2 = (f32[256]{0:T(256)S(1)}, f32[256,256]{1,0:T(8,128)S(1)}) fusion(bf16[256,2048]{0,1:T(8,128)(2,1)S(1)} %fusion, bf16[2048,256]{1,0:T(8,128)(2,1)} %param.21, f32[256]{0:T(256)S(1)} %add_rsqrt_fusion.2), kind=kOutput, calls=%fused_computation.18 | convolution fusion | flops 268631808 | bytes 2361344 | tf_op jit(solution)/shard_map/dot_general | solution.py:509
  26.1 0.8 fusion.4
  27.0 0.8 multiply_reduce_fusion.1
  27.9 0.3 fusion.18
  28.2 0.3 convolution_convert_fusion
  28.7 0.1 multiply_convert_fusion.1
  28.8 0.7 pad_maximum_fusion.xp_ref
  29.5 1.4 %fusion.6.glu_ref = bf16[256,512]{1,0:T(8,128)(2,1)} fusion(f32[256,512]{1,0:T(8,128)S(1)} %fusion.4, bf16[256,2048]{0,1:T(8,128)(2,1)S(1)} %fusion, bf16[2048,512]{1,0:T(8,128)(2,1)S(1)} %copy-done.11, f32[256]{0:T(256)S(1)} %add_rsqrt_fusion.2), kind=kOutput, calls=%fused_computation.11 | convolution fusion | flops 537264128 | bytes 3933184 | tf_op jit(solution)/shard_map/dot_general | solution.py:509
  30.9 66.8 %attend.1 = bf16[256,512]{1,0:T(8,128)(2,1)} custom-call(bf16[2,144,256]{2,1,0:T(8,128)(2,1)} %pad_maximum_fusion.xp_ref, bf16[4,128,256]{2,1,0:T(8,128)(2,1)} %bitcast.74, bf16[256,256]{1,0:T(8,128)(2,1)} %ku_ref.1, bf16[256,256]{1,0:T(8,128)(2,1)} %bitcast.73, bf16[256,2048]{1,0:T(8,128)(2,1)} %wa_ref.1, bf16[256,512]{1,0:T(8,128)(2,1)} %fusion.6.glu_ref, ...), custom_call_target="tpu_custom_call" | custom-call | flops 10737418240 | bytes 2000000 | tf_op jit(solution)/shard_map/attend/pallas_call | solution.py:427
  97.7 1.7 %copy.38 = bf16[256,512]{1,0:T(8,128)(2,1)} copy(bf16[256,512]{1,0:T(8,128)(2,1)} %attend.1) | data formatting | bytes 524288
  (43 shorter events, 0.4 us)
Async XLA Ops:
  0.0 26.9 %copy-start = (bf16[2048,512]{1,0:T(8,128)(2,1)S(1)}, bf16[2048,512]{1,0:T(8,128)(2,1)}, u32[]{:S(2)}) copy-start(bf16[2048,512]{1,0:T(8,128)(2,1)} %param.20) | copy-start | bytes 6291460
  0.0 7.1 %copy-start.3 = (bf16[256,256]{1,0:T(8,128)(2,1)S(1)}, bf16[256,256]{1,0:T(8,128)(2,1)}, u32[]{:S(2)}) copy-start(bf16[256,256]{1,0:T(8,128)(2,1)} %param.28) | copy-start | bytes 393220
  1.2 20.2 %copy-start.6 = (f32[2048]{0:T(1024)S(1)}, f32[2048]{0:T(1024)}, u32[]{:S(2)}) copy-start(f32[2048]{0:T(1024)} %param.19) | copy-start | bytes 24580
  2.3 18.2 %all-to-all-start = ((bf16[4,256,512]{1,2,0:T(8,128)(2,1)}), bf16[4,256,512]{1,2,0:T(8,128)(2,1)S(1)}, u32[]{:S(2)}, u32[]{:S(2)}) async-start(bf16[4,256,512]{1,2,0:T(8,128)(2,1)} %broadcast_in_dim.8), calls=%async_computation | async-start | bytes 2097152 | tf_op jit(solution)/shard_map/all_to_all | solution.py:25
  7.1 15.9 %copy-start.5 = (bf16[2048,32]{0,1:T(8,128)(2,1)S(1)}, bf16[2048,32]{0,1:T(8,128)(2,1)}, u32[]{:S(2)}) copy-start(bf16[2048,32]{0,1:T(8,128)(2,1)} %param.22) | copy-start | bytes 393220
  20.5 1.0 copy-start.1
  24.2 1.9 %copy-start.10 = (bf16[2048,512]{1,0:T(8,128)(2,1)S(1)}, bf16[2048,512]{1,0:T(8,128)(2,1)}, u32[]{:S(2)}) copy-start(bf16[2048,512]{1,0:T(8,128)(2,1)} %param.30) | copy-start | bytes 6291460
  26.9 0.9 copy-start.4
  27.0 0.9 copy-start.7
  27.0 1.2 %copy-start.2 = (bf16[512,256]{1,0:T(8,128)(2,1)S(1)}, bf16[512,256]{1,0:T(8,128)(2,1)}, u32[]{:S(2)}) copy-start(bf16[512,256]{1,0:T(8,128)(2,1)} %param.25) | copy-start | bytes 786436
  27.8 0.9 copy-start.9
  27.8 1.7 %copy-start.11 = (bf16[2048,512]{1,0:T(8,128)(2,1)S(1)}, bf16[2048,512]{1,0:T(8,128)(2,1)}, u32[]{:S(2)}) copy-start(bf16[2048,512]{1,0:T(8,128)(2,1)} %param.29) | copy-start | bytes 6291460
  28.7 2.2 %copy-start.8 = (bf16[256,512]{0,1:T(8,128)(2,1)}, bf16[256,512]{0,1:T(8,128)(2,1)S(1)}, u32[]{:S(2)}) copy-start(bf16[256,512]{0,1:T(8,128)(2,1)S(1)} %fusion.7) | copy-start | bytes 786436

commit v6 on v5

--- a/solution.py
+++ b/solution.py
@@ -13,21 +13,6 @@
 theta = 10000.0
 bf16 = jnp.bfloat16
 f32 = jnp.float32
-
-def laid_out(blocks, dim):
-    dims = list(blocks.shape[1:])
-    dims[dim] *= blocks.shape[0]
-    return jnp.moveaxis(blocks, 0, dim).reshape(dims)
-
-
-def sent_to_all(shard, axis):
-    copies = jnp.broadcast_to(shard, (lax.axis_size(axis), *shard.shape))
-    return lax.all_to_all(copies, axis, split_axis=0, concat_axis=0, tiled=True)
-
-
-def gather_directly(shard, axis, dim):
-    return laid_out(sent_to_all(shard, axis), dim)
-
 
 def rms_scale(values, gain):
     return values * lax.rsqrt(jnp.mean(values * values, axis=-1, keepdims=True) + eps_norm) * gain
@@ -468,7 +453,7 @@
             dma((4,)),
         ],
         compiler_params=pltpu.CompilerParams(
-            collective_id=0, has_side_effects=True, vmem_limit_bytes=56 * 2**20
+            collective_id=0, has_side_effects=True, vmem_limit_bytes=40 * 2**20
         ),
         cost_estimate=pl.CostEstimate(
             flops=2 * 8192 * 2 * own_q * heads * 320,
@@ -477,6 +462,135 @@
         ),
         name="attend",
     )(xp, qt, key_up, value_up_t, out_attend, glu, taps, bias[None], gain[None], out_conv)
+
+
+def project_kernel(
+    tok_ref, gain_ref, qg_ref, lg_ref, wq_ref, wl_ref, wr_ref, wv_ref, wg_ref,
+    q_ref, kv_ref, rope_ref, glu_ref,
+    blocks, wq, wl, wr, wv, wg, aq, al, ar, av, ag, squares,
+    sent, got, sent_relay, local,
+):
+    sp, tp = lax.axis_index("sp"), lax.axis_index("tp")
+    width = tok_ref.shape[2]
+    half = tok_ref.shape[1]
+
+    def turn(a):
+        return lax.rem(a + 4, 4)
+
+    sides = [(sp, turn(tp + 1)), (sp, turn(tp - 1))]
+    barrier = pltpu.get_barrier_semaphore()
+    for peer in sides:
+        pl.semaphore_signal(barrier, inc=1, device_id=peer, device_id_type=pl.DeviceIdType.MESH)
+    pl.semaphore_wait(barrier, 2)
+
+    def remote(src, at, n, sem, target):
+        return pltpu.make_async_remote_copy(
+            src_ref=src, dst_ref=blocks.at[at, n], send_sem=sem, recv_sem=got.at[at, n],
+            device_id=target, device_id_type=pl.DeviceIdType.MESH,
+        )
+
+    first = [
+        remote(tok_ref.at[m], tp, m, sent.at[way, m], sides[way])
+        for n in range(2)
+        for way, m in ((0, n), (1, 1 - n))
+    ]
+    for copy in first:
+        copy.start()
+    loads = [
+        pltpu.make_async_copy(a, b, local.at[i])
+        for i, (a, b) in enumerate(
+            ((wq_ref, wq), (wl_ref, wl), (wr_ref, wr), (wv_ref, wv), (wg_ref, wg))
+        )
+    ]
+    for copy in loads:
+        copy.start()
+
+    def relay(n):
+        source = turn(tp - 1 + 2 * n)
+        return remote(blocks.at[source, n], source, n, sent_relay.at[n], sides[n])
+
+    def arrived(offset, n):
+        source = turn(tp + offset)
+        remote(blocks.at[source, n], source, n, sent_relay.at[n], sides[n]).wait_recv()
+
+    def add(source, piece, n, fresh):
+        here = slice(n * half, (n + 1) * half)
+        value = piece.astype(f32)
+        scaled = (value * gain_ref[source]).astype(bf16)
+        square = jnp.broadcast_to(jnp.sum(value * value, axis=1, keepdims=True), (half, 128))
+        rows = pl.ds(pl.multiple_of(source * width, width), width)
+        squares[here] = square if fresh else squares[here] + square
+        for w, a in ((wq, aq), (wl, al), (wr, ar), (wv, av), (wg, ag)):
+            if w is wr:
+                part = lax.dot_general(
+                    scaled, w[:, rows], (((1,), (1,)), ((), ())), preferred_element_type=f32
+                )
+            else:
+                part = jnp.dot(scaled, w[rows, :], preferred_element_type=f32)
+            a[here] = part if fresh else a[here] + part
+
+    for copy in loads:
+        copy.wait()
+    for n in range(2):
+        add(tp, tok_ref[n], n, True)
+    arrived(-1, 0)
+    relay(0).start()
+    arrived(1, 1)
+    relay(1).start()
+    left, right, across = turn(tp - 1), turn(tp + 1), turn(tp + 2)
+    add(left, blocks[left, 0], 0, False)
+    add(right, blocks[right, 1], 1, False)
+    arrived(-1, 1)
+    add(left, blocks[left, 1], 1, False)
+    arrived(1, 0)
+    add(right, blocks[right, 0], 0, False)
+    for n in range(2):
+        arrived(2, n)
+        add(across, blocks[across, n], n, False)
+    row_scale = lax.rsqrt(squares[:, :1] / (4 * width) + eps_norm)
+    q_ref[...] = rms_scale(row_scale * aq[...], qg_ref[...]).astype(bf16)
+    kv_ref[...] = rms_scale(row_scale * al[...], lg_ref[...]).astype(bf16)
+    rope_ref[...] = row_scale * ar[...]
+    glu_ref[...] = (row_scale * av[...] * jax.nn.sigmoid(row_scale * ag[...])).astype(bf16)
+    for copy in first:
+        copy.wait_send()
+    for n in range(2):
+        relay(n).wait_send()
+
+
+def project(tokens, in_gain, query_gain, latent_gain, weights):
+    rows, width = tokens.shape
+    vmem = pl.BlockSpec(memory_space=pltpu.VMEM)
+    dma = pltpu.SemaphoreType.DMA
+    wide = [min(w.shape) for w in weights]
+    return pl.pallas_call(
+        project_kernel,
+        out_shape=(
+            jax.ShapeDtypeStruct((rows, wide[0]), bf16),
+            jax.ShapeDtypeStruct((rows, wide[1]), bf16),
+            jax.ShapeDtypeStruct((rows, wide[2]), f32),
+            jax.ShapeDtypeStruct((rows, wide[3]), bf16),
+        ),
+        in_specs=[vmem] * 4 + [pl.BlockSpec(memory_space=pl.ANY)] * 5,
+        out_specs=(vmem,) * 4,
+        scratch_shapes=[pltpu.VMEM((4, 2, rows // 2, width), bf16)]
+        + [pltpu.VMEM(w.shape, bf16) for w in weights]
+        + [pltpu.VMEM((rows, n), f32) for n in wide]
+        + [pltpu.VMEM((rows, 128), f32), dma((2, 2)), dma((4, 2)), dma((2,)), dma((5,))],
+        compiler_params=pltpu.CompilerParams(
+            collective_id=1, has_side_effects=True, vmem_limit_bytes=60 * 2**20
+        ),
+        cost_estimate=pl.CostEstimate(
+            flops=2 * rows * 4 * width * sum(wide), bytes_accessed=10**7, transcendentals=10**5
+        ),
+        name="project",
+    )(
+        tokens.reshape(2, rows // 2, width),
+        in_gain.reshape(4, 1, width),
+        query_gain[None],
+        latent_gain[None],
+        *weights,
+    )
 
 
 def per_device(
@@ -500,24 +614,15 @@
     out_conv,
 ):
     row_count = tokens.shape[0]
-    width = in_gain.shape[0]
     positions = (lax.axis_index("sp") * row_count + jnp.arange(row_count)).astype(f32)
-    piece_f = gather_directly(tokens, "tp", 1).astype(f32)
-    scaled = (piece_f * in_gain).astype(bf16)
-
-    def add_rows(weight):
-        return jnp.dot(scaled, weight, preferred_element_type=f32)
-
-    square_sum = jnp.sum(piece_f * piece_f, axis=1)
-    q_pre = add_rows(query_down)
-    kv_pre = add_rows(latent_down)
-    rope_pre = add_rows(rope_down)
-    value_pre = add_rows(conv_value)
-    gate_pre = add_rows(conv_gate)
-    row_scale = lax.rsqrt(square_sum / width + eps_norm)[:, None]
-    q_latent = rms_scale(row_scale * q_pre, query_gain).astype(bf16)
-    kv_latent = rms_scale(row_scale * kv_pre, latent_gain).astype(bf16)
-    rope_key = rotate(row_scale * rope_pre, positions).astype(bf16)
+    q_latent, kv_latent, rope_pre, glu = project(
+        tokens,
+        in_gain,
+        query_gain,
+        latent_gain,
+        (query_down, latent_down, jnp.transpose(rope_down), conv_value, conv_gate),
+    )
+    rope_key = rotate(rope_pre, positions).astype(bf16)
     rope_size = rope_down.shape[1]
     heads = query_rope.shape[1] // rope_size
     nope = query_nope.shape[1] // heads
@@ -542,7 +647,6 @@
         else:
             cols += [r_heads[:, h], empty, q_heads[:, h]]
     q_own = jnp.transpose(jnp.concatenate(cols, axis=1))
-    glu = (row_scale * value_pre * jax.nn.sigmoid(row_scale * gate_pre)).astype(bf16)
     return attend(
         xp,
         q_own.reshape(heads, 128, row_count),

time: 99.8 us -> 87.1 us (0.87)
  waiting for transfers between devices: 12.6 us -> 0 us
  Pallas kernels: 66.8 us -> 78.9 us
  starting transfers between devices: 4.83 us -> 0 us
  matrix products: 5.89 us -> 2.42 us
  local copies, waits for them, and re-layouts: 6.07 us -> 3.29 us
  other arithmetic: 2.94 us -> 1.85 us
    pallas_call x0 -> x1, Pallas kernels: none -> 14.9 us  [project(): pl.pallas_call(project_kernel, out_shape=(jax.ShapeDtypeStruct((rows, wid...]
    all_to_all x1 -> x0, waiting for transfers between devices: 12.6 us -> none  [sent_to_all(): return lax.all_to_all(copies, axis, split_axis=0, concat_axis=0, tiled=True)]
    dot_general x5 -> x0, matrix products: 5.25 us -> none  [add_rows(): return jnp.dot(scaled, weight, preferred_element_type=f32)]
    all_to_all x1 -> x0, starting transfers between devices: 4.83 us -> none  [sent_to_all(): return lax.all_to_all(copies, axis, split_axis=0, concat_axis=0, tiled=True)]
    pallas_call x1, Pallas kernels: 66.8 us -> 64 us  [attend(): pl.pallas_call(functools.partial(attend_kernel, heads, scale), out_shape=...]
    convert_element_type x2 -> x0, other arithmetic: 1.67 us -> none  [the longest x1 1.56 us: per_device(): scaled = (piece_f * in_gain).astype(bf16)]
    cos x1, other arithmetic: 0.15 us -> 1.69 us  [rotate(): cosine = jnp.cos(angles)]
    unnamed x34 -> x29, local copies, waits for them, and re-layouts: 4.44 us -> 3 us
  transfers between devices with their start and end apart: 1 -> 0, of which waited for: 1 -> 0; matrix products, arithmetic and copies ran while one was open for 1% -> 0% of each run, Pallas kernels for 0% -> 0%
where the time goes in v6:
time: 87.1 us; the launch traced here: 86.7 us
  Pallas kernels  78.9 us (91%)
  local copies, waits for them, and re-layouts  3.29 us (4%)
  matrix products  2.42 us (3%)
  other arithmetic  1.85 us (2%)
    pallas_call x1, Pallas kernels, attend(): pl.pallas_call(functools.partial(attend_kernel, heads, scale), out_shape=...  64 us
    pallas_call x1, Pallas kernels, project(): pl.pallas_call(project_kernel, out_shape=(jax.ShapeDtypeStruct((rows, wid...  14.9 us
    unnamed x29, local copies, waits for them, and re-layouts  3 us

profile of v6, /device:TPU:1, one launch (start us, length us, event | category | flops | bytes accessed | tf_op | source)
XLA Modules:
  0.0 86.7 jit_solution(1202517991579446095)
XLA Ops:
  0.0 0.0 copy-start
  0.0 14.9 %project.1 = (bf16[256,512]{1,0:T(8,128)(2,1)}, bf16[256,256]{1,0:T(8,128)(2,1)}, f32[256,32]{1,0:T(8,128)}, bf16[256,512]{1,0:T(8,128)(2,1)}) custom-call(bf16[2,128,512]{2,1,0:T(8,128)(2,1)} %bitcast.65, f32[4,1,512]{2,1,0:T(1,128)} %bitcast.70, f32[1,512]{1,0:T(1,128)} %bitcast.71, f32[1,256]{1,0:T(1,128)} %bitcast.72, bf16[2048,512]{1,0:T(8,128)(2,1)} %wq_ref.1, ...), custom_call_target="tpu_custom_call" | custom-call | flops 1912602624 | bytes 10000000 | tf_op jit(solution)/shard_map/project/pallas_call | solution.py:566
  14.9 0.0 copy-start.8
  14.9 0.0 copy-start.1
  14.9 0.0 copy-start.3
  14.9 0.0 copy-start.4
  14.9 0.0 copy-start.5
  14.9 0.0 copy-start.6
  14.9 0.0 copy-start.7
  15.0 1.7 %multiply_cosine_fusion = (f32[256,16]{1,0:T(8,128)S(1)}, f32[256,16]{1,0:T(8,128)S(1)}, bf16[256,16]{1,0:T(8,128)(2,1)S(1)}, bf16[256,16]{1,0:T(8,128)(2,1)S(1)}) fusion(f32[256]{0:T(256)S(1)} %add_convert_fusion.2, f32[16]{0:T(128)S(1)} %multiply_power_fusion, f32[256,32]{1,0:T(8,128)} %get-tuple-element.10), kind=kLoop, calls=%fused_computation.2 | loop fusion | flops 36864 | bytes 83008 | tf_op jit(solution)/shard_map/cos | solution.py:25
  16.7 0.1 copy.27
  16.8 0.1 copy.28
  16.8 0.0 copy-done.9
  16.8 1.2 %fusion.11 = f32[256,128]{0,1:T(8,128)S(1)} fusion(bf16[256,512]{1,0:T(8,128)(2,1)} %get-tuple-element.11, bf16[512,128]{1,0:T(8,128)(2,1)S(1)} %copy-done.9), kind=kOutput, calls=%fused_computation.41 | convolution fusion | flops 33554432 | bytes 524288 | tf_op jit(solution)/shard_map/dot_general | solution.py:638
  18.1 0.0 copy-done
  18.1 1.2 %convolution_convert_fusion = bf16[256,256]{0,1:T(8,128)(2,1)S(1)} fusion(bf16[256,512]{1,0:T(8,128)(2,1)} %get-tuple-element.11, bf16[512,256]{1,0:T(8,128)(2,1)S(1)} %copy-done), kind=kOutput, calls=%fused_computation | convolution fusion | flops 67174400 | bytes 655360 | tf_op jit(solution)/shard_map/dot_general | solution.py:634
  19.5 0.1 maximum_bitcast_fusion
  19.6 0.1 reshape.111
  19.7 0.0 copy-done.8
  19.7 1.0 %copy.29 = bf16[256,256]{0,1:T(8,128)(2,1)S(1)} copy(bf16[256,256]{1,0:T(8,128)(2,1)} %param.28) | data formatting | bytes 262144 | tf_op args[10]
  20.8 0.0 copy-start.2
  20.8 1.2 %copy-done.2 = bf16[256,2048]{1,0:T(8,128)(2,1)S(1)} copy-done((bf16[256,2048]{1,0:T(8,128)(2,1)S(1)}, bf16[256,2048]{1,0:T(8,128)(2,1)}, u32[]{:S(2)}) %copy-start.2) | copy-done | bytes 1048600
  22.0 64.0 %attend.1 = bf16[256,512]{1,0:T(8,128)(2,1)S(1)} custom-call(bf16[2,144,256]{2,1,0:T(8,128)(2,1)S(1)} %pad_maximum_fusion.xp_ref, bf16[4,128,256]{2,1,0:T(8,128)(2,1)S(1)} %bitcast.57, bf16[256,256]{1,0:T(8,128)(2,1)S(1)} %copy-done.4, bf16[256,256]{1,0:T(8,128)(2,1)S(1)} %bitcast.56, bf16[256,2048]{1,0:T(8,128)(2,1)S(1)} %copy-done.2, ...), custom_call_target="tpu_custom_call" | custom-call | flops 10737418240 | bytes 2000000 | tf_op jit(solution)/shard_map/attend/pallas_call | solution.py:412
  86.0 0.7 copy.42
  (25 shorter events, 0.1 us)
Async XLA Ops:
  0.0 18.1 %copy-start = (bf16[512,256]{1,0:T(8,128)(2,1)S(1)}, bf16[512,256]{1,0:T(8,128)(2,1)}, u32[]{:S(2)}) copy-start(bf16[512,256]{1,0:T(8,128)(2,1)} %param.25) | copy-start | bytes 786436
  0.0 16.8 %copy-start.9 = (bf16[512,128]{1,0:T(8,128)(2,1)S(1)}, bf16[512,128]{1,0:T(8,128)(2,1)}, u32[]{:S(2)}) copy-start(bf16[512,128]{1,0:T(8,128)(2,1)} %param.26) | copy-start | bytes 393220
  14.9 4.8 %copy-start.8 = (bf16[256,256]{1,0:T(8,128)(2,1)S(1)}, bf16[256,256]{1,0:T(8,128)(2,1)}, u32[]{:S(2)}) copy-start(bf16[256,256]{1,0:T(8,128)(2,1)} %get-tuple-element.9) | copy-start | bytes 393220
  14.9 5.8 %copy-start.1 = (bf16[512,2048]{1,0:T(8,128)(2,1)S(1)}, bf16[512,2048]{1,0:T(8,128)(2,1)}, u32[]{:S(2)}) copy-start(bf16[512,2048]{1,0:T(8,128)(2,1)} %oc_ref.1) | copy-start | bytes 6291460
  14.9 5.8 %copy-start.3 = (bf16[256,512]{1,0:T(8,128)(2,1)S(1)}, bf16[256,512]{1,0:T(8,128)(2,1)}, u32[]{:S(2)}) copy-start(bf16[256,512]{1,0:T(8,128)(2,1)} %get-tuple-element.12.glu_ref) | copy-start | bytes 786436
  14.9 5.8 %copy-start.4 = (bf16[256,256]{1,0:T(8,128)(2,1)S(1)}, bf16[256,256]{1,0:T(8,128)(2,1)}, u32[]{:S(2)}) copy-start(bf16[256,256]{1,0:T(8,128)(2,1)} %ku_ref.1) | copy-start | bytes 393220
  14.9 5.8 %copy-start.5 = (f32[31,512]{1,0:T(8,128)S(1)}, f32[31,512]{1,0:T(8,128)}, u32[]{:S(2)}) copy-start(f32[31,512]{1,0:T(8,128)} %taps_ref.1) | copy-start | bytes 190468
  14.9 5.8 %copy-start.6 = (f32[512]{0:T(512)S(1)}, f32[512]{0:T(512)}, u32[]{:S(2)}) copy-start(f32[512]{0:T(512)} %param.32) | copy-start | bytes 6148
  14.9 5.8 %copy-start.7 = (f32[512]{0:T(512)S(1)}, f32[512]{0:T(512)}, u32[]{:S(2)}) copy-start(f32[512]{0:T(512)} %param.33) | copy-start | bytes 6148
  20.8 1.2 %copy-start.2 = (bf16[256,2048]{1,0:T(8,128)(2,1)S(1)}, bf16[256,2048]{1,0:T(8,128)(2,1)}, u32[]{:S(2)}) copy-start(bf16[256,2048]{1,0:T(8,128)(2,1)} %wa_ref.1) | copy-start | bytes 3145732

commit v7 on v6

--- a/solution.py
+++ b/solution.py
@@ -32,12 +32,12 @@
 
 
 def attend_kernel(
-    heads, scale, xp_ref, qt_ref, ku_ref, vut_ref, wa_ref, glu_ref,
+    heads, scale, xp_ref, qt_ref, ku_ref, vu_ref, wa_ref, glu_ref,
     taps_ref, bias_ref, gain_ref, oc_ref, out_ref,
     x, q, keys, vals, acc, high, acc_in, high_in, part_out, stat_out, part_in, stat_in, wide, conv_in, weight_in,
-    halo, padded, shifted, conv, moments, active, cp_ref,
+    halo, padded, shifted, conv, moments, active, cp_ref, vut_ref,
     got_x, sent_x, got_q, sent_q, sent_relay, sent_pair_q, got_pair_q, pair_sem, part_sem,
-    sent_t, got_t, halo_sem, sent_m, got_m,
+    sent_t, got_t, halo_sem, sent_m, got_m, sent_f, got_f, relay_f,
 ):
     sp, tp = lax.axis_index("sp"), lax.axis_index("tp")
     core = lax.rem(sp, 2)
@@ -45,7 +45,7 @@
     z = sp // 8
     own_q = qt_ref.shape[2]
     depth = xp_ref.shape[1] - 16
-    vrows = vut_ref.shape[0] // heads
+    vrows = vu_ref.shape[1] // heads
     half_heads = heads // 2
 
     def device(pz, py):
@@ -127,6 +127,7 @@
         copy.start()
     x[z] = xp_ref[...]
     q[y, core] = qt_ref[...]
+    vut_ref[...] = jnp.transpose(vu_ref[...].astype(f32)).astype(bf16)
     acc[...] = jnp.zeros_like(acc)
     high[...] = jnp.full_like(high, -jnp.inf)
 
@@ -368,6 +369,7 @@
             copy.wait()
     for copy in swap(0):
         copy.wait()
+    half = own_q // 2
     for h in range(heads):
         tops = [high[0, h : h + 1, :own_q], high_in[0, h : h + 1, :]]
         totals = [acc[0, h, vrows : vrows + 1, :own_q], acc_in[0, h, vrows : vrows + 1, :]]
@@ -380,30 +382,71 @@
         whole = acc[0, h, :vrows, :own_q] * shares[0] + acc_in[0, h, :vrows, :] * shares[1]
         for r in range(3):
             whole = whole + part_in[r, h].astype(f32) * (shares[2 + r] * totals[2 + r])
-        wide[tp, :, h * vrows : (h + 1) * vrows] = jnp.transpose(whole / total).astype(bf16)
+        done = jnp.transpose(whole / total).astype(bf16)
+        for n in range(2):
+            wide[tp, n, :, h * vrows : (h + 1) * vrows] = done[n * half : (n + 1) * half]
+    def final_copy(source, n, sem, target):
+        at = wide.at[source, n]
+        return remote(at, at, sem, got_f.at[source, n], target)
+
+    sides = others[:2]
     last = [
-        remote(wide.at[tp], wide.at[tp], sent_t.at[2, i], got_t.at[2, tp], peer)
-        for i, peer in enumerate(others)
+        final_copy(tp, m, sent_f.at[way, m], sides[way])
+        for n in range(2)
+        for way, m in ((0, n), (1, 1 - n))
     ]
     for copy in last:
         copy.start()
-    result = jnp.dot(wide[tp], block(wa_ref, tp)[...], preferred_element_type=f32)
-    result = result + block(cp_ref, tp)[...].astype(f32)
-    for i in (1, 3, 2):
-        source = lax.rem(tp + i, 4)
-        for kind, dst in enumerate((weight_in, conv_in, wide)):
+    own_weight = block(wa_ref, tp)[...]
+    around = [lax.rem(tp + i, 4) for i in (1, 2, 3)]
+    for source in around:
+        for kind, dst in enumerate((weight_in, conv_in)):
             at = dst.at[source]
             remote(at, at, sent_t.at[kind, 0], got_t.at[kind, source], others[0]).wait_recv()
-        result = result + jnp.dot(wide[source], weight_in[source], preferred_element_type=f32)
-        result = result + conv_in[source].astype(f32)
-    out_ref[...] = result.astype(bf16)
+    result = []
+    for n in range(2):
+        rows = slice(n * half, (n + 1) * half)
+        part = jnp.dot(wide[tp, n], own_weight, preferred_element_type=f32)
+        part = part + block(cp_ref, tp)[rows].astype(f32)
+        for source in around:
+            part = part + conv_in[source, rows].astype(f32)
+        result.append(part)
+    right_x, across_x, left_x = around
+
+    def relay_final(n):
+        return final_copy(left_x if n == 0 else right_x, n, relay_f.at[n], sides[n])
+
+    def final_arrived(source, n):
+        final_copy(source, n, relay_f.at[n], sides[n]).wait_recv()
+
+    def take(source, n):
+        result[n] = result[n] + jnp.dot(
+            wide[source, n], weight_in[source], preferred_element_type=f32
+        )
+
+    final_arrived(left_x, 0)
+    relay_final(0).start()
+    final_arrived(right_x, 1)
+    relay_final(1).start()
+    take(left_x, 0)
+    take(right_x, 1)
+    final_arrived(left_x, 1)
+    take(left_x, 1)
+    final_arrived(right_x, 0)
+    take(right_x, 0)
+    for n in range(2):
+        final_arrived(across_x, n)
+        take(across_x, n)
+        out_ref[n * half : (n + 1) * half, :] = result[n].astype(bf16)
     for copy in last:
         copy.wait_send()
-
-
-def attend(xp, qt, key_up, value_up_t, out_attend, glu, taps, bias, gain, out_conv, size):
+    for n in range(2):
+        relay_final(n).wait_send()
+
+
+def attend(xp, qt, key_up, value_up, out_attend, glu, taps, bias, gain, out_conv, size):
     heads, width, own_q = qt.shape
-    vdim = value_up_t.shape[0] // heads
+    vdim = value_up.shape[1] // heads
     columns = out_attend.shape[1] // 4
     channels = glu.shape[1]
     vmem = pl.BlockSpec(memory_space=pltpu.VMEM)
@@ -427,7 +470,7 @@
             pltpu.VMEM((3, heads, 8, own_q), f32),
             pltpu.VMEM((3, heads, vdim, own_q), bf16),
             pltpu.VMEM((3, heads, 8, own_q), f32),
-            pltpu.VMEM((4, own_q, heads * vdim), bf16),
+            pltpu.VMEM((4, 2, own_q // 2, heads * vdim), bf16),
             pltpu.VMEM((4, own_q, columns), bf16),
             pltpu.VMEM((4, heads * vdim, columns), bf16),
             pltpu.VMEM((2, 16, channels), bf16),
@@ -437,6 +480,7 @@
             pltpu.VMEM((4, 8, own_q), f32),
             pltpu.VMEM((own_q, channels), bf16),
             pltpu.VMEM((own_q, 4 * columns), bf16),
+            pltpu.VMEM(value_up.shape[::-1], bf16),
             dma((8, 2)),
             dma((8, 2)),
             dma((4, 2)),
@@ -446,11 +490,14 @@
             dma((4, 2)),
             dma((4, 4)),
             dma((3, 2, 2)),
-            dma((3, 3)),
-            dma((3, 4)),
+            dma((2, 3)),
+            dma((2, 4)),
             dma((2, 2)),
             dma((3,)),
             dma((4,)),
+            dma((2, 2)),
+            dma((4, 2)),
+            dma((2,)),
         ],
         compiler_params=pltpu.CompilerParams(
             collective_id=0, has_side_effects=True, vmem_limit_bytes=40 * 2**20
@@ -461,7 +508,7 @@
             transcendentals=8192 * 2 * own_q * heads,
         ),
         name="attend",
-    )(xp, qt, key_up, value_up_t, out_attend, glu, taps, bias[None], gain[None], out_conv)
+    )(xp, qt, key_up, value_up, out_attend, glu, taps, bias[None], gain[None], out_conv)
 
 
 def project_kernel(
@@ -651,7 +698,7 @@
         xp,
         q_own.reshape(heads, 128, row_count),
         key_up,
-        jnp.transpose(value_up),
+        value_up,
         out_attend,
         glu,
         conv_taps,

time: 87.1 us -> 85.9 us (0.986)
  local copies, waits for them, and re-layouts: 3.29 us -> 2.28 us
  Pallas kernels: 78.9 us -> 78 us
    unnamed x29 -> x28, local copies, waits for them, and re-layouts: 3 us -> 2 us
where the time goes in v7:
time: 85.9 us; the launch traced here: 84.9 us
  Pallas kernels  78 us (91%)
  matrix products  2.45 us (3%)
  local copies, waits for them, and re-layouts  2.28 us (3%)
  other arithmetic  1.85 us (2%)
    pallas_call x1, Pallas kernels, attend(): pl.pallas_call(functools.partial(attend_kernel, heads, scale), out_shape=...  63.1 us
    pallas_call x1, Pallas kernels, project(): pl.pallas_call(project_kernel, out_shape=(jax.ShapeDtypeStruct((rows, wid...  14.8 us
    unnamed x28, local copies, waits for them, and re-layouts  2 us

profile of v7, /device:TPU:1, one launch (start us, length us, event | category | flops | bytes accessed | tf_op | source)
XLA Modules:
  0.0 84.9 jit_solution(11028715349757990619)
XLA Ops:
  0.0 0.0 copy-start
  0.0 14.8 %project.1 = (bf16[256,512]{1,0:T(8,128)(2,1)}, bf16[256,256]{1,0:T(8,128)(2,1)}, f32[256,32]{1,0:T(8,128)}, bf16[256,512]{1,0:T(8,128)(2,1)}) custom-call(bf16[2,128,512]{2,1,0:T(8,128)(2,1)} %bitcast.63, f32[4,1,512]{2,1,0:T(1,128)} %bitcast.68, f32[1,512]{1,0:T(1,128)} %bitcast.69, f32[1,256]{1,0:T(1,128)} %bitcast.70, bf16[2048,512]{1,0:T(8,128)(2,1)} %wq_ref.1, ...), custom_call_target="tpu_custom_call" | custom-call | flops 1912602624 | bytes 10000000 | tf_op jit(solution)/shard_map/project/pallas_call | solution.py:613
  14.8 0.0 copy-start.9
  14.8 0.0 copy-start.1
  14.9 0.0 copy-start.3
  14.9 0.0 copy-start.4
  14.9 0.0 copy-start.5
  14.9 0.0 copy-start.6
  14.9 0.0 copy-start.7
  14.9 0.0 copy-start.8
  15.0 1.7 %multiply_cosine_fusion = (f32[256,16]{1,0:T(8,128)S(1)}, f32[256,16]{1,0:T(8,128)S(1)}, bf16[256,16]{1,0:T(8,128)(2,1)S(1)}, bf16[256,16]{1,0:T(8,128)(2,1)S(1)}) fusion(f32[256]{0:T(256)S(1)} %add_convert_fusion.2, f32[16]{0:T(128)S(1)} %multiply_power_fusion, f32[256,32]{1,0:T(8,128)} %get-tuple-element.10), kind=kLoop, calls=%fused_computation.2 | loop fusion | flops 36864 | bytes 83008 | tf_op jit(solution)/shard_map/cos | solution.py:25
  16.7 0.1 copy.26
  16.7 0.1 copy.27
  16.8 1.2 %fusion.11 = f32[256,128]{0,1:T(8,128)S(1)} fusion(bf16[256,512]{1,0:T(8,128)(2,1)} %get-tuple-element.11, bf16[512,128]{1,0:T(8,128)(2,1)} %param.26), kind=kOutput, calls=%fused_computation.41 | convolution fusion | flops 33554432 | bytes 524288 | tf_op jit(solution)/shard_map/dot_general | solution.py:685
  18.0 0.0 copy-done
  18.1 1.2 %convolution_convert_fusion = bf16[256,256]{0,1:T(8,128)(2,1)S(1)} fusion(bf16[256,512]{1,0:T(8,128)(2,1)} %get-tuple-element.11, bf16[512,256]{1,0:T(8,128)(2,1)S(1)} %copy-done), kind=kOutput, calls=%fused_computation | convolution fusion | flops 67174400 | bytes 655360 | tf_op jit(solution)/shard_map/dot_general | solution.py:681
  19.5 0.1 maximum_bitcast_fusion
  19.6 0.1 reshape.111
  19.7 0.0 copy-done.9
  19.7 0.0 copy-done.1
  19.8 0.0 copy-start.2
  19.8 1.2 %copy-done.2 = bf16[256,2048]{1,0:T(8,128)(2,1)S(1)} copy-done((bf16[256,2048]{1,0:T(8,128)(2,1)S(1)}, bf16[256,2048]{1,0:T(8,128)(2,1)}, u32[]{:S(2)}) %copy-start.2) | copy-done | bytes 1048600
  21.0 63.1 %attend.1 = bf16[256,512]{1,0:T(8,128)(2,1)S(1)} custom-call(bf16[2,144,256]{2,1,0:T(8,128)(2,1)S(1)} %pad_maximum_fusion.xp_ref, bf16[4,128,256]{2,1,0:T(8,128)(2,1)S(1)} %bitcast.55, bf16[256,256]{1,0:T(8,128)(2,1)S(1)} %copy-done.4, bf16[256,256]{1,0:T(8,128)(2,1)S(1)} %copy-done.5, bf16[256,2048]{1,0:T(8,128)(2,1)S(1)} %copy-done.2, ...), custom_call_target="tpu_custom_call" | custom-call | flops 10737418240 | bytes 2000000 | tf_op jit(solution)/shard_map/attend/pallas_call | solution.py:455
  84.2 0.7 copy.40
  (24 shorter events, 0.1 us)
Async XLA Ops:
  0.0 18.0 %copy-start = (bf16[512,256]{1,0:T(8,128)(2,1)S(1)}, bf16[512,256]{1,0:T(8,128)(2,1)}, u32[]{:S(2)}) copy-start(bf16[512,256]{1,0:T(8,128)(2,1)} %param.25) | copy-start | bytes 786436
  14.8 4.9 %copy-start.9 = (bf16[256,256]{1,0:T(8,128)(2,1)S(1)}, bf16[256,256]{1,0:T(8,128)(2,1)}, u32[]{:S(2)}) copy-start(bf16[256,256]{1,0:T(8,128)(2,1)} %get-tuple-element.9) | copy-start | bytes 393220
  14.8 4.9 %copy-start.1 = (bf16[512,2048]{1,0:T(8,128)(2,1)S(1)}, bf16[512,2048]{1,0:T(8,128)(2,1)}, u32[]{:S(2)}) copy-start(bf16[512,2048]{1,0:T(8,128)(2,1)} %oc_ref.1) | copy-start | bytes 6291460
  14.9 4.9 %copy-start.3 = (bf16[256,512]{1,0:T(8,128)(2,1)S(1)}, bf16[256,512]{1,0:T(8,128)(2,1)}, u32[]{:S(2)}) copy-start(bf16[256,512]{1,0:T(8,128)(2,1)} %get-tuple-element.12.glu_ref) | copy-start | bytes 786436
  14.9 4.9 %copy-start.4 = (bf16[256,256]{1,0:T(8,128)(2,1)S(1)}, bf16[256,256]{1,0:T(8,128)(2,1)}, u32[]{:S(2)}) copy-start(bf16[256,256]{1,0:T(8,128)(2,1)} %ku_ref.1) | copy-start | bytes 393220
  14.9 4.9 %copy-start.5 = (bf16[256,256]{1,0:T(8,128)(2,1)S(1)}, bf16[256,256]{1,0:T(8,128)(2,1)}, u32[]{:S(2)}) copy-start(bf16[256,256]{1,0:T(8,128)(2,1)} %vu_ref.1) | copy-start | bytes 393220
  14.9 4.9 %copy-start.6 = (f32[31,512]{1,0:T(8,128)S(1)}, f32[31,512]{1,0:T(8,128)}, u32[]{:S(2)}) copy-start(f32[31,512]{1,0:T(8,128)} %taps_ref.1) | copy-start | bytes 190468
  14.9 4.9 %copy-start.7 = (f32[512]{0:T(512)S(1)}, f32[512]{0:T(512)}, u32[]{:S(2)}) copy-start(f32[512]{0:T(512)} %param.32) | copy-start | bytes 6148
  14.9 4.9 %copy-start.8 = (f32[512]{0:T(512)S(1)}, f32[512]{0:T(512)}, u32[]{:S(2)}) copy-start(f32[512]{0:T(512)} %param.33) | copy-start | bytes 6148
  19.8 1.2 %copy-start.2 = (bf16[256,2048]{1,0:T(8,128)(2,1)S(1)}, bf16[256,2048]{1,0:T(8,128)(2,1)}, u32[]{:S(2)}) copy-start(bf16[256,2048]{1,0:T(8,128)(2,1)} %wa_ref.1) | copy-start | bytes 3145732

commit v8 on v7

--- a/solution.py
+++ b/solution.py
@@ -18,12 +18,8 @@
     return values * lax.rsqrt(jnp.mean(values * values, axis=-1, keepdims=True) + eps_norm) * gain
 
 
-def rotate(values, positions):
+def rotate(values, cosine, sine):
     half = values.shape[-1] // 2
-    freqs = theta ** (-jnp.arange(half).astype(f32) / half)
-    angles = positions[..., None] * freqs
-    cosine = jnp.cos(angles)
-    sine = jnp.sin(angles)
     first = values[..., :half]
     second = values[..., half:]
     return jnp.concatenate(
@@ -512,9 +508,10 @@
 
 
 def project_kernel(
-    tok_ref, gain_ref, qg_ref, lg_ref, wq_ref, wl_ref, wr_ref, wv_ref, wg_ref,
-    q_ref, kv_ref, rope_ref, glu_ref,
-    blocks, wq, wl, wr, wv, wg, aq, al, ar, av, ag, squares,
+    tok_ref, gain_ref, qg_ref, lg_ref, freq_ref,
+    wq_ref, wl_ref, wr_ref, wv_ref, wg_ref, wn_ref, wt_ref,
+    qt_ref, kv_ref, rope_ref, glu_ref, cos_ref, sin_ref,
+    blocks, wq, wl, wr, wv, wg, wn, wt, aq, al, ar, av, ag, squares,
     sent, got, sent_relay, local,
 ):
     sp, tp = lax.axis_index("sp"), lax.axis_index("tp")
@@ -546,7 +543,10 @@
     loads = [
         pltpu.make_async_copy(a, b, local.at[i])
         for i, (a, b) in enumerate(
-            ((wq_ref, wq), (wl_ref, wl), (wr_ref, wr), (wv_ref, wv), (wg_ref, wg))
+            (
+                (wq_ref, wq), (wl_ref, wl), (wr_ref, wr), (wv_ref, wv), (wg_ref, wg),
+                (wn_ref, wn), (wt_ref, wt),
+            )
         )
     ]
     for copy in loads:
@@ -576,6 +576,10 @@
                 part = jnp.dot(scaled, w[rows, :], preferred_element_type=f32)
             a[here] = part if fresh else a[here] + part
 
+    place = sp * cos_ref.shape[1] + lax.broadcasted_iota(jnp.int32, cos_ref.shape, 1)
+    angles = freq_ref[...] * place.astype(f32)
+    cos_ref[...] = jnp.cos(angles)
+    sin_ref[...] = jnp.sin(angles)
     for copy in loads:
         copy.wait()
     for n in range(2):
@@ -595,7 +599,25 @@
         arrived(2, n)
         add(across, blocks[across, n], n, False)
     row_scale = lax.rsqrt(squares[:, :1] / (4 * width) + eps_norm)
-    q_ref[...] = rms_scale(row_scale * aq[...], qg_ref[...]).astype(bf16)
+    latent = rms_scale(row_scale * aq[...], qg_ref[...]).astype(bf16)
+    plain = jnp.transpose(jnp.dot(latent, wn[...], preferred_element_type=f32)).astype(bf16)
+    turned = jnp.transpose(jnp.dot(latent, wt[...], preferred_element_type=f32))
+    heads = qt_ref.shape[0]
+    nope, both = plain.shape[0] // heads, turned.shape[0] // heads
+    cosine, sine = cos_ref[...], sin_ref[...]
+    for h in range(heads):
+        one = turned[h * both : h * both + both // 2]
+        two = turned[h * both + both // 2 : (h + 1) * both]
+        parts = [
+            plain[h * nope : (h + 1) * nope],
+            (one * cosine - two * sine).astype(bf16),
+            (two * cosine + one * sine).astype(bf16),
+            jnp.zeros((nope - both, plain.shape[1]), bf16),
+        ]
+        at = 0
+        for part in parts if h % 2 == 0 else parts[1:] + parts[:1]:
+            qt_ref[h, at : at + part.shape[0], :] = part
+            at += part.shape[0]
     kv_ref[...] = rms_scale(row_scale * al[...], lg_ref[...]).astype(bf16)
     rope_ref[...] = row_scale * ar[...]
     glu_ref[...] = (row_scale * av[...] * jax.nn.sigmoid(row_scale * ag[...])).astype(bf16)
@@ -605,25 +627,28 @@
         relay(n).wait_send()
 
 
-def project(tokens, in_gain, query_gain, latent_gain, weights):
+def project(tokens, in_gain, query_gain, latent_gain, freqs, weights):
     rows, width = tokens.shape
     vmem = pl.BlockSpec(memory_space=pltpu.VMEM)
     dma = pltpu.SemaphoreType.DMA
-    wide = [min(w.shape) for w in weights]
+    wide = [min(w.shape) for w in weights[:5]]
+    half = freqs.shape[0]
     return pl.pallas_call(
         project_kernel,
         out_shape=(
-            jax.ShapeDtypeStruct((rows, wide[0]), bf16),
+            jax.ShapeDtypeStruct((weights[6].shape[1] // (2 * half), 128, rows), bf16),
             jax.ShapeDtypeStruct((rows, wide[1]), bf16),
             jax.ShapeDtypeStruct((rows, wide[2]), f32),
             jax.ShapeDtypeStruct((rows, wide[3]), bf16),
+            jax.ShapeDtypeStruct((half, rows), f32),
+            jax.ShapeDtypeStruct((half, rows), f32),
         ),
-        in_specs=[vmem] * 4 + [pl.BlockSpec(memory_space=pl.ANY)] * 5,
-        out_specs=(vmem,) * 4,
+        in_specs=[vmem] * 5 + [pl.BlockSpec(memory_space=pl.ANY)] * 7,
+        out_specs=(vmem,) * 6,
         scratch_shapes=[pltpu.VMEM((4, 2, rows // 2, width), bf16)]
         + [pltpu.VMEM(w.shape, bf16) for w in weights]
         + [pltpu.VMEM((rows, n), f32) for n in wide]
-        + [pltpu.VMEM((rows, 128), f32), dma((2, 2)), dma((4, 2)), dma((2,)), dma((5,))],
+        + [pltpu.VMEM((rows, 128), f32), dma((2, 2)), dma((4, 2)), dma((2,)), dma((7,))],
         compiler_params=pltpu.CompilerParams(
             collective_id=1, has_side_effects=True, vmem_limit_bytes=60 * 2**20
         ),
@@ -636,6 +661,7 @@
         in_gain.reshape(4, 1, width),
         query_gain[None],
         latent_gain[None],
+        freqs[:, None],
         *weights,
     )
 
@@ -661,15 +687,26 @@
     out_conv,
 ):
     row_count = tokens.shape[0]
-    positions = (lax.axis_index("sp") * row_count + jnp.arange(row_count)).astype(f32)
-    q_latent, kv_latent, rope_pre, glu = project(
+    half = rope_down.shape[1] // 2
+    freqs = theta ** (-jnp.arange(half).astype(f32) / half)
+    qt, kv_latent, rope_pre, glu, cosine, sine = project(
         tokens,
         in_gain,
         query_gain,
         latent_gain,
-        (query_down, latent_down, jnp.transpose(rope_down), conv_value, conv_gate),
+        freqs,
+        (
+            query_down,
+            latent_down,
+            jnp.transpose(rope_down),
+            conv_value,
+            conv_gate,
+            query_nope,
+            query_rope,
+        ),
     )
-    rope_key = rotate(rope_pre, positions).astype(bf16)
+    cosine, sine = jnp.transpose(cosine), jnp.transpose(sine)
+    rope_key = rotate(rope_pre, cosine, sine).astype(bf16)
     rope_size = rope_down.shape[1]
     heads = query_rope.shape[1] // rope_size
     nope = query_nope.shape[1] // heads
@@ -677,26 +714,9 @@
     packed = jnp.transpose(rope_key.reshape(2, 8, 16, rope_size), (0, 2, 1, 3)).reshape(2, 16, 8 * rope_size)
     xp = jnp.concatenate([kv_latent.reshape(2, row_count // 2, -1), packed], axis=1)
 
-    q_heads = (
-        jnp.dot(q_latent, query_nope, preferred_element_type=f32)
-        .astype(bf16)
-        .reshape(row_count, heads, nope)
-    )
-    q_turn = jnp.dot(q_latent, query_rope, preferred_element_type=f32).reshape(
-        row_count, heads, rope_size
-    )
-    r_heads = rotate(q_turn, positions[:, None]).astype(bf16)
-    empty = jnp.zeros((row_count, 64 - rope_size), bf16)
-    cols = []
-    for h in range(heads):
-        if h % 2 == 0:
-            cols += [q_heads[:, h], r_heads[:, h], empty]
-        else:
-            cols += [r_heads[:, h], empty, q_heads[:, h]]
-    q_own = jnp.transpose(jnp.concatenate(cols, axis=1))
     return attend(
         xp,
-        q_own.reshape(heads, 128, row_count),
+        qt,
         key_up,
         value_up,
         out_attend,

time: 85.9 us -> 90.6 us (1.055)
  local copies, waits for them, and re-layouts: 2.28 us -> 6.75 us
  matrix products: 2.45 us -> 0 us
  other arithmetic: 1.85 us -> 3.86 us
    dot_general x2 -> x0, matrix products: 2.45 us -> none  [the longest x1 1.23 us: per_device(): jnp.dot(q_latent, query_nope, preferred_element_type=f32).astype(bf16)]
    concatenate x2 -> x4, local copies, waits for them, and re-layouts: 0.04 us -> 2.43 us  [rotate(): jnp.concatenate([first * cosine - second * sine, second * cosine + first...]
    cos x1 -> x0, other arithmetic: 1.69 us -> none  [rotate(): cosine = jnp.cos(angles)]
    another operation x1, other arithmetic: 0.02 us -> 1.36 us
    pallas_call x0 -> x1, local copies, waits for them, and re-layouts: none -> 0.97 us  [project(): pl.pallas_call(project_kernel, out_shape=(jax.ShapeDtypeStruct((weights[6...]
    concatenate x1, other arithmetic: 0.01 us -> 0.93 us  [per_device(): jnp.concatenate([kv_latent.reshape(2, row_count // 2, -1), packed], axis=1)]
    unnamed x28 -> x19, local copies, waits for them, and re-layouts: 2 us -> 2.63 us
where the time goes in v8:
time: 90.6 us; the launch traced here: 89.3 us
  Pallas kernels  78.6 us (87%)
  local copies, waits for them, and re-layouts  6.75 us (7%)
  other arithmetic  3.86 us (4%)
    pallas_call x1, Pallas kernels, attend(): pl.pallas_call(functools.partial(attend_kernel, heads, scale), out_shape=...  63.2 us
    pallas_call x1, Pallas kernels, project(): pl.pallas_call(project_kernel, out_shape=(jax.ShapeDtypeStruct((weights[6...  15.4 us
    unnamed x19, local copies, waits for them, and re-layouts  2.63 us
    concatenate x4, local copies, waits for them, and re-layouts, rotate(): jnp.concatenate([first * cosine - second * sine, second * cosine + first...  2.43 us

profile of v8, /device:TPU:1, one launch (start us, length us, event | category | flops | bytes accessed | tf_op | source)
XLA Modules:
  0.0 89.3 jit_solution(13843330729386449851)
XLA Ops:
  0.0 0.6 multiply_power_fusion.freq_ref
  0.6 0.0 copy-start.6
  0.6 0.0 copy-start.7
  0.6 0.0 copy-start.8
  0.7 15.4 %project.1 = (bf16[4,128,256]{2,1,0:T(8,128)(2,1)}, bf16[256,256]{1,0:T(8,128)(2,1)}, f32[256,32]{1,0:T(8,128)}, bf16[256,512]{1,0:T(8,128)(2,1)}, f32[16,256]{1,0:T(8,128)}, /*index=5*/f32[16,256]{1,0:T(8,128)}) custom-call(bf16[2,128,512]{2,1,0:T(8,128)(2,1)} %bitcast.36, f32[4,1,512]{2,1,0:T(1,128)} %bitcast.39, f32[1,512]{1,0:T(1,128)} %bitcast.40, ...), custom_call_target="tpu_custom_call" | custom-call | flops 1912602624 | bytes 10000000 | tf_op jit(solution)/shard_map/project/pallas_call | solution.py:636
  16.1 1.0 %copy.19 = f32[256,32]{0,1:T(8,128)S(1)} copy(f32[256,32]{1,0:T(8,128)} %get-tuple-element.12) | data formatting | bytes 65536 | tf_op jit(solution)/shard_map/project/pallas_call | solution.py:636
  17.1 1.4 %fusion.1 = (bf16[256,16]{0,1:T(8,128)(2,1)}, bf16[256,16]{0,1:T(8,128)(2,1)S(1)}) fusion(f32[16,256]{1,0:T(8,128)} %get-tuple-element.14, f32[16,256]{1,0:T(8,128)} %get-tuple-element.13, f32[256,32]{0,1:T(8,128)S(1)} %copy.19), kind=kLoop, calls=%fused_computation.5 | loop fusion | flops 32768 | bytes 81920 | tf_op jit(solution)/shard_map/convert.3
  18.4 0.8 concatenate.12
  19.2 0.8 copy.21
  20.0 0.1 concatenate.13
  20.1 0.8 copy.22
  20.9 1.0 %maximum_bitcast_fusion = bf16[2,16,8,32]{3,2,1,0:T(8,128)(2,1)S(1)} fusion(bf16[2,8,16,16]{3,1,2,0:T(8,128)(2,1)} %copy.22, bf16[2,8,16,16]{3,1,2,0:T(8,128)(2,1)} %copy.21), kind=kLoop, calls=%fused_computation.1 | loop fusion | flops 32768 | bytes 32768 | tf_op jit(solution)/shard_map/transpose | solution.py:714
  21.8 0.7 reshape.36
  22.6 0.9 %pad_maximum_fusion.xp_ref = bf16[2,144,256]{2,1,0:T(8,128)(2,1)S(1)} fusion(bf16[2,16,256]{2,1,0:T(8,128)(2,1)} %reshape.36, bf16[2,128,256]{2,1,0:T(8,128)(2,1)} %bitcast.38), kind=kLoop, calls=%fused_computation | loop fusion | flops 294912 | bytes 294912 | tf_op jit(solution)/shard_map/concatenate | solution.py:715
  23.5 0.0 copy-done
  23.5 0.0 copy-done.1
  23.5 0.0 copy-done.4
  23.5 0.0 copy-done.5
  23.5 0.0 copy-done.6
  23.5 0.0 copy-done.7
  23.6 0.9 %copy-done.2 = bf16[4,128,256]{2,1,0:T(8,128)(2,1)S(1)} copy-done((bf16[4,128,256]{2,1,0:T(8,128)(2,1)S(1)}, bf16[4,128,256]{2,1,0:T(8,128)(2,1)}, u32[]{:S(2)}) %copy-start.2) | copy-done | bytes 262168
  24.5 0.9 %copy-done.3 = bf16[256,512]{1,0:T(8,128)(2,1)S(1)} copy-done((bf16[256,512]{1,0:T(8,128)(2,1)S(1)}, bf16[256,512]{1,0:T(8,128)(2,1)}, u32[]{:S(2)}) %copy-start.3) | copy-done | bytes 262168
  25.5 63.2 %attend.1 = bf16[256,512]{1,0:T(8,128)(2,1)S(1)} custom-call(bf16[2,144,256]{2,1,0:T(8,128)(2,1)S(1)} %pad_maximum_fusion.xp_ref, bf16[4,128,256]{2,1,0:T(8,128)(2,1)S(1)} %copy-done.2, bf16[256,256]{1,0:T(8,128)(2,1)S(1)} %copy-done.4, bf16[256,256]{1,0:T(8,128)(2,1)S(1)} %copy-done.5, bf16[256,2048]{1,0:T(8,128)(2,1)S(1)} %copy-done.1, ...), custom_call_target="tpu_custom_call" | custom-call | flops 10737418240 | bytes 2000000 | tf_op jit(solution)/shard_map/attend/pallas_call | solution.py:451
  88.6 0.7 copy.24
  (7 shorter events, 0.0 us)
Async XLA Ops:
  0.6 22.9 %copy-start = (bf16[512,2048]{1,0:T(8,128)(2,1)S(1)}, bf16[512,2048]{1,0:T(8,128)(2,1)}, u32[]{:S(2)}) copy-start(bf16[512,2048]{1,0:T(8,128)(2,1)} %oc_ref.1) | copy-start | bytes 6291460
  0.6 22.9 %copy-start.1 = (bf16[256,2048]{1,0:T(8,128)(2,1)S(1)}, bf16[256,2048]{1,0:T(8,128)(2,1)}, u32[]{:S(2)}) copy-start(bf16[256,2048]{1,0:T(8,128)(2,1)} %wa_ref.1) | copy-start | bytes 3145732
  0.6 22.9 %copy-start.4 = (bf16[256,256]{1,0:T(8,128)(2,1)S(1)}, bf16[256,256]{1,0:T(8,128)(2,1)}, u32[]{:S(2)}) copy-start(bf16[256,256]{1,0:T(8,128)(2,1)} %ku_ref.1) | copy-start | bytes 393220
  0.6 22.9 %copy-start.5 = (bf16[256,256]{1,0:T(8,128)(2,1)S(1)}, bf16[256,256]{1,0:T(8,128)(2,1)}, u32[]{:S(2)}) copy-start(bf16[256,256]{1,0:T(8,128)(2,1)} %vu_ref.1) | copy-start | bytes 393220
  0.6 22.9 %copy-start.6 = (f32[31,512]{1,0:T(8,128)S(1)}, f32[31,512]{1,0:T(8,128)}, u32[]{:S(2)}) copy-start(f32[31,512]{1,0:T(8,128)} %taps_ref.1) | copy-start | bytes 190468
  0.6 22.9 %copy-start.7 = (f32[512]{0:T(512)S(1)}, f32[512]{0:T(512)}, u32[]{:S(2)}) copy-start(f32[512]{0:T(512)} %param.32) | copy-start | bytes 6148
  0.6 22.9 %copy-start.8 = (f32[512]{0:T(512)S(1)}, f32[512]{0:T(512)}, u32[]{:S(2)}) copy-start(f32[512]{0:T(512)} %param.33) | copy-start | bytes 6148
  23.6 1.0 %copy-start.2 = (bf16[4,128,256]{2,1,0:T(8,128)(2,1)S(1)}, bf16[4,128,256]{2,1,0:T(8,128)(2,1)}, u32[]{:S(2)}) copy-start(bf16[4,128,256]{2,1,0:T(8,128)(2,1)} %get-tuple-element.15.qt_ref) | copy-start | bytes 786436
  24.5 0.9 %copy-start.3 = (bf16[256,512]{1,0:T(8,128)(2,1)S(1)}, bf16[256,512]{1,0:T(8,128)(2,1)}, u32[]{:S(2)}) copy-start(bf16[256,512]{1,0:T(8,128)(2,1)} %get-tuple-element.16.glu_ref) | copy-start | bytes 786436
